TPU v7x, 128 devices: a whole 4x4x4 slice. The times are simulated.
128 devices in a mesh: ra: 16 (over z, x), cb: 4 (over y), dp: 2 (over core).
Axes of the slice: x: 4, y: 4, z: 4, core: 2. Of those that a mesh axis runs over, the one named last changes fastest.
Arguments:
- carried: bfloat16 [3072, 4096], P('dp', 'ra'), may hold values from -100 to 100
- branch_in: bfloat16 [3072, 4096], P('dp', 'ra'), may hold values from -12 to 12
- gain_in: float32 [4096], P('ra'), may hold values from 0.1 to 1.9
- bias_in: float32 [4096], P('ra'), may hold values from -1.8 to 1.8
- up_weight: bfloat16 [4096, 16384], P('ra', 'cb'), may hold values from -0.125 to 0.125
- down_weight: bfloat16 [16384, 4096], P('cb', 'ra'), may hold values from -0.046875 to 0.046875
- gain_out: float32 [4096], P('ra'), may hold values from 0.1 to 1.9
- bias_out: float32 [4096], P('ra'), may hold values from -1.8 to 1.8
Outputs:
- layer_out: bfloat16 [3072, 4096], P('dp', 'ra')
All inputs are finite; a program needn't handle non-finite values.
Results may differ from a plain program's by a relative error of at most 0.006.
Values may be sent and summed in bfloat16 or wider, within the bound.
No kernel may reach another device: no remote copies, remote signals or barrier semaphores. Data moves between devices by JAX's collectives and lax.ppermute only.
A program may use at most 64 MiB of HBM per device.

v0:
```python
import jax
import jax.numpy as jnp
from jax import lax
from jax.experimental import pallas as pl
from jax.experimental.pallas import tpu as pltpu
from jax.sharding import PartitionSpec as P


residual_scale = 2.0**0.25
norm_eps = 1e-05
others = (1, 3, 2)
f32, bf16 = jnp.float32, jnp.bfloat16


def ring_pairs(gathers, distance):
    pairs = []
    for z in range(4):
        for x in range(4):
            for c in range(2):
                if (c == 0) == gathers:
                    source = (z * 4 + (x + distance) % 4) * 2 + c
                else:
                    source = (((z + distance) % 4) * 4 + x) * 2 + c
                pairs.append((source, (z * 4 + x) * 2 + c))
    return pairs


def from_gather_ring(array, distance):
    return lax.ppermute(array, ("ra", "dp"), ring_pairs(True, distance % 4))


def from_sum_ring(array, distance):
    return lax.ppermute(array, ("ra", "dp"), ring_pairs(False, distance % 4))


def from_plane(array, distance):
    return lax.ppermute(array, "cb", [((y + distance) % 4, y) for y in range(4)])


def from_other_core(array):
    return lax.ppermute(array, "dp", [(0, 1), (1, 0)])


def dot(a, b):
    return lax.dot_general(a, b, (((1,), (0,)), ((), ())), preferred_element_type=f32)


def call(body, out_shape, flops, *operands):
    size = sum(o.size * o.dtype.itemsize for o in operands)
    return pl.pallas_call(
        body,
        out_shape=out_shape,
        in_specs=[pl.BlockSpec(memory_space=pltpu.VMEM)] * len(operands),
        out_specs=[pl.BlockSpec(memory_space=pltpu.VMEM)] * len(out_shape),
        compiler_params=pltpu.CompilerParams(vmem_limit_bytes=24 * 2**20),
        cost_estimate=pl.CostEstimate(flops=flops, bytes_accessed=size, transcendentals=0),
    )(*operands)


def up_products(features, weights):
    rows = features.shape[0] // 4
    flat = [w for ws in weights for w in ws]
    counts = [len(ws) for ws in weights]
    wide = flat[0].shape[-1]

    def up(*refs):
        a_ref, w_refs, outs = refs[0], refs[1 : 1 + len(flat)], refs[1 + len(flat) :]
        for i, out in enumerate(outs):
            at = 0
            for n, count in enumerate(counts):
                total, depth = None, 0
                for w_ref in w_refs[at : at + count]:
                    k = w_ref.shape[0]
                    term = dot(a_ref[i * rows : (i + 1) * rows, depth : depth + k], w_ref[...])
                    total = term if total is None else total + term
                    depth += k
                at += count
                out[:, n * wide : (n + 1) * wide] = total.astype(out.dtype)

    full = wide * len(weights)
    shapes = [jax.ShapeDtypeStruct((rows, full), f32 if i == 0 else bf16) for i in range(4)]
    return call(up, shapes, 2 * features.size * full, features, *flat)


def down_products(hidden, weights, start, last):
    rows = hidden[0].shape[0]
    flat = [w for ws in weights for w in ws]
    counts = [len(ws) for ws in weights]
    wide = flat[0].shape[0]
    begun = [] if start is None else list(start)

    def down(*refs):
        h_refs, refs = refs[:4], refs[4:]
        w_refs, refs = refs[: len(flat)], refs[len(flat) :]
        s_refs, outs = refs[: len(begun)], refs[len(begun) :]
        for i, h_ref in enumerate(h_refs):
            for j, out in enumerate(outs):
                cols = slice(j * out.shape[1], (j + 1) * out.shape[1])
                total = s_refs[j][i * rows : (i + 1) * rows, :] if begun else None
                at = 0
                for n, count in enumerate(counts):
                    depth = 0
                    for w_ref in w_refs[at : at + count]:
                        w = w_ref.shape[1]
                        if depth <= cols.start < depth + w:
                            term = dot(
                                h_ref[:, n * wide : (n + 1) * wide],
                                w_ref[:, cols.start - depth : cols.stop - depth],
                            )
                            total = term if total is None else total + term
                        depth += w
                    at += count
                out[i * rows : (i + 1) * rows, :] = total.astype(out.dtype)

    each = sum(w.shape[1] for w in weights[0]) // 4
    shapes = [
        jax.ShapeDtypeStruct((4 * rows, each), bf16 if last and j else f32) for j in range(4)
    ]
    flops = 2 * 4 * rows * wide * len(weights) * 4 * each
    return call(down, shapes, flops, *hidden, *flat, *begun)


def group_sums(mixed, width):
    sums = jnp.stack([jnp.sum(mixed, axis=1), jnp.sum(mixed * mixed, axis=1)])
    members = lax.axis_size("ra")
    sent = jnp.broadcast_to(sums.reshape(1, -1, 128), (members, sums.size // 128, 128))
    sums = lax.all_to_all(sent, "ra", 0, 0, tiled=True)
    sums = sums.sum(axis=0).reshape(2, -1)
    return sums[0][:, None] / width, sums[1][:, None] / width


def normalize(mixed, width, gain, bias):
    mean, square = group_sums(mixed, width)
    return (mixed - mean) * lax.rsqrt(square - mean * mean + norm_eps) * gain + bias


def layer(carried, branch_in, gain_in, bias_in, up_weight, down_weight, gain_out, bias_out):
    width = carried.shape[1] * lax.axis_size("ra")
    r, y, c = lax.axis_index("ra"), lax.axis_index("cb"), lax.axis_index("dp")
    z, x = r // 4, r % 4
    a, b = jnp.where(c == 0, x, z), jnp.where(c == 0, z, x)
    held = carried.shape[1]
    few = carried.shape[0] // 4
    half = few // 2
    wide = up_weight.shape[1] // 8

    def columns_for(distance):
        return (c * 4 + (a + distance) % 4) * wide

    def up_for(distance):
        return lax.dynamic_slice(up_weight, (0, columns_for(distance)), (held, wide))

    def down_for(distance):
        return lax.dynamic_slice(down_weight, (columns_for(distance), 0), (wide, held))

    up_own, down_own = up_for(0), down_for(0)
    uo = {d: from_plane(up_own, d) for d in (1, 3)}
    do = {d: from_plane(down_own, d) for d in (1, 3)}
    up_rest = jnp.concatenate([from_gather_ring(up_for(-j), j) for j in others], axis=0)
    ur = {d: from_plane(up_rest, d) for d in (1, 3)}
    up_far = (
        from_plane(jnp.concatenate([uo[1], ur[1][:held]], axis=0), 1), from_plane(ur[3][held:], 3)
    )
    down_rest = jnp.concatenate([from_gather_ring(down_for(-j), j) for j in others], axis=1)
    dr = {d: from_plane(down_rest, d) for d in (1, 3)}
    down_far = (
        from_plane(jnp.concatenate([do[1], dr[1][:, :held]], axis=1), 1),
        from_plane(dr[3][:, held:], 3),
    )

    def quarter(array):
        return lax.dynamic_slice(array, (y * few, 0), (few, held)).astype(f32)

    mixed_in = residual_scale * quarter(carried) + quarter(branch_in)
    normed = normalize(mixed_in, width, gain_in, bias_in).astype(bf16)
    both = jnp.concatenate([normed, from_other_core(normed)], axis=0)
    turn = (b - 2 * c) % 4
    turned = lax.dynamic_slice(jnp.concatenate([both, both], axis=0), (turn * half, 0), both.shape)
    features = jnp.concatenate([turned] + [from_gather_ring(turned, j) for j in others], axis=1)

    def activated(parts):
        total = parts[0]
        for j in (1, 2, 3):
            total = total + from_sum_ring(parts[j], -j).astype(f32)
        own = jnp.square(jnp.maximum(total, 0.0)).astype(bf16)
        return [own] + [from_sum_ring(own, j) for j in (1, 2, 3)]

    near = activated(up_products(features, [(up_own, up_rest)] + [(uo[d], ur[d]) for d in (1, 3)]))
    far = activated(up_products(features, [up_far]))
    begun = down_products(
        near, [(down_own, down_rest)] + [(do[d], dr[d]) for d in (1, 3)], None, False
    )
    parts = down_products(far, [down_far], begun, True)
    total = parts[0]
    for j, part in zip(others, parts[1:]):
        total = total + from_gather_ring(part, -j).astype(f32)
    total = jnp.concatenate([total, total], axis=0)
    mine = lax.dynamic_slice(total, ((-turn) % 4 * half, 0), (few, held))
    theirs = lax.dynamic_slice(total, ((2 - turn) % 4 * half, 0), (few, held))
    mixed_out = residual_scale * normed.astype(f32) + (mine + from_other_core(theirs))
    out = normalize(mixed_out, width, gain_out, bias_out).astype(bf16)
    result = jnp.zeros(carried.shape, bf16)
    for d in range(4):
        block = out if d == 0 else from_plane(out, d)
        result = lax.dynamic_update_slice(result, block, ((y + d) % 4 * few, 0))
    return result


def solution(mesh):
    in_specs = (
        P("dp", "ra"),
        P("dp", "ra"),
        P("ra"),
        P("ra"),
        P("ra", "cb"),
        P("cb", "ra"),
        P("ra"),
        P("ra"),
    )
    return jax.shard_map(
        layer, mesh=mesh, in_specs=in_specs, out_specs=P("dp", "ra"), check_vma=False
    )
```

profile of v0, /device:TPU:0, one launch (start us, length us, event | category | flops | bytes accessed | tf_op | source)
XLA Modules:
  0.0 169.6 jit_solution(12905912802640421537)
XLA Ops:
  1.9 8.0 %all-to-all-start = ((f32[16,6,128]{2,1,0:T(8,128)}), f32[16,6,128]{2,1,0:T(8,128)S(1)}, u32[]{:S(2)}, u32[]{:S(2)}) async-start(f32[16,6,128]{2,1,0:T(8,128)} %broadcast_in_dim.23), calls=%async_computation | async-start | bytes 131072 | tf_op jit(solution)/shard_map/all_to_all | solution.py:127
  11.3 3.1 %collective-permute-start.5 = (bf16[256,512]{1,0:T(8,128)(2,1)S(1)}, bf16[256,512]{1,0:T(8,128)(2,1)}, u32[]{:S(2)}, u32[]{:S(2)}) collective-permute-start(bf16[256,512]{1,0:T(8,128)(2,1)S(1)} %get-tuple-element.49), channel_id=1, source_target_pairs={{8,0},{33,1},{16,8},{41,9},{24,16},{49,17},{0,24},{57,25},{40,32},... | collective-permute-start | bytes 786440 | tf_op jit(solution)/shard_map/ppermute | solution.py:29
  22.1 3.1 %collective-permute-done.6 = bf16[256,512]{1,0:T(8,128)(2,1)} collective-permute-done((bf16[256,512]{1,0:T(8,128)(2,1)S(1)}, bf16[256,512]{1,0:T(8,128)(2,1)}, u32[]{:S(2)}, u32[]{:S(2)}) %collective-permute-start.6) | collective-permute-done | bytes 262176 | tf_op jit(solution)/shard_map/ppermute | solution.py:29
  33.9 2.5 %collective-permute-start.1 = (bf16[768,256]{1,0:T(8,128)(2,1)S(1)}, bf16[768,256]{1,0:T(8,128)(2,1)S(1)}, u32[]{:S(2)}, u32[]{:S(2)}) collective-permute-start(bf16[768,256]{1,0:T(8,128)(2,1)S(1)} %fusion.2), channel_id=1, source_target_pairs={{8,0},{33,1},{16,8},{41,9},{24,16},{49,17},{0,24},{57,25},{40,32},... | collective-permute-start | bytes 1179656 | tf_op jit(solution)/shard_map/ppermute | solution.py:29
  36.5 5.3 %collective-permute-done.3 = bf16[768,256]{1,0:T(8,128)(2,1)S(1)} collective-permute-done((bf16[768,256]{1,0:T(8,128)(2,1)S(1)}, bf16[768,256]{1,0:T(8,128)(2,1)S(1)}, u32[]{:S(2)}, u32[]{:S(2)}) %collective-permute-start.3) | collective-permute-done | bytes 393248 | tf_op jit(solution)/shard_map/ppermute | solution.py:29
  49.5 2.4 %collective-permute-done.4.refs_3_ = bf16[256,512]{1,0:T(8,128)(2,1)S(1)} collective-permute-done((bf16[256,512]{1,0:T(8,128)(2,1)S(1)}, bf16[256,512]{1,0:T(8,128)(2,1)S(1)}, u32[]{:S(2)}, u32[]{:S(2)}) %collective-permute-start.4) | collective-permute-done | bytes 262176 | tf_op jit(solution)/shard_map/ppermute | solution.py:37
  55.2 2.6 %shard_map.83 = (f32[192,1536]{1,0:T(8,128)S(1)}, bf16[192,1536]{1,0:T(8,128)(2,1)S(1)}, bf16[192,1536]{1,0:T(8,128)(2,1)S(1)}, bf16[192,1536]{1,0:T(8,128)(2,1)S(1)}) custom-call(bf16[768,1024]{1,0:T(8,128)(2,1)S(1)} %pad_maximum_fusion.refs_0_, bf16[256,512]{1,0:T(8,128)(2,1)S(1)} %get-tuple-element.48.refs_1_, ...), custom_call_target="tpu_custom_call" | custom-call | flops 2415919104 | bytes 4718592 | tf_op jit(solution)/shard_map/pallas_call | solution.py:50
  57.8 3.2 %collective-permute-start.27 = (bf16[192,1536]{1,0:T(8,128)(2,1)S(1)}, bf16[192,1536]{1,0:T(8,128)(2,1)S(1)}, u32[]{:S(2)}, u32[]{:S(2)}) collective-permute-start(bf16[192,1536]{1,0:T(8,128)(2,1)S(1)} %get-tuple-element.26), channel_id=1, source_target_pairs={{96,0},{25,1},{104,8},{1,9},{112,16},{9,17},{120,24},{17,25},{0,32... | collective-permute-start | bytes 1769480 | tf_op jit(solution)/shard_map/ppermute | solution.py:33
  61.0 2.5 %collective-permute-start.28 = (bf16[192,1536]{1,0:T(8,128)(2,1)S(1)}, bf16[192,1536]{1,0:T(8,128)(2,1)S(1)}, u32[]{:S(2)}, u32[]{:S(2)}) collective-permute-start(bf16[192,1536]{1,0:T(8,128)(2,1)S(1)} %get-tuple-element.27), channel_id=1, source_target_pairs={{64,0},{17,1},{72,8},{25,9},{80,16},{1,17},{88,24},{9,25},{96,32},... | collective-permute-start | bytes 1769480 | tf_op jit(solution)/shard_map/ppermute | solution.py:33
  71.5 6.2 %collective-permute-done.28 = bf16[192,1536]{1,0:T(8,128)(2,1)S(1)} collective-permute-done((bf16[192,1536]{1,0:T(8,128)(2,1)S(1)}, bf16[192,1536]{1,0:T(8,128)(2,1)S(1)}, u32[]{:S(2)}, u32[]{:S(2)}) %collective-permute-start.28) | collective-permute-done | bytes 589856 | tf_op jit(solution)/shard_map/ppermute | solution.py:33
  79.6 8.4 %collective-permute-done.33.refs_8_ = bf16[512,256]{1,0:T(8,128)(2,1)S(1)} collective-permute-done((bf16[512,256]{1,0:T(8,128)(2,1)S(1)}, bf16[512,256]{1,0:T(8,128)(2,1)S(1)}, u32[]{:S(2)}, u32[]{:S(2)}) %collective-permute-start.33) | collective-permute-done | bytes 262176 | tf_op jit(solution)/shard_map/ppermute | solution.py:37
  87.9 2.9 %collective-permute-start.31 = (bf16[192,1536]{1,0:T(8,128)(2,1)S(1)}, bf16[192,1536]{1,0:T(8,128)(2,1)S(1)}, u32[]{:S(2)}, u32[]{:S(2)}) collective-permute-start(bf16[192,1536]{1,0:T(8,128)(2,1)S(1)} %multiply_convert_fusion.refs_0_), channel_id=1, source_target_pairs={{64,0},{17,1},{72,8},{25,9},{80,16},{1,17},{88,24},{9,25},{96,32},... | collective-permute-start | bytes 1769480 | tf_op jit(solution)/shard_map/ppermute | solution.py:33
  95.7 11.1 %collective-permute-done.13 = bf16[192,512]{1,0:T(8,128)(2,1)S(1)} collective-permute-done((bf16[192,512]{1,0:T(8,128)(2,1)S(1)}, bf16[192,512]{1,0:T(8,128)(2,1)S(1)}, u32[]{:S(2)}, u32[]{:S(2)}) %collective-permute-start.13) | collective-permute-done | bytes 196640 | tf_op jit(solution)/shard_map/ppermute | solution.py:33
  106.8 3.7 %collective-permute-done.14 = bf16[192,512]{1,0:T(8,128)(2,1)S(1)} collective-permute-done((bf16[192,512]{1,0:T(8,128)(2,1)S(1)}, bf16[192,512]{1,0:T(8,128)(2,1)S(1)}, u32[]{:S(2)}, u32[]{:S(2)}) %collective-permute-start.14) | collective-permute-done | bytes 196640 | tf_op jit(solution)/shard_map/ppermute | solution.py:33
  113.3 2.7 %collective-permute-start.16 = (bf16[192,512]{1,0:T(8,128)(2,1)S(1)}, bf16[192,512]{1,0:T(8,128)(2,1)S(1)}, u32[]{:S(2)}, u32[]{:S(2)}) collective-permute-start(bf16[192,512]{1,0:T(8,128)(2,1)S(1)} %multiply_convert_fusion.1.refs_0_), channel_id=1, source_target_pairs={{64,0},{17,1},{72,8},{25,9},{80,16},{1,17},{88,24},{9,25},{96,32},... | collective-permute-start | bytes 589832 | tf_op jit(solution)/shard_map/ppermute | solution.py:33
  116.6 2.6 %shard_map.84 = (f32[768,256]{1,0:T(8,128)S(1)}, f32[768,256]{1,0:T(8,128)S(1)}, f32[768,256]{1,0:T(8,128)S(1)}, f32[768,256]{1,0:T(8,128)S(1)}) custom-call(bf16[192,1536]{1,0:T(8,128)(2,1)S(1)} %multiply_convert_fusion.refs_0_, bf16[192,1536]{1,0:T(8,128)(2,1)S(1)} %collective-permute-done.30.refs_1_, ...), custom_call_target="tpu_custom_call" | custom-call | flops 2415919104 | bytes 5505024 | tf_op jit(solution)/shard_map/pallas_call | solution.py:50
  124.6 5.8 %collective-permute-start.34 = (bf16[768,256]{1,0:T(8,128)(2,1)S(1)}, bf16[768,256]{1,0:T(8,128)(2,1)S(1)}, u32[]{:S(2)}, u32[]{:S(2)}) collective-permute-start(bf16[768,256]{1,0:T(8,128)(2,1)S(1)} %get-tuple-element.34), channel_id=1, source_target_pairs={{24,0},{97,1},{0,8},{105,9},{8,16},{113,17},{16,24},{121,25},{56,3... | collective-permute-start | bytes 1179656 | tf_op jit(solution)/shard_map/ppermute | solution.py:29
  131.2 2.7 %collective-permute-start.36 = (bf16[768,256]{1,0:T(8,128)(2,1)S(1)}, bf16[768,256]{1,0:T(8,128)(2,1)S(1)}, u32[]{:S(2)}, u32[]{:S(2)}) collective-permute-start(bf16[768,256]{1,0:T(8,128)(2,1)S(1)} %get-tuple-element.36), channel_id=1, source_target_pairs={{16,0},{65,1},{24,8},{73,9},{0,16},{81,17},{8,24},{89,25},{48,32},... | collective-permute-start | bytes 1179656 | tf_op jit(solution)/shard_map/ppermute | solution.py:29
  133.9 3.0 %collective-permute-done.34 = bf16[768,256]{1,0:T(8,128)(2,1)S(1)} collective-permute-done((bf16[768,256]{1,0:T(8,128)(2,1)S(1)}, bf16[768,256]{1,0:T(8,128)(2,1)S(1)}, u32[]{:S(2)}, u32[]{:S(2)}) %collective-permute-start.34) | collective-permute-done | bytes 393248 | tf_op jit(solution)/shard_map/ppermute | solution.py:29
  138.2 4.4 %collective-permute-done.36 = bf16[768,256]{1,0:T(8,128)(2,1)S(1)} collective-permute-done((bf16[768,256]{1,0:T(8,128)(2,1)S(1)}, bf16[768,256]{1,0:T(8,128)(2,1)S(1)}, u32[]{:S(2)}, u32[]{:S(2)}) %collective-permute-start.36) | collective-permute-done | bytes 393248 | tf_op jit(solution)/shard_map/ppermute | solution.py:29
  145.6 3.9 %all-to-all-start.1 = ((f32[16,6,128]{2,1,0:T(8,128)}), f32[16,6,128]{2,1,0:T(8,128)S(1)}, u32[]{:S(2)}, u32[]{:S(2)}) async-start(f32[16,6,128]{2,1,0:T(8,128)} %broadcast_in_dim.25), calls=%async_computation.1 | async-start | bytes 131072 | tf_op jit(solution)/shard_map/all_to_all | solution.py:127
  149.6 7.6 %all-to-all-done.1 = f32[16,6,128]{2,1,0:T(8,128)S(1)} async-done(((f32[16,6,128]{2,1,0:T(8,128)}), f32[16,6,128]{2,1,0:T(8,128)S(1)}, u32[]{:S(2)}, u32[]{:S(2)}) %all-to-all-start.1) | async-done | bytes 49184 | tf_op jit(solution)/shard_map/all_to_all | solution.py:127
  157.6 2.6 %collective-permute-start.39 = (bf16[384,256]{1,0:T(8,128)(2,1)S(1)}, bf16[384,256]{1,0:T(8,128)(2,1)S(1)}, u32[]{:S(2)}, u32[]{:S(2)}) collective-permute-start(bf16[384,256]{1,0:T(8,128)(2,1)S(1)} %get-tuple-element.42), channel_id=1, source_target_pairs={{4,0},{6,2},{0,4},{2,6},{5,1},{7,3},{1,5},{3,7},{12,8},{14,10},{8,... | collective-permute-start | bytes 589832 | tf_op jit(solution)/shard_map/ppermute | solution.py:37
  160.2 5.0 %collective-permute-done.38 = bf16[384,256]{1,0:T(8,128)(2,1)S(1)} collective-permute-done((bf16[384,256]{1,0:T(8,128)(2,1)S(1)}, bf16[384,256]{1,0:T(8,128)(2,1)S(1)}, u32[]{:S(2)}, u32[]{:S(2)}) %collective-permute-start.38) | collective-permute-done | bytes 196640 | tf_op jit(solution)/shard_map/ppermute | solution.py:37
  (122 shorter events, 63.7 us)
Async XLA Ops:
  1.9 15.7 %all-to-all-start = ((f32[16,6,128]{2,1,0:T(8,128)}), f32[16,6,128]{2,1,0:T(8,128)S(1)}, u32[]{:S(2)}, u32[]{:S(2)}) async-start(f32[16,6,128]{2,1,0:T(8,128)} %broadcast_in_dim.23), calls=%async_computation | async-start | bytes 131072 | tf_op jit(solution)/shard_map/all_to_all | solution.py:127
  14.4 11.8 %collective-permute-start.7 = (bf16[256,512]{1,0:T(8,128)(2,1)S(1)}, bf16[256,512]{1,0:T(8,128)(2,1)}, u32[]{:S(2)}, u32[]{:S(2)}) collective-permute-start(bf16[256,512]{1,0:T(8,128)(2,1)S(1)} %get-tuple-element.50), channel_id=1, source_target_pairs={{16,0},{65,1},{24,8},{73,9},{0,16},{81,17},{8,24},{89,25},{48,32},... | collective-permute-start | bytes 786440 | tf_op jit(solution)/shard_map/ppermute | solution.py:29
  27.2 19.9 %collective-permute-start.10 = (bf16[768,512]{1,0:T(8,128)(2,1)S(1)}, bf16[768,512]{1,0:T(8,128)(2,1)S(1)}, u32[]{:S(2)}, u32[]{:S(2)}) collective-permute-start(bf16[768,512]{1,0:T(8,128)(2,1)S(1)} %constant_dynamic-update-slice_fusion.refs_2_), channel_id=1, source_target_pairs={{6,0},{0,2},{2,4},{4,6},{7,1},{1,3},{3,5},{5,7},{14,8},{8,10},{10,... | collective-permute-start | bytes 2359304 | tf_op jit(solution)/shard_map/ppermute | solution.py:37
  28.8 20.2 %collective-permute-start.8 = (bf16[768,512]{1,0:T(8,128)(2,1)S(1)}, bf16[768,512]{1,0:T(8,128)(2,1)S(1)}, u32[]{:S(2)}, u32[]{:S(2)}) collective-permute-start(bf16[768,512]{1,0:T(8,128)(2,1)S(1)} %constant_dynamic-update-slice_fusion.refs_2_), channel_id=1, source_target_pairs={{2,0},{4,2},{6,4},{0,6},{3,1},{5,3},{7,5},{1,7},{10,8},{12,10},{14... | collective-permute-start | bytes 2359304 | tf_op jit(solution)/shard_map/ppermute | solution.py:37
  33.2 12.6 %collective-permute-start.2 = (bf16[768,256]{1,0:T(8,128)(2,1)S(1)}, bf16[768,256]{1,0:T(8,128)(2,1)S(1)}, u32[]{:S(2)}, u32[]{:S(2)}) collective-permute-start(bf16[768,256]{1,0:T(8,128)(2,1)S(1)} %fusion.2), channel_id=1, source_target_pairs={{24,0},{97,1},{0,8},{105,9},{8,16},{113,17},{16,24},{121,25},{56,3... | collective-permute-start | bytes 1179656 | tf_op jit(solution)/shard_map/ppermute | solution.py:29
  33.9 12.3 %collective-permute-start.1 = (bf16[768,256]{1,0:T(8,128)(2,1)S(1)}, bf16[768,256]{1,0:T(8,128)(2,1)S(1)}, u32[]{:S(2)}, u32[]{:S(2)}) collective-permute-start(bf16[768,256]{1,0:T(8,128)(2,1)S(1)} %fusion.2), channel_id=1, source_target_pairs={{8,0},{33,1},{16,8},{41,9},{24,16},{49,17},{0,24},{57,25},{40,32},... | collective-permute-start | bytes 1179656 | tf_op jit(solution)/shard_map/ppermute | solution.py:29
  47.1 13.9 %collective-permute-start.21 = (bf16[512,256]{1,0:T(8,128)(2,1)S(1)}, bf16[512,256]{1,0:T(8,128)(2,1)S(1)}, u32[]{:S(2)}, u32[]{:S(2)}) collective-permute-start(bf16[512,256]{1,0:T(8,128)(2,1)S(1)} %get-tuple-element.46), channel_id=1, source_target_pairs={{16,0},{65,1},{24,8},{73,9},{0,16},{81,17},{8,24},{89,25},{48,32},... | collective-permute-start | bytes 786440 | tf_op jit(solution)/shard_map/ppermute | solution.py:29
  49.0 14.5 %collective-permute-start.20 = (bf16[512,256]{1,0:T(8,128)(2,1)S(1)}, bf16[512,256]{1,0:T(8,128)(2,1)S(1)}, u32[]{:S(2)}, u32[]{:S(2)}) collective-permute-start(bf16[512,256]{1,0:T(8,128)(2,1)S(1)} %get-tuple-element.47), channel_id=1, source_target_pairs={{24,0},{97,1},{0,8},{105,9},{8,16},{113,17},{16,24},{121,25},{56,3... | collective-permute-start | bytes 786440 | tf_op jit(solution)/shard_map/ppermute | solution.py:29
  51.8 13.4 %collective-permute-start.11 = (bf16[512,512]{1,0:T(8,128)(2,1)S(1)}, bf16[512,512]{1,0:T(8,128)(2,1)S(1)}, u32[]{:S(2)}, u32[]{:S(2)}) collective-permute-start(bf16[512,512]{1,0:T(8,128)(2,1)S(1)} %slice.37), channel_id=1, source_target_pairs={{6,0},{0,2},{2,4},{4,6},{7,1},{1,3},{3,5},{5,7},{14,8},{8,10},{10,... | collective-permute-start | bytes 1572872 | tf_op jit(solution)/shard_map/ppermute | solution.py:37
  54.0 12.8 %collective-permute-start.9 = (bf16[512,512]{1,0:T(8,128)(2,1)S(1)}, bf16[512,512]{1,0:T(8,128)(2,1)S(1)}, u32[]{:S(2)}, u32[]{:S(2)}) collective-permute-start(bf16[512,512]{1,0:T(8,128)(2,1)S(1)} %pad_maximum_fusion.1), channel_id=1, source_target_pairs={{2,0},{4,2},{6,4},{0,6},{3,1},{5,3},{7,5},{1,7},{10,8},{12,10},{14... | collective-permute-start | bytes 1572872 | tf_op jit(solution)/shard_map/ppermute | solution.py:37
  57.8 12.1 %collective-permute-start.27 = (bf16[192,1536]{1,0:T(8,128)(2,1)S(1)}, bf16[192,1536]{1,0:T(8,128)(2,1)S(1)}, u32[]{:S(2)}, u32[]{:S(2)}) collective-permute-start(bf16[192,1536]{1,0:T(8,128)(2,1)S(1)} %get-tuple-element.26), channel_id=1, source_target_pairs={{96,0},{25,1},{104,8},{1,9},{112,16},{9,17},{120,24},{17,25},{0,32... | collective-permute-start | bytes 1769480 | tf_op jit(solution)/shard_map/ppermute | solution.py:33
  61.0 16.7 %collective-permute-start.28 = (bf16[192,1536]{1,0:T(8,128)(2,1)S(1)}, bf16[192,1536]{1,0:T(8,128)(2,1)S(1)}, u32[]{:S(2)}, u32[]{:S(2)}) collective-permute-start(bf16[192,1536]{1,0:T(8,128)(2,1)S(1)} %get-tuple-element.27), channel_id=1, source_target_pairs={{64,0},{17,1},{72,8},{25,9},{80,16},{1,17},{88,24},{9,25},{96,32},... | collective-permute-start | bytes 1769480 | tf_op jit(solution)/shard_map/ppermute | solution.py:33
  63.5 15.1 %collective-permute-start.29 = (bf16[192,1536]{1,0:T(8,128)(2,1)S(1)}, bf16[192,1536]{1,0:T(8,128)(2,1)S(1)}, u32[]{:S(2)}, u32[]{:S(2)}) collective-permute-start(bf16[192,1536]{1,0:T(8,128)(2,1)S(1)} %get-tuple-element.28), channel_id=1, source_target_pairs={{32,0},{9,1},{40,8},{17,9},{48,16},{25,17},{56,24},{1,25},{64,32},... | collective-permute-start | bytes 1769480 | tf_op jit(solution)/shard_map/ppermute | solution.py:33
  65.2 25.6 %collective-permute-start.24 = (bf16[512,768]{1,0:T(8,128)(2,1)S(1)}, bf16[512,768]{1,0:T(8,128)(2,1)S(1)}, u32[]{:S(2)}, u32[]{:S(2)}) collective-permute-start(bf16[512,768]{1,0:T(8,128)(2,1)S(1)} %constant_dynamic-update-slice_fusion.3.refs_5_), channel_id=1, source_target_pairs={{6,0},{0,2},{2,4},{4,6},{7,1},{1,3},{3,5},{5,7},{14,8},{8,10},{10,... | collective-permute-start | bytes 2359304 | tf_op jit(solution)/shard_map/ppermute | solution.py:37
  66.8 25.3 %collective-permute-start.22 = (bf16[512,768]{1,0:T(8,128)(2,1)S(1)}, bf16[512,768]{1,0:T(8,128)(2,1)S(1)}, u32[]{:S(2)}, u32[]{:S(2)}) collective-permute-start(bf16[512,768]{1,0:T(8,128)(2,1)S(1)} %constant_dynamic-update-slice_fusion.3.refs_5_), channel_id=1, source_target_pairs={{2,0},{4,2},{6,4},{0,6},{3,1},{5,3},{7,5},{1,7},{10,8},{12,10},{14... | collective-permute-start | bytes 2359304 | tf_op jit(solution)/shard_map/ppermute | solution.py:37
  69.9 18.0 %collective-permute-start.33 = (bf16[512,256]{1,0:T(8,128)(2,1)S(1)}, bf16[512,256]{1,0:T(8,128)(2,1)S(1)}, u32[]{:S(2)}, u32[]{:S(2)}) collective-permute-start(bf16[512,256]{1,0:T(8,128)(2,1)S(1)} %get-tuple-element.44.refs_4_), channel_id=1, source_target_pairs={{6,0},{0,2},{2,4},{4,6},{7,1},{1,3},{3,5},{5,7},{14,8},{8,10},{10,... | collective-permute-start | bytes 786440 | tf_op jit(solution)/shard_map/ppermute | solution.py:37
  78.6 15.5 %collective-permute-start.12 = (bf16[192,512]{1,0:T(8,128)(2,1)S(1)}, bf16[192,512]{1,0:T(8,128)(2,1)S(1)}, u32[]{:S(2)}, u32[]{:S(2)}) collective-permute-start(bf16[192,512]{1,0:T(8,128)(2,1)S(1)} %get-tuple-element.22), channel_id=1, source_target_pairs={{96,0},{25,1},{104,8},{1,9},{112,16},{9,17},{120,24},{17,25},{0,32... | collective-permute-start | bytes 589832 | tf_op jit(solution)/shard_map/ppermute | solution.py:33
  87.9 23.7 %collective-permute-start.32 = (bf16[192,1536]{1,0:T(8,128)(2,1)S(1)}, bf16[192,1536]{1,0:T(8,128)(2,1)S(1)}, u32[]{:S(2)}, u32[]{:S(2)}) collective-permute-start(bf16[192,1536]{1,0:T(8,128)(2,1)S(1)} %multiply_convert_fusion.refs_0_), channel_id=1, source_target_pairs={{96,0},{25,1},{104,8},{1,9},{112,16},{9,17},{120,24},{17,25},{0,32... | collective-permute-start | bytes 1769480 | tf_op jit(solution)/shard_map/ppermute | solution.py:33
  87.9 25.4 %collective-permute-start.31 = (bf16[192,1536]{1,0:T(8,128)(2,1)S(1)}, bf16[192,1536]{1,0:T(8,128)(2,1)S(1)}, u32[]{:S(2)}, u32[]{:S(2)}) collective-permute-start(bf16[192,1536]{1,0:T(8,128)(2,1)S(1)} %multiply_convert_fusion.refs_0_), channel_id=1, source_target_pairs={{64,0},{17,1},{72,8},{25,9},{80,16},{1,17},{88,24},{9,25},{96,32},... | collective-permute-start | bytes 1769480 | tf_op jit(solution)/shard_map/ppermute | solution.py:33
  90.9 25.2 %collective-permute-start.30 = (bf16[192,1536]{1,0:T(8,128)(2,1)S(1)}, bf16[192,1536]{1,0:T(8,128)(2,1)S(1)}, u32[]{:S(2)}, u32[]{:S(2)}) collective-permute-start(bf16[192,1536]{1,0:T(8,128)(2,1)S(1)} %multiply_convert_fusion.refs_0_), channel_id=1, source_target_pairs={{32,0},{9,1},{40,8},{17,9},{48,16},{25,17},{56,24},{1,25},{64,32},... | collective-permute-start | bytes 1769480 | tf_op jit(solution)/shard_map/ppermute | solution.py:33
  92.1 14.8 %collective-permute-start.13 = (bf16[192,512]{1,0:T(8,128)(2,1)S(1)}, bf16[192,512]{1,0:T(8,128)(2,1)S(1)}, u32[]{:S(2)}, u32[]{:S(2)}) collective-permute-start(bf16[192,512]{1,0:T(8,128)(2,1)S(1)} %get-tuple-element.23), channel_id=1, source_target_pairs={{64,0},{17,1},{72,8},{25,9},{80,16},{1,17},{88,24},{9,25},{96,32},... | collective-permute-start | bytes 589832 | tf_op jit(solution)/shard_map/ppermute | solution.py:33
  94.1 16.4 %collective-permute-start.14 = (bf16[192,512]{1,0:T(8,128)(2,1)S(1)}, bf16[192,512]{1,0:T(8,128)(2,1)S(1)}, u32[]{:S(2)}, u32[]{:S(2)}) collective-permute-start(bf16[192,512]{1,0:T(8,128)(2,1)S(1)} %get-tuple-element.24), channel_id=1, source_target_pairs={{32,0},{9,1},{40,8},{17,9},{48,16},{25,17},{56,24},{1,25},{64,32},... | collective-permute-start | bytes 589832 | tf_op jit(solution)/shard_map/ppermute | solution.py:33
  106.8 14.6 %collective-permute-start.25 = (bf16[512,512]{1,0:T(8,128)(2,1)S(1)}, bf16[512,512]{1,0:T(8,128)(2,1)S(1)}, u32[]{:S(2)}, u32[]{:S(2)}) collective-permute-start(bf16[512,512]{1,0:T(8,128)(2,1)S(1)} %slice.39), channel_id=1, source_target_pairs={{6,0},{0,2},{2,4},{4,6},{7,1},{1,3},{3,5},{5,7},{14,8},{8,10},{10,... | collective-permute-start | bytes 1572872 | tf_op jit(solution)/shard_map/ppermute | solution.py:37
  124.6 12.3 %collective-permute-start.34 = (bf16[768,256]{1,0:T(8,128)(2,1)S(1)}, bf16[768,256]{1,0:T(8,128)(2,1)S(1)}, u32[]{:S(2)}, u32[]{:S(2)}) collective-permute-start(bf16[768,256]{1,0:T(8,128)(2,1)S(1)} %get-tuple-element.34), channel_id=1, source_target_pairs={{24,0},{97,1},{0,8},{105,9},{8,16},{113,17},{16,24},{121,25},{56,3... | collective-permute-start | bytes 1179656 | tf_op jit(solution)/shard_map/ppermute | solution.py:29
  (25 other events, 277.1 us)
where the time goes:
time: 170 us
  waiting for transfers between devices  78.1 us (46%)
  starting transfers between devices  71.4 us (42%)
  Pallas kernels  7.19 us (4%)
  local copies, waits for them, and re-layouts  6.52 us (4%)
  other arithmetic  5.79 us (3%)
    ppermute x12, waiting for transfers between devices, from_sum_ring(): return lax.ppermute(array, ('ra', 'dp'), ring_pairs(False, distance % 4))  22.9 us
    ppermute x15, waiting for transfers between devices, from_plane(): lax.ppermute(array, 'cb', [((y + distance) % 4, y) for y in range(4)])  22.9 us
    ppermute x12, waiting for transfers between devices, from_gather_ring(): return lax.ppermute(array, ('ra', 'dp'), ring_pairs(True, distance % 4))  21.4 us
    ppermute x12, starting transfers between devices, from_gather_ring(): return lax.ppermute(array, ('ra', 'dp'), ring_pairs(True, distance % 4))  21 us
    ppermute x12, starting transfers between devices, from_sum_ring(): return lax.ppermute(array, ('ra', 'dp'), ring_pairs(False, distance % 4))  20.5 us
    ppermute x15, starting transfers between devices, from_plane(): lax.ppermute(array, 'cb', [((y + distance) % 4, y) for y in range(4)])  17.8 us
    all_to_all x2, starting transfers between devices, group_sums(): sums = lax.all_to_all(sent, 'ra', 0, 0, tiled=True)  11.9 us
    all_to_all x2, waiting for transfers between devices, group_sums(): sums = lax.all_to_all(sent, 'ra', 0, 0, tiled=True)  9.13 us
  transfers between devices with their start and end apart: 43, of which 24 were waited for; matrix products, arithmetic and copies ran while one was open for 5% of the time, Pallas kernels for 4%

commit v1 on v0

v1 whole, which is shorter than its diff:
```python
import jax
import jax.numpy as jnp
from jax import lax
from jax.experimental import pallas as pl
from jax.experimental.pallas import tpu as pltpu
from jax.sharding import PartitionSpec as P


residual_scale = 2.0**0.25
norm_eps = 1e-05
others = (1, 3, 2)
f32, bf16 = jnp.float32, jnp.bfloat16


def ring_pairs(gathers, distance):
    pairs = []
    for z in range(4):
        for x in range(4):
            for c in range(2):
                if (c == 0) == gathers:
                    source = (z * 4 + (x + distance) % 4) * 2 + c
                else:
                    source = (((z + distance) % 4) * 4 + x) * 2 + c
                pairs.append((source, (z * 4 + x) * 2 + c))
    return pairs


def from_gather_ring(array, distance):
    return lax.ppermute(array, ("ra", "dp"), ring_pairs(True, distance))


def to_gather_ring(array, distance):
    return lax.ppermute(array, ("ra", "dp"), ring_pairs(True, -distance))


def from_sum_ring(array, distance):
    return lax.ppermute(array, ("ra", "dp"), ring_pairs(False, distance))


def to_sum_ring(array, distance):
    return lax.ppermute(array, ("ra", "dp"), ring_pairs(False, -distance))


def from_plane(array, distance):
    return lax.ppermute(array, "cb", [((y + distance) % 4, y) for y in range(4)])


def from_other_core(array):
    return lax.ppermute(array, "dp", [(0, 1), (1, 0)])


def dot(a, b):
    return lax.dot_general(a, b, (((1,), (0,)), ((), ())), preferred_element_type=f32)


def call(body, out_shape, flops, turn, *operands):
    size = sum(o.size * o.dtype.itemsize for o in operands)
    specs = [pl.BlockSpec(memory_space=pltpu.SMEM)] if turn is not None else []
    whole = pl.BlockSpec(memory_space=pltpu.VMEM)
    return pl.pallas_call(
        body,
        out_shape=out_shape,
        in_specs=specs + [whole] * len(operands),
        out_specs=[whole] * len(out_shape),
        compiler_params=pltpu.CompilerParams(vmem_limit_bytes=24 * 2**20),
        cost_estimate=pl.CostEstimate(flops=flops, bytes_accessed=size, transcendentals=0),
    )(*([turn] if turn is not None else []), *operands)


def stacked(*blocks):
    def stack(*refs):
        at = 0
        for ref in refs[:-1]:
            refs[-1][at : at + ref.shape[0], :] = ref[...]
            at += ref.shape[0]

    rows = sum(block.shape[0] for block in blocks)
    shape = jax.ShapeDtypeStruct((rows, blocks[0].shape[1]), blocks[0].dtype)
    return call(stack, [shape], 10**8, None, *blocks)[0]


def up_products(turn, features, weights):
    rows = features[0].shape[0] // 4
    flat = [w for ws in weights for w in ws]
    wide = flat[0].shape[1]

    def up(turn_ref, *refs):
        pieces, refs = refs[: len(features)], refs[len(features) :]
        w_refs, outs = refs[: len(flat)], refs[len(flat) :]
        for i, out in enumerate(outs):
            start = pl.multiple_of((turn_ref[0] + i) % 4 * rows, rows)
            blocks = [piece[pl.ds(start, rows), :] for piece in pieces]
            at = 0
            for n, ws in enumerate(weights):
                total, left = None, list(blocks)
                for w_ref in w_refs[at : at + len(ws)]:
                    done = 0
                    while done < w_ref.shape[0]:
                        block = left.pop(0)
                        term = dot(block, w_ref[done : done + block.shape[1], :])
                        total = term if total is None else total + term
                        done += block.shape[1]
                at += len(ws)
                out[:, n * wide : (n + 1) * wide] = total.astype(out.dtype)

    full = wide * len(weights)
    shapes = [jax.ShapeDtypeStruct((rows, full), bf16 if i else f32) for i in range(4)]
    flops = 2 * 4 * rows * full * sum(p.shape[1] for p in features)
    return call(up, shapes, flops, turn, *features, *flat)


def down_products(turn, hidden, weights, begun, last):
    rows = hidden[0][0].shape[0]
    chunks = [h for hs in hidden for h in hs]
    flat = [w for ws in weights for w in ws]
    wide = sum(w.shape[0] for w in weights[0]) // 4
    each = flat[0].shape[1]

    def down(turn_ref, *refs):
        h_refs, refs = refs[: len(chunks)], refs[len(chunks) :]
        w_refs, refs = refs[: len(flat)], refs[len(flat) :]
        s_refs, outs = refs[: len(begun)], refs[len(begun) :]
        for i in range(4):
            start = pl.multiple_of((turn_ref[0] + i) % 4 * rows, rows)
            for j, out in enumerate(outs):
                total = s_refs[j][pl.ds(start, rows), :] if begun else None
                at = which = 0
                for n in range(len(hidden)):
                    h_ref = h_refs[4 * n + i]
                    for k in range(h_ref.shape[1] // wide):
                        depth = 0
                        for w_ref in w_refs[at : at + len(weights[which])]:
                            if depth <= j * wide < depth + w_ref.shape[0]:
                                first = j * wide - depth
                                term = dot(
                                    h_ref[:, k * wide : (k + 1) * wide],
                                    w_ref[first : first + wide, :],
                                )
                                total = term if total is None else total + term
                            depth += w_ref.shape[0]
                        at += len(weights[which])
                        which += 1
                out[pl.ds(start, rows), :] = total.astype(out.dtype)

    shapes = [
        jax.ShapeDtypeStruct((4 * rows, each), bf16 if last and j else f32) for j in range(4)
    ]
    flops = 2 * 4 * rows * wide * len(weights) * 4 * each
    return call(down, shapes, flops, turn, *chunks, *flat, *begun)


def group_sums(mixed, width):
    sums = jnp.stack([jnp.sum(mixed, axis=1), jnp.sum(mixed * mixed, axis=1)])
    members = lax.axis_size("ra")
    sent = jnp.broadcast_to(sums.reshape(1, -1, 128), (members, sums.size // 128, 128))
    sums = lax.all_to_all(sent, "ra", 0, 0, tiled=True)
    sums = sums.sum(axis=0).reshape(2, -1)
    mean = sums[0] / width
    return mean, lax.rsqrt(sums[1] / width - mean * mean + norm_eps)


def layer(carried, branch_in, gain_in, bias_in, up_weight, down_weight, gain_out, bias_out):
    width = carried.shape[1] * lax.axis_size("ra")
    r, y, c = lax.axis_index("ra"), lax.axis_index("cb"), lax.axis_index("dp")
    z, x = r // 4, r % 4
    a, b = jnp.where(c == 0, x, z), jnp.where(c == 0, z, x)
    turn = ((b - 2 * c) % 4).reshape(1).astype(jnp.int32)
    held = carried.shape[1]
    few = carried.shape[0] // 4
    wide = up_weight.shape[1] // 8

    def columns_for(distance):
        return (c * 4 + (a + distance) % 4) * wide

    def up_for(distance):
        return lax.dynamic_slice(up_weight, (0, columns_for(distance)), (held, wide))

    def down_for(distance):
        return lax.dynamic_slice(down_weight, (columns_for(distance), 0), (wide, held))

    def gathered(own, block_for):
        own = stacked(own, *[from_gather_ring(block_for(-j), j) for j in others])
        near = {d: from_plane(own, d) for d in (1, 3)}
        cut = own.shape[0] // 2
        far = (from_plane(near[1][:cut], 1), from_plane(near[3][cut:], 3))
        return own, near, far

    up_own, up_near, up_far = gathered(up_for(0), up_for)
    down_own, down_near, down_far = gathered(down_for(0), down_for)

    def quarter(array):
        return lax.dynamic_slice(array, (y * few, 0), (few, held)).astype(f32)

    mixed_in = residual_scale * quarter(carried) + quarter(branch_in)
    theirs = from_other_core(mixed_in)
    scales = jnp.concatenate([gain_in[None], bias_in[None], jnp.zeros((6, held), f32)], axis=0)
    sent = stacked(mixed_in, theirs, scales)
    arrived = [sent] + [from_gather_ring(sent, j) for j in others]
    mean, inverse = group_sums(mixed_in, width)
    own_half = jnp.stack([mean, inverse]).reshape(-1, 128)
    other_half = from_other_core(own_half)
    mean, inverse = (
        jnp.concatenate([mine.reshape(2, -1)[k] for mine in (own_half, other_half)])[:, None]
        for k in range(2)
    )

    def normed_of(piece):
        tokens, gain, bias = piece[: 2 * few], piece[2 * few], piece[2 * few + 1]
        return ((tokens - mean) * inverse * gain + bias).astype(bf16)

    features = [normed_of(piece) for piece in arrived]

    def activated(weights):
        parts = up_products(turn, features, weights)
        total = parts[0]
        for j in (1, 2, 3):
            total = total + to_sum_ring(parts[j], j).astype(f32)
        own = jnp.square(jnp.maximum(total, 0.0)).astype(bf16)
        return [own] + [from_sum_ring(own, j) for j in (1, 2, 3)]

    hidden_own = activated([(up_own,)])
    hidden_near = activated([(up_near[1],), (up_near[3],)])
    hidden_far = activated([up_far])
    begun = down_products(
        turn,
        [hidden_own, hidden_near],
        [(down_own,), (down_near[1],), (down_near[3],)],
        [],
        False,
    )
    parts = down_products(turn, [hidden_far], [down_far], begun, True)
    total = parts[0]
    for j, part in zip(others, parts[1:]):
        total = total + to_gather_ring(part, j).astype(f32)
    mine, theirs = total[:few], from_other_core(total[few:])
    mixed_out = residual_scale * features[0][:few].astype(f32) + (mine + theirs)
    mean, inverse = group_sums(mixed_out, width)
    out = (mixed_out - mean[:, None]) * inverse[:, None] * gain_out + bias_out
    out = out.astype(bf16)
    result = jnp.zeros(carried.shape, bf16)
    for d in range(4):
        block = from_plane(out, d) if d else out
        result = lax.dynamic_update_slice(result, block, ((y + d) % 4 * few, 0))
    return result


def solution(mesh):
    in_specs = (
        P("dp", "ra"),
        P("dp", "ra"),
        P("ra"),
        P("ra"),
        P("ra", "cb"),
        P("cb", "ra"),
        P("ra"),
        P("ra"),
    )
    return jax.shard_map(
        layer, mesh=mesh, in_specs=in_specs, out_specs=P("dp", "ra"), check_vma=False
    )
```

time: 170 us -> 192 us (1.13)
  waiting for transfers between devices: 78.1 us -> 96.5 us
  starting transfers between devices: 71.4 us -> 76.3 us
    ppermute x15 -> x11, waiting for transfers between devices: 22.9 us -> 36.1 us  [from_plane(): lax.ppermute(array, 'cb', [((y + distance) % 4, y) for y in range(4)])]
    ppermute x24 -> x30, waiting for transfers between devices: 44.4 us -> 49.9 us  [the longest x9 19.9 us: from_gather_ring(): return lax.ppermute(array, ('ra', 'dp'), ring_pairs(True, distance))]
    ppermute x24 -> x30, starting transfers between devices: 41.6 us -> 46.1 us  [the longest x9 17.5 us: to_sum_ring(): return lax.ppermute(array, ('ra', 'dp'), ring_pairs(False, -distance))]
    concatenate x5 -> x2, other arithmetic: 2.23 us -> 0.08 us  [the longest x1 0.07 us: layer(): jnp.concatenate([gain_in[None], bias_in[None], jnp.zeros((6, held), f32)]...]
    unnamed x16 -> x12, local copies, waits for them, and re-layouts: 2 us -> 0.04 us
    ppermute x15 -> x11, starting transfers between devices: 17.8 us -> 17.1 us  [from_plane(): lax.ppermute(array, 'cb', [((y + distance) % 4, y) for y in range(4)])]
    pallas_call x4 -> x8, Pallas kernels: 7.19 us -> 7.54 us  [call(): pl.pallas_call(body, out_shape=out_shape, in_specs=specs + [whole] * len(...]
  transfers between devices with their start and end apart: 43 -> 46, of which waited for: 24 -> 24; matrix products, arithmetic and copies ran while one was open for 5% -> 4% of each run, Pallas kernels for 4% -> 3%
where the time goes in v1:
time: 192 us; the launch traced here: 191 us
  waiting for transfers between devices  96.5 us (50%)
  starting transfers between devices  76.3 us (40%)
  Pallas kernels  7.54 us (4%)
  local copies, waits for them, and re-layouts  6.28 us (3%)
  other arithmetic  4.13 us (2%)
    ppermute x11, waiting for transfers between devices, from_plane(): lax.ppermute(array, 'cb', [((y + distance) % 4, y) for y in range(4)])  36.1 us
    ppermute x9, waiting for transfers between devices, from_gather_ring(): return lax.ppermute(array, ('ra', 'dp'), ring_pairs(True, distance))  19.9 us
    ppermute x9, waiting for transfers between devices, from_sum_ring(): return lax.ppermute(array, ('ra', 'dp'), ring_pairs(False, distance))  19.5 us
    ppermute x9, starting transfers between devices, to_sum_ring(): return lax.ppermute(array, ('ra', 'dp'), ring_pairs(False, -distance))  17.5 us
    ppermute x11, starting transfers between devices, from_plane(): lax.ppermute(array, 'cb', [((y + distance) % 4, y) for y in range(4)])  17.1 us
    all_to_all x2, starting transfers between devices, group_sums(): sums = lax.all_to_all(sent, 'ra', 0, 0, tiled=True)  13 us
    ppermute x9, starting transfers between devices, from_gather_ring(): return lax.ppermute(array, ('ra', 'dp'), ring_pairs(True, distance))  11.4 us
    ppermute x9, starting transfers between devices, from_sum_ring(): return lax.ppermute(array, ('ra', 'dp'), ring_pairs(False, distance))  10.6 us
  transfers between devices with their start and end apart: 46, of which 24 were waited for; matrix products, arithmetic and copies ran while one was open for 4% of the time, Pallas kernels for 3%

profile of v1, /device:TPU:0, one launch (start us, length us, event | category | flops | bytes accessed | tf_op | source)
XLA Modules:
  0.0 191.3 jit_solution(8014784933110845724)
XLA Ops:
  2.0 8.0 %all-to-all-start = ((f32[16,6,128]{2,1,0:T(8,128)}), f32[16,6,128]{2,1,0:T(8,128)S(1)}, u32[]{:S(2)}, u32[]{:S(2)}) async-start(f32[16,6,128]{2,1,0:T(8,128)} %broadcast_in_dim.37), calls=%async_computation | async-start | bytes 131072 | tf_op jit(solution)/shard_map/all_to_all | solution.py:156
  12.4 3.0 %collective-permute-start.5 = (bf16[256,512]{1,0:T(8,128)(2,1)}, bf16[256,512]{1,0:T(8,128)(2,1)S(1)}, u32[]{:S(2)}, u32[]{:S(2)}) collective-permute-start(bf16[256,512]{1,0:T(8,128)(2,1)} %get-tuple-element.60), channel_id=1, source_target_pairs={{8,0},{33,1},{16,8},{41,9},{24,16},{49,17},{0,24},{57,25},{40,32},... | collective-permute-start | bytes 786440 | tf_op jit(solution)/shard_map/ppermute | solution.py:29
  20.0 2.8 %collective-permute-start.4 = (f32[776,256]{1,0:T(8,128)S(1)}, f32[776,256]{1,0:T(8,128)}, u32[]{:S(2)}, u32[]{:S(2)}) collective-permute-start(f32[776,256]{1,0:T(8,128)S(1)} %shard_map.82), channel_id=1, source_target_pairs={{16,0},{65,1},{24,8},{73,9},{0,16},{81,17},{8,24},{89,25},{48,32},... | collective-permute-start | bytes 2383880 | tf_op jit(solution)/shard_map/ppermute | solution.py:29
  22.9 11.6 %collective-permute-done.6.refs_2_ = bf16[256,512]{1,0:T(8,128)(2,1)S(1)} collective-permute-done((bf16[256,512]{1,0:T(8,128)(2,1)}, bf16[256,512]{1,0:T(8,128)(2,1)S(1)}, u32[]{:S(2)}, u32[]{:S(2)}) %collective-permute-start.6) | collective-permute-done | bytes 262176 | tf_op jit(solution)/shard_map/ppermute | solution.py:29
  35.7 3.0 %collective-permute-start.8 = (bf16[1024,512]{1,0:T(8,128)(2,1)S(1)}, bf16[1024,512]{1,0:T(8,128)(2,1)S(1)}, u32[]{:S(2)}, u32[]{:S(2)}) collective-permute-start(bf16[1024,512]{1,0:T(8,128)(2,1)S(1)} %shard_map.83.refs_4_), channel_id=1, source_target_pairs={{2,0},{4,2},{6,4},{0,6},{3,1},{5,3},{7,5},{1,7},{10,8},{12,10},{14... | collective-permute-start | bytes 3145736 | tf_op jit(solution)/shard_map/ppermute | solution.py:45
  46.6 4.2 %collective-permute-done.2 = f32[776,256]{1,0:T(8,128)S(1)} collective-permute-done((f32[776,256]{1,0:T(8,128)S(1)}, f32[776,256]{1,0:T(8,128)S(1)}, u32[]{:S(2)}, u32[]{:S(2)}) %collective-permute-start.2) | collective-permute-done | bytes 794656 | tf_op jit(solution)/shard_map/ppermute | solution.py:29
  53.2 9.0 %collective-permute-done.8.refs_4_ = bf16[1024,512]{1,0:T(8,128)(2,1)S(1)} collective-permute-done((bf16[1024,512]{1,0:T(8,128)(2,1)S(1)}, bf16[1024,512]{1,0:T(8,128)(2,1)S(1)}, u32[]{:S(2)}, u32[]{:S(2)}) %collective-permute-start.8) | collective-permute-done | bytes 1048608 | tf_op jit(solution)/shard_map/ppermute | solution.py:45
  62.3 3.8 %collective-permute-start.9 = (bf16[512,512]{1,0:T(8,128)(2,1)S(1)}, bf16[512,512]{1,0:T(8,128)(2,1)S(1)}, u32[]{:S(2)}, u32[]{:S(2)}) collective-permute-start(bf16[512,512]{1,0:T(8,128)(2,1)S(1)} %slice.119), channel_id=1, source_target_pairs={{2,0},{4,2},{6,4},{0,6},{3,1},{5,3},{7,5},{1,7},{10,8},{12,10},{14... | collective-permute-start | bytes 1572872 | tf_op jit(solution)/shard_map/ppermute | solution.py:45
  68.8 2.7 %collective-permute-start.27 = (bf16[192,512]{1,0:T(8,128)(2,1)S(1)}, bf16[192,512]{1,0:T(8,128)(2,1)S(1)}, u32[]{:S(2)}, u32[]{:S(2)}) collective-permute-start(bf16[192,512]{1,0:T(8,128)(2,1)S(1)} %get-tuple-element.32), channel_id=1, source_target_pairs={{32,0},{9,1},{40,8},{17,9},{48,16},{25,17},{56,24},{1,25},{64,32},... | collective-permute-start | bytes 589832 | tf_op jit(solution)/shard_map/ppermute | solution.py:41
  71.6 13.1 %collective-permute-done.21.refs_9_ = bf16[2048,256]{1,0:T(8,128)(2,1)S(1)} collective-permute-done((bf16[2048,256]{1,0:T(8,128)(2,1)S(1)}, bf16[2048,256]{1,0:T(8,128)(2,1)S(1)}, u32[]{:S(2)}, u32[]{:S(2)}) %collective-permute-start.21) | collective-permute-done | bytes 1048608 | tf_op jit(solution)/shard_map/ppermute | solution.py:45
  84.7 3.0 %collective-permute-start.26 = (bf16[192,512]{1,0:T(8,128)(2,1)S(1)}, bf16[192,512]{1,0:T(8,128)(2,1)S(1)}, u32[]{:S(2)}, u32[]{:S(2)}) collective-permute-start(bf16[192,512]{1,0:T(8,128)(2,1)S(1)} %get-tuple-element.31), channel_id=1, source_target_pairs={{64,0},{17,1},{72,8},{25,9},{80,16},{1,17},{88,24},{9,25},{96,32},... | collective-permute-start | bytes 589832 | tf_op jit(solution)/shard_map/ppermute | solution.py:41
  96.7 4.3 %collective-permute-done.11.refs_5_ = bf16[512,512]{1,0:T(8,128)(2,1)S(1)} collective-permute-done((bf16[512,512]{1,0:T(8,128)(2,1)S(1)}, bf16[512,512]{1,0:T(8,128)(2,1)S(1)}, u32[]{:S(2)}, u32[]{:S(2)}) %collective-permute-start.11) | collective-permute-done | bytes 524320 | tf_op jit(solution)/shard_map/ppermute | solution.py:45
  101.1 2.9 %collective-permute-start.28 = (bf16[192,512]{1,0:T(8,128)(2,1)S(1)}, bf16[192,512]{1,0:T(8,128)(2,1)S(1)}, u32[]{:S(2)}, u32[]{:S(2)}) collective-permute-start(bf16[192,512]{1,0:T(8,128)(2,1)S(1)} %multiply_convert_fusion.1.refs_0_), channel_id=1, source_target_pairs={{32,0},{9,1},{40,8},{17,9},{48,16},{25,17},{56,24},{1,25},{64,32},... | collective-permute-start | bytes 589832 | tf_op jit(solution)/shard_map/ppermute | solution.py:37
  105.1 4.2 %collective-permute-done.28.refs_1_ = bf16[192,512]{1,0:T(8,128)(2,1)S(1)} collective-permute-done((bf16[192,512]{1,0:T(8,128)(2,1)S(1)}, bf16[192,512]{1,0:T(8,128)(2,1)S(1)}, u32[]{:S(2)}, u32[]{:S(2)}) %collective-permute-start.28) | collective-permute-done | bytes 196640 | tf_op jit(solution)/shard_map/ppermute | solution.py:37
  109.4 3.7 %collective-permute-start.14 = (bf16[192,512]{1,0:T(8,128)(2,1)S(1)}, bf16[192,512]{1,0:T(8,128)(2,1)S(1)}, u32[]{:S(2)}, u32[]{:S(2)}) collective-permute-start(bf16[192,512]{1,0:T(8,128)(2,1)S(1)} %get-tuple-element.28), channel_id=1, source_target_pairs={{32,0},{9,1},{40,8},{17,9},{48,16},{25,17},{56,24},{1,25},{64,32},... | collective-permute-start | bytes 589832 | tf_op jit(solution)/shard_map/ppermute | solution.py:41
  123.1 4.5 %collective-permute-done.34.refs_5_ = bf16[192,1024]{1,0:T(8,128)(2,1)S(1)} collective-permute-done((bf16[192,1024]{1,0:T(8,128)(2,1)S(1)}, bf16[192,1024]{1,0:T(8,128)(2,1)S(1)}, u32[]{:S(2)}, u32[]{:S(2)}) %collective-permute-start.34) | collective-permute-done | bytes 393248 | tf_op jit(solution)/shard_map/ppermute | solution.py:37
  127.7 3.7 %collective-permute-start.15 = (bf16[192,512]{1,0:T(8,128)(2,1)S(1)}, bf16[192,512]{1,0:T(8,128)(2,1)S(1)}, u32[]{:S(2)}, u32[]{:S(2)}) collective-permute-start(bf16[192,512]{1,0:T(8,128)(2,1)S(1)} %multiply_convert_fusion.2.refs_0_), channel_id=1, source_target_pairs={{32,0},{9,1},{40,8},{17,9},{48,16},{25,17},{56,24},{1,25},{64,32},... | collective-permute-start | bytes 589832 | tf_op jit(solution)/shard_map/ppermute | solution.py:37
  138.6 6.7 %collective-permute-done.17.refs_3_ = bf16[192,512]{1,0:T(8,128)(2,1)S(1)} collective-permute-done((bf16[192,512]{1,0:T(8,128)(2,1)S(1)}, bf16[192,512]{1,0:T(8,128)(2,1)S(1)}, u32[]{:S(2)}, u32[]{:S(2)}) %collective-permute-start.17) | collective-permute-done | bytes 196640 | tf_op jit(solution)/shard_map/ppermute | solution.py:37
  146.3 4.5 %collective-permute-start.39 = (bf16[768,256]{1,0:T(8,128)(2,1)S(1)}, bf16[768,256]{1,0:T(8,128)(2,1)S(1)}, u32[]{:S(2)}, u32[]{:S(2)}) collective-permute-start(bf16[768,256]{1,0:T(8,128)(2,1)S(1)} %get-tuple-element.44), channel_id=1, source_target_pairs={{16,0},{65,1},{24,8},{73,9},{0,16},{81,17},{8,24},{89,25},{48,32},... | collective-permute-start | bytes 1179656 | tf_op jit(solution)/shard_map/ppermute | solution.py:33
  152.8 3.8 %collective-permute-done.39 = bf16[768,256]{1,0:T(8,128)(2,1)S(1)} collective-permute-done((bf16[768,256]{1,0:T(8,128)(2,1)S(1)}, bf16[768,256]{1,0:T(8,128)(2,1)S(1)}, u32[]{:S(2)}, u32[]{:S(2)}) %collective-permute-start.39) | collective-permute-done | bytes 393248 | tf_op jit(solution)/shard_map/ppermute | solution.py:33
  163.7 5.0 %all-to-all-start.1 = ((f32[16,6,128]{2,1,0:T(8,128)}), f32[16,6,128]{2,1,0:T(8,128)S(1)}, u32[]{:S(2)}, u32[]{:S(2)}) async-start(f32[16,6,128]{2,1,0:T(8,128)} %broadcast_in_dim.39), calls=%async_computation.1 | async-start | bytes 131072 | tf_op jit(solution)/shard_map/all_to_all | solution.py:156
  168.7 7.7 %all-to-all-done.1 = f32[16,6,128]{2,1,0:T(8,128)S(1)} async-done(((f32[16,6,128]{2,1,0:T(8,128)}), f32[16,6,128]{2,1,0:T(8,128)S(1)}, u32[]{:S(2)}, u32[]{:S(2)}) %all-to-all-start.1) | async-done | bytes 49184 | tf_op jit(solution)/shard_map/all_to_all | solution.py:156
  176.7 3.3 %collective-permute-start.41 = (bf16[384,256]{1,0:T(8,128)(2,1)S(1)}, bf16[384,256]{1,0:T(8,128)(2,1)S(1)}, u32[]{:S(2)}, u32[]{:S(2)}) collective-permute-start(bf16[384,256]{1,0:T(8,128)(2,1)S(1)} %get-tuple-element.50), channel_id=1, source_target_pairs={{2,0},{4,2},{6,4},{0,6},{3,1},{5,3},{7,5},{1,7},{10,8},{12,10},{14... | collective-permute-start | bytes 589832 | tf_op jit(solution)/shard_map/ppermute | solution.py:45
  180.9 6.3 %collective-permute-done.41 = bf16[384,256]{1,0:T(8,128)(2,1)S(1)} collective-permute-done((bf16[384,256]{1,0:T(8,128)(2,1)S(1)}, bf16[384,256]{1,0:T(8,128)(2,1)S(1)}, u32[]{:S(2)}, u32[]{:S(2)}) %collective-permute-start.41) | collective-permute-done | bytes 196640 | tf_op jit(solution)/shard_map/ppermute | solution.py:45
  (135 shorter events, 66.0 us)
Async XLA Ops:
  1.2 18.8 %collective-permute-start = (f32[384,256]{1,0:T(8,128)S(1)}, f32[384,256]{1,0:T(8,128)S(1)}, u32[]{:S(2)}, u32[]{:S(2)}) collective-permute-start(f32[384,256]{1,0:T(8,128)S(1)} %get-tuple-element.54.refs_0_), channel_id=1, source_target_pairs={{0,1},{1,0},{2,3},{3,2},{4,5},{5,4},{6,7},{7,6},{8,9},{9,8},{10,11... | collective-permute-start | bytes 1179656 | tf_op jit(solution)/shard_map/ppermute | solution.py:49
  2.0 17.9 %all-to-all-start = ((f32[16,6,128]{2,1,0:T(8,128)}), f32[16,6,128]{2,1,0:T(8,128)S(1)}, u32[]{:S(2)}, u32[]{:S(2)}) async-start(f32[16,6,128]{2,1,0:T(8,128)} %broadcast_in_dim.37), calls=%async_computation | async-start | bytes 131072 | tf_op jit(solution)/shard_map/all_to_all | solution.py:156
  15.4 19.1 %collective-permute-start.6 = (bf16[256,512]{1,0:T(8,128)(2,1)}, bf16[256,512]{1,0:T(8,128)(2,1)S(1)}, u32[]{:S(2)}, u32[]{:S(2)}) collective-permute-start(bf16[256,512]{1,0:T(8,128)(2,1)} %get-tuple-element.62), channel_id=1, source_target_pairs={{24,0},{97,1},{0,8},{105,9},{8,16},{113,17},{16,24},{121,25},{56,3... | collective-permute-start | bytes 786440 | tf_op jit(solution)/shard_map/ppermute | solution.py:29
  15.4 19.1 %collective-permute-start.7 = (bf16[256,512]{1,0:T(8,128)(2,1)}, bf16[256,512]{1,0:T(8,128)(2,1)S(1)}, u32[]{:S(2)}, u32[]{:S(2)}) collective-permute-start(bf16[256,512]{1,0:T(8,128)(2,1)} %get-tuple-element.59), channel_id=1, source_target_pairs={{16,0},{65,1},{24,8},{73,9},{0,16},{81,17},{8,24},{89,25},{48,32},... | collective-permute-start | bytes 786440 | tf_op jit(solution)/shard_map/ppermute | solution.py:29
  18.6 20.1 %collective-permute-start.18 = (bf16[512,256]{1,0:T(8,128)(2,1)}, bf16[512,256]{1,0:T(8,128)(2,1)S(1)}, u32[]{:S(2)}, u32[]{:S(2)}) collective-permute-start(bf16[512,256]{1,0:T(8,128)(2,1)} %get-tuple-element.56), channel_id=1, source_target_pairs={{8,0},{33,1},{16,8},{41,9},{24,16},{49,17},{0,24},{57,25},{40,32},... | collective-permute-start | bytes 786440 | tf_op jit(solution)/shard_map/ppermute | solution.py:29
  20.0 24.0 %collective-permute-start.4 = (f32[776,256]{1,0:T(8,128)S(1)}, f32[776,256]{1,0:T(8,128)}, u32[]{:S(2)}, u32[]{:S(2)}) collective-permute-start(f32[776,256]{1,0:T(8,128)S(1)} %shard_map.82), channel_id=1, source_target_pairs={{16,0},{65,1},{24,8},{73,9},{0,16},{81,17},{8,24},{89,25},{48,32},... | collective-permute-start | bytes 2383880 | tf_op jit(solution)/shard_map/ppermute | solution.py:29
  22.8 17.1 %collective-permute-start.19 = (bf16[512,256]{1,0:T(8,128)(2,1)}, bf16[512,256]{1,0:T(8,128)(2,1)S(1)}, u32[]{:S(2)}, u32[]{:S(2)}) collective-permute-start(bf16[512,256]{1,0:T(8,128)(2,1)} %get-tuple-element.58), channel_id=1, source_target_pairs={{24,0},{97,1},{0,8},{105,9},{8,16},{113,17},{16,24},{121,25},{56,3... | collective-permute-start | bytes 786440 | tf_op jit(solution)/shard_map/ppermute | solution.py:29
  35.7 26.6 %collective-permute-start.8 = (bf16[1024,512]{1,0:T(8,128)(2,1)S(1)}, bf16[1024,512]{1,0:T(8,128)(2,1)S(1)}, u32[]{:S(2)}, u32[]{:S(2)}) collective-permute-start(bf16[1024,512]{1,0:T(8,128)(2,1)S(1)} %shard_map.83.refs_4_), channel_id=1, source_target_pairs={{2,0},{4,2},{6,4},{0,6},{3,1},{5,3},{7,5},{1,7},{10,8},{12,10},{14... | collective-permute-start | bytes 3145736 | tf_op jit(solution)/shard_map/ppermute | solution.py:45
  38.7 12.1 %collective-permute-start.2 = (f32[776,256]{1,0:T(8,128)S(1)}, f32[776,256]{1,0:T(8,128)S(1)}, u32[]{:S(2)}, u32[]{:S(2)}) collective-permute-start(f32[776,256]{1,0:T(8,128)S(1)} %shard_map.82), channel_id=1, source_target_pairs={{8,0},{33,1},{16,8},{41,9},{24,16},{49,17},{0,24},{57,25},{40,32},... | collective-permute-start | bytes 2383880 | tf_op jit(solution)/shard_map/ppermute | solution.py:29
  39.9 13.3 %collective-permute-start.3 = (f32[776,256]{1,0:T(8,128)S(1)}, f32[776,256]{1,0:T(8,128)S(1)}, u32[]{:S(2)}, u32[]{:S(2)}) collective-permute-start(f32[776,256]{1,0:T(8,128)S(1)} %shard_map.82), channel_id=1, source_target_pairs={{24,0},{97,1},{0,8},{105,9},{8,16},{113,17},{16,24},{121,25},{56,3... | collective-permute-start | bytes 2383880 | tf_op jit(solution)/shard_map/ppermute | solution.py:29
  42.4 29.1 %collective-permute-start.10 = (bf16[1024,512]{1,0:T(8,128)(2,1)S(1)}, bf16[1024,512]{1,0:T(8,128)(2,1)S(1)}, u32[]{:S(2)}, u32[]{:S(2)}) collective-permute-start(bf16[1024,512]{1,0:T(8,128)(2,1)S(1)} %shard_map.83.refs_4_), channel_id=1, source_target_pairs={{6,0},{0,2},{2,4},{4,6},{7,1},{1,3},{3,5},{5,7},{14,8},{8,10},{10,... | collective-permute-start | bytes 3145736 | tf_op jit(solution)/shard_map/ppermute | solution.py:45
  44.1 40.6 %collective-permute-start.21 = (bf16[2048,256]{1,0:T(8,128)(2,1)S(1)}, bf16[2048,256]{1,0:T(8,128)(2,1)S(1)}, u32[]{:S(2)}, u32[]{:S(2)}) collective-permute-start(bf16[2048,256]{1,0:T(8,128)(2,1)S(1)} %shard_map.85.refs_8_), channel_id=1, source_target_pairs={{2,0},{4,2},{6,4},{0,6},{3,1},{5,3},{7,5},{1,7},{10,8},{12,10},{14... | collective-permute-start | bytes 3145736 | tf_op jit(solution)/shard_map/ppermute | solution.py:45
  50.8 54.2 %collective-permute-start.23 = (bf16[2048,256]{1,0:T(8,128)(2,1)S(1)}, bf16[2048,256]{1,0:T(8,128)(2,1)S(1)}, u32[]{:S(2)}, u32[]{:S(2)}) collective-permute-start(bf16[2048,256]{1,0:T(8,128)(2,1)S(1)} %shard_map.85.refs_8_), channel_id=1, source_target_pairs={{6,0},{0,2},{2,4},{4,6},{7,1},{1,3},{3,5},{5,7},{14,8},{8,10},{10,... | collective-permute-start | bytes 3145736 | tf_op jit(solution)/shard_map/ppermute | solution.py:45
  62.3 33.8 %collective-permute-start.9 = (bf16[512,512]{1,0:T(8,128)(2,1)S(1)}, bf16[512,512]{1,0:T(8,128)(2,1)S(1)}, u32[]{:S(2)}, u32[]{:S(2)}) collective-permute-start(bf16[512,512]{1,0:T(8,128)(2,1)S(1)} %slice.119), channel_id=1, source_target_pairs={{2,0},{4,2},{6,4},{0,6},{3,1},{5,3},{7,5},{1,7},{10,8},{12,10},{14... | collective-permute-start | bytes 1572872 | tf_op jit(solution)/shard_map/ppermute | solution.py:45
  68.8 18.9 %collective-permute-start.27 = (bf16[192,512]{1,0:T(8,128)(2,1)S(1)}, bf16[192,512]{1,0:T(8,128)(2,1)S(1)}, u32[]{:S(2)}, u32[]{:S(2)}) collective-permute-start(bf16[192,512]{1,0:T(8,128)(2,1)S(1)} %get-tuple-element.32), channel_id=1, source_target_pairs={{32,0},{9,1},{40,8},{17,9},{48,16},{25,17},{56,24},{1,25},{64,32},... | collective-permute-start | bytes 589832 | tf_op jit(solution)/shard_map/ppermute | solution.py:41
  71.6 29.5 %collective-permute-start.11 = (bf16[512,512]{1,0:T(8,128)(2,1)S(1)}, bf16[512,512]{1,0:T(8,128)(2,1)S(1)}, u32[]{:S(2)}, u32[]{:S(2)}) collective-permute-start(bf16[512,512]{1,0:T(8,128)(2,1)S(1)} %slice.120), channel_id=1, source_target_pairs={{6,0},{0,2},{2,4},{4,6},{7,1},{1,3},{3,5},{5,7},{14,8},{8,10},{10,... | collective-permute-start | bytes 1572872 | tf_op jit(solution)/shard_map/ppermute | solution.py:45
  91.9 17.5 %collective-permute-start.33 = (bf16[192,1024]{1,0:T(8,128)(2,1)S(1)}, bf16[192,1024]{1,0:T(8,128)(2,1)S(1)}, u32[]{:S(2)}, u32[]{:S(2)}) collective-permute-start(bf16[192,1024]{1,0:T(8,128)(2,1)S(1)} %get-tuple-element.36), channel_id=1, source_target_pairs={{32,0},{9,1},{40,8},{17,9},{48,16},{25,17},{56,24},{1,25},{64,32},... | collective-permute-start | bytes 1179656 | tf_op jit(solution)/shard_map/ppermute | solution.py:41
  94.6 18.4 %collective-permute-start.32 = (bf16[192,1024]{1,0:T(8,128)(2,1)S(1)}, bf16[192,1024]{1,0:T(8,128)(2,1)S(1)}, u32[]{:S(2)}, u32[]{:S(2)}) collective-permute-start(bf16[192,1024]{1,0:T(8,128)(2,1)S(1)} %get-tuple-element.35), channel_id=1, source_target_pairs={{64,0},{17,1},{72,8},{25,9},{80,16},{1,17},{88,24},{9,25},{96,32},... | collective-permute-start | bytes 1179656 | tf_op jit(solution)/shard_map/ppermute | solution.py:41
  96.1 18.5 %collective-permute-start.31 = (bf16[192,1024]{1,0:T(8,128)(2,1)S(1)}, bf16[192,1024]{1,0:T(8,128)(2,1)S(1)}, u32[]{:S(2)}, u32[]{:S(2)}) collective-permute-start(bf16[192,1024]{1,0:T(8,128)(2,1)S(1)} %get-tuple-element.34), channel_id=1, source_target_pairs={{96,0},{25,1},{104,8},{1,9},{112,16},{9,17},{120,24},{17,25},{0,32... | collective-permute-start | bytes 1179656 | tf_op jit(solution)/shard_map/ppermute | solution.py:41
  118.1 13.2 %collective-permute-start.35 = (bf16[192,1024]{1,0:T(8,128)(2,1)S(1)}, bf16[192,1024]{1,0:T(8,128)(2,1)S(1)}, u32[]{:S(2)}, u32[]{:S(2)}) collective-permute-start(bf16[192,1024]{1,0:T(8,128)(2,1)S(1)} %multiply_convert_fusion.refs_4_), channel_id=1, source_target_pairs={{64,0},{17,1},{72,8},{25,9},{80,16},{1,17},{88,24},{9,25},{96,32},... | collective-permute-start | bytes 1179656 | tf_op jit(solution)/shard_map/ppermute | solution.py:37
  118.9 12.7 %collective-permute-start.36 = (bf16[192,1024]{1,0:T(8,128)(2,1)S(1)}, bf16[192,1024]{1,0:T(8,128)(2,1)S(1)}, u32[]{:S(2)}, u32[]{:S(2)}) collective-permute-start(bf16[192,1024]{1,0:T(8,128)(2,1)S(1)} %multiply_convert_fusion.refs_4_), channel_id=1, source_target_pairs={{96,0},{25,1},{104,8},{1,9},{112,16},{9,17},{120,24},{17,25},{0,32... | collective-permute-start | bytes 1179656 | tf_op jit(solution)/shard_map/ppermute | solution.py:37
  120.3 14.5 %collective-permute-start.22 = (bf16[1024,256]{1,0:T(8,128)(2,1)S(1)}, bf16[1024,256]{1,0:T(8,128)(2,1)S(1)}, u32[]{:S(2)}, u32[]{:S(2)}) collective-permute-start(bf16[1024,256]{1,0:T(8,128)(2,1)S(1)} %slice.121), channel_id=1, source_target_pairs={{2,0},{4,2},{6,4},{0,6},{3,1},{5,3},{7,5},{1,7},{10,8},{12,10},{14... | collective-permute-start | bytes 1572872 | tf_op jit(solution)/shard_map/ppermute | solution.py:45
  131.6 13.7 %collective-permute-start.17 = (bf16[192,512]{1,0:T(8,128)(2,1)S(1)}, bf16[192,512]{1,0:T(8,128)(2,1)S(1)}, u32[]{:S(2)}, u32[]{:S(2)}) collective-permute-start(bf16[192,512]{1,0:T(8,128)(2,1)S(1)} %multiply_convert_fusion.2.refs_0_), channel_id=1, source_target_pairs={{96,0},{25,1},{104,8},{1,9},{112,16},{9,17},{120,24},{17,25},{0,32... | collective-permute-start | bytes 589832 | tf_op jit(solution)/shard_map/ppermute | solution.py:37
  163.7 12.7 %all-to-all-start.1 = ((f32[16,6,128]{2,1,0:T(8,128)}), f32[16,6,128]{2,1,0:T(8,128)S(1)}, u32[]{:S(2)}, u32[]{:S(2)}) async-start(f32[16,6,128]{2,1,0:T(8,128)} %broadcast_in_dim.39), calls=%async_computation.1 | async-start | bytes 131072 | tf_op jit(solution)/shard_map/all_to_all | solution.py:156
  (28 other events, 246.2 us)

commit v2 on v1

v2 whole, which is shorter than its diff:
```python
import jax
import jax.numpy as jnp
from jax import lax
from jax.experimental import pallas as pl
from jax.experimental.pallas import tpu as pltpu
from jax.sharding import PartitionSpec as P


residual_scale = 2.0**0.25
norm_eps = 1e-05
others = (1, 3, 2)
f32, bf16 = jnp.float32, jnp.bfloat16


def ring_pairs(gathers, distance):
    pairs = []
    for z in range(4):
        for x in range(4):
            for c in range(2):
                if (c == 0) == gathers:
                    source = (z * 4 + (x + distance) % 4) * 2 + c
                else:
                    source = (((z + distance) % 4) * 4 + x) * 2 + c
                pairs.append((source, (z * 4 + x) * 2 + c))
    return pairs


def from_gather_ring(array, distance):
    return lax.ppermute(array, ("ra", "dp"), ring_pairs(True, distance))


def to_gather_ring(array, distance):
    return lax.ppermute(array, ("ra", "dp"), ring_pairs(True, -distance))


def from_sum_ring(array, distance):
    return lax.ppermute(array, ("ra", "dp"), ring_pairs(False, distance))


def to_sum_ring(array, distance):
    return lax.ppermute(array, ("ra", "dp"), ring_pairs(False, -distance))


def from_plane(array, distance):
    return lax.ppermute(array, "cb", [((y + distance) % 4, y) for y in range(4)])


def from_next_plane(array):
    pairs = []
    for y in range(4):
        for c in range(2):
            pairs.append(((y + 1 - 2 * c) % 4 * 2 + c, y * 2 + c))
    return lax.ppermute(array, ("cb", "dp"), pairs)


def from_other_core(array):
    return lax.ppermute(array, "dp", [(0, 1), (1, 0)])


def dot(a, b):
    return lax.dot_general(a, b, (((1,), (0,)), ((), ())), preferred_element_type=f32)


def call(body, out_shape, flops, place, *operands, mib=16):
    size = sum(o.size * o.dtype.itemsize for o in operands)
    whole = pl.BlockSpec(memory_space=pltpu.VMEM)
    return pl.pallas_call(
        body,
        out_shape=out_shape,
        in_specs=[pl.BlockSpec(memory_space=pltpu.SMEM)] + [whole] * len(operands),
        out_specs=[whole] * len(out_shape),
        compiler_params=pltpu.CompilerParams(vmem_limit_bytes=mib * 2**20),
        cost_estimate=pl.CostEstimate(flops=flops, bytes_accessed=size, transcendentals=0),
    )(place, *operands)


def cut_columns(place, weight, wide):
    held = weight.shape[0]

    def cut(place_ref, w_ref, *outs):
        for j, out in zip((0, *others), outs):
            for h in range(2):
                first = pl.multiple_of((h * 4 + (place_ref[2] - j + 4) % 4) * wide, wide)
                out[h * held : (h + 1) * held, :] = w_ref[:, pl.ds(first, wide)]

    shape = jax.ShapeDtypeStruct((2 * held, wide), weight.dtype)
    return call(cut, [shape] * 4, 10**8, place, weight, mib=9)


def cut_rows(place, weight, wide):
    def cut(place_ref, w_ref, *outs):
        for j, out in zip((0, *others), outs):
            for h in range(2):
                first = pl.multiple_of((h * 4 + (place_ref[2] - j + 4) % 4) * wide, wide)
                out[h * wide : (h + 1) * wide, :] = w_ref[pl.ds(first, wide), :]

    shape = jax.ShapeDtypeStruct((2 * wide, weight.shape[1]), weight.dtype)
    return call(cut, [shape] * 4, 10**8, place, weight, mib=9)


def stacked(place, blocks, parts):
    each = blocks[0].shape[0] // parts

    def stack(place_ref, *refs):
        for p in range(parts):
            for n, ref in enumerate(refs[:-1]):
                at = (p * len(blocks) + n) * each
                refs[-1][at : at + each, :] = ref[p * each : (p + 1) * each, :]

    shape = (len(blocks) * blocks[0].shape[0], blocks[0].shape[1])
    return call(
        stack, [jax.ShapeDtypeStruct(shape, blocks[0].dtype)], 10**8, place, *blocks, mib=9
    )[0]


def my_half(place, array):
    rows = array.shape[0] // 2

    def half(place_ref, ref, out):
        out[...] = ref[pl.ds(pl.multiple_of(place_ref[1] * rows, rows), rows), :]

    shape = jax.ShapeDtypeStruct((rows, array.shape[1]), array.dtype)
    return call(half, [shape], 10**8, place, array, mib=6)[0]


def up_products(place, features, weights, picks):
    rows = features[0].shape[0] // 4
    depth = sum(p.shape[1] for p in features)
    wide = weights[0].shape[1]

    def up(place_ref, *refs):
        pieces, refs = refs[: len(features)], refs[len(features) :]
        w_refs, outs = refs[: len(weights)], refs[len(weights) :]
        for i, out in enumerate(outs):
            start = pl.multiple_of((place_ref[0] + i) % 4 * rows, rows)
            blocks = [piece[pl.ds(start, rows), :] for piece in pieces]
            for n, (w, half) in enumerate(picks):
                half = place_ref[1] if half is None else half
                total, done = None, 0
                for block in blocks:
                    first = half * depth + done
                    if not isinstance(first, int):
                        first = pl.multiple_of(first, block.shape[1])
                    term = dot(block, w_refs[w][pl.ds(first, block.shape[1]), :])
                    total = term if total is None else total + term
                    done += block.shape[1]
                out[:, n * wide : (n + 1) * wide] = total.astype(out.dtype)

    full = wide * len(picks)
    shapes = [jax.ShapeDtypeStruct((rows, full), bf16 if i else f32) for i in range(4)]
    return call(up, shapes, 8 * rows * full * depth, place, *features, *weights)


def down_products(place, hidden, weights, picks, begun, last):
    rows = hidden[0].shape[0]
    wide = hidden[0].shape[1] // len(picks)
    each = weights[0].shape[1]

    def down(place_ref, *refs):
        h_refs, refs = refs[:4], refs[4:]
        w_refs, refs = refs[: len(weights)], refs[len(weights) :]
        s_refs, outs = refs[: len(begun)], refs[len(begun) :]
        for i, h_ref in enumerate(h_refs):
            start = pl.multiple_of((place_ref[0] + i) % 4 * rows, rows)
            for j, out in enumerate(outs):
                total = s_refs[j][pl.ds(start, rows), :] if begun else None
                for n, (w, half) in enumerate(picks):
                    half = place_ref[1] if half is None else half
                    first = (half * 4 + j) * wide
                    if not isinstance(first, int):
                        first = pl.multiple_of(first, wide)
                    term = dot(
                        h_ref[:, n * wide : (n + 1) * wide], w_refs[w][pl.ds(first, wide), :]
                    )
                    total = term if total is None else total + term
                out[pl.ds(start, rows), :] = total.astype(out.dtype)

    shapes = [
        jax.ShapeDtypeStruct((4 * rows, each), bf16 if last and j else f32) for j in range(4)
    ]
    flops = 2 * 4 * rows * wide * len(picks) * 4 * each
    return call(down, shapes, flops, place, *hidden, *weights, *begun)


def own_sums(mixed):
    sums = jnp.stack([jnp.sum(mixed, axis=1), jnp.sum(mixed * mixed, axis=1)])
    return sums.reshape(-1, 128)


def scales(sums, width):
    sums = sums.reshape(2, -1)
    mean = sums[0] / width
    return mean[:, None], lax.rsqrt(sums[1] / width - mean * mean + norm_eps)[:, None]


def group_sums(mixed):
    sums = own_sums(mixed)
    members = lax.axis_size("ra")
    sent = jnp.broadcast_to(sums[None], (members, *sums.shape))
    sums = lax.all_to_all(sent, "ra", 0, 0, tiled=True)
    return sums.sum(axis=0)


def layer(carried, branch_in, gain_in, bias_in, up_weight, down_weight, gain_out, bias_out):
    width = carried.shape[1] * lax.axis_size("ra")
    r, y, c = lax.axis_index("ra"), lax.axis_index("cb"), lax.axis_index("dp")
    z, x = r // 4, r % 4
    a, b = jnp.where(c == 0, x, z), jnp.where(c == 0, z, x)
    place = jnp.stack([(b - 2 * c) % 4, c, a]).astype(jnp.int32)
    held = carried.shape[1]
    few = carried.shape[0] // 4
    wide = up_weight.shape[1] // 8

    def gathered(cuts):
        blocks = [cuts[0]] + [from_gather_ring(cut, j) for j, cut in zip(others, cuts[1:])]
        own = stacked(place, blocks, 2)
        near = from_next_plane(own)
        return own, near, from_next_plane(my_half(place, near))

    up_own, up_near, up_far = gathered(cut_columns(place, up_weight, wide))
    down_own, down_near, down_far = gathered(cut_rows(place, down_weight, wide))

    def quarter(array):
        return lax.dynamic_slice(array, (y * few, 0), (few, held)).astype(f32)

    mixed_in = residual_scale * quarter(carried) + quarter(branch_in)
    sums = own_sums(mixed_in)
    sums = sum([from_sum_ring(sums, j) for j in others], sums)
    sums = sum([from_gather_ring(sums, j) for j in others], sums)
    mean, inverse = scales(sums, width)
    normed = (mixed_in - mean) * inverse * gain_in + bias_in
    normed = normed.astype(bf16)
    both = stacked(place, [normed, from_other_core(normed)], 1)
    features = [both] + [from_gather_ring(both, j) for j in others]

    def activated(weights, picks):
        parts = up_products(place, features, weights, picks)
        total = parts[0]
        for j in (1, 2, 3):
            total = total + to_sum_ring(parts[j], j).astype(f32)
        own = jnp.square(jnp.maximum(total, 0.0)).astype(bf16)
        return [own] + [from_sum_ring(own, j) for j in (1, 2, 3)]

    picks = [(0, None), (1, 0), (1, 1)]
    near = activated([up_own, up_near], picks)
    far = activated([up_far], [(0, 0)])
    begun = down_products(place, near, [down_own, down_near], picks, [], False)
    parts = down_products(place, far, [down_far], [(0, 0)], begun, True)
    total = parts[0]
    for j, part in zip(others, parts[1:]):
        total = total + to_gather_ring(part, j).astype(f32)
    mine, theirs = total[:few], from_other_core(total[few:])
    mixed_out = residual_scale * normed.astype(f32) + (mine + theirs)
    mean, inverse = scales(group_sums(mixed_out), width)
    out = (mixed_out - mean) * inverse * gain_out + bias_out
    out = out.astype(bf16)
    result = jnp.zeros(carried.shape, bf16)
    for d in range(4):
        block = from_plane(out, d) if d else out
        result = lax.dynamic_update_slice(result, block, ((y + d) % 4 * few, 0))
    return result


def solution(mesh):
    in_specs = (
        P("dp", "ra"),
        P("dp", "ra"),
        P("ra"),
        P("ra"),
        P("ra", "cb"),
        P("cb", "ra"),
        P("ra"),
        P("ra"),
    )
    return jax.shard_map(
        layer, mesh=mesh, in_specs=in_specs, out_specs=P("dp", "ra"), check_vma=False
    )
```

time: 192 us -> 175 us (0.911)
  starting transfers between devices: 76.3 us -> 60.1 us
  Pallas kernels: 7.54 us -> 17.8 us
  waiting for transfers between devices: 96.5 us -> 89.3 us
  local copies, waits for them, and re-layouts: 6.28 us -> 3.09 us
    ppermute x11 -> x3, waiting for transfers between devices: 36.1 us -> 9.66 us  [from_plane(): lax.ppermute(array, 'cb', [((y + distance) % 4, y) for y in range(4)])]
    ppermute x11 -> x3, starting transfers between devices: 17.1 us -> 3.4 us  [from_plane(): lax.ppermute(array, 'cb', [((y + distance) % 4, y) for y in range(4)])]
    ppermute x9 -> x6, waiting for transfers between devices: 2.54 us -> 14.3 us  [to_sum_ring(): return lax.ppermute(array, ('ra', 'dp'), ring_pairs(False, -distance))]
    pallas_call x8 -> x11, Pallas kernels: 7.54 us -> 17.8 us  [call(): pl.pallas_call(body, out_shape=out_shape, in_specs=[pl.BlockSpec(memory_s...]
    ppermute x9 -> x6, starting transfers between devices: 17.5 us -> 8.87 us  [to_sum_ring(): return lax.ppermute(array, ('ra', 'dp'), ring_pairs(False, -distance))]
    ppermute x0 -> x4, waiting for transfers between devices: none -> 6.98 us  [from_next_plane(): return lax.ppermute(array, ('cb', 'dp'), pairs)]
    all_to_all x2 -> x1, starting transfers between devices: 13 us -> 6.34 us  [group_sums(): sums = lax.all_to_all(sent, 'ra', 0, 0, tiled=True)]
    ppermute x9 -> x12, starting transfers between devices: 11.4 us -> 17.7 us  [from_gather_ring(): return lax.ppermute(array, ('ra', 'dp'), ring_pairs(True, distance))]
  transfers between devices with their start and end apart: 46 -> 40, of which waited for: 24 -> 22; matrix products, arithmetic and copies ran while one was open for 4% -> 2% of each run, Pallas kernels for 3% -> 9%
where the time goes in v2:
time: 175 us; the launch traced here: 174 us
  waiting for transfers between devices  89.3 us (51%)
  starting transfers between devices  60.1 us (34%)
  Pallas kernels  17.8 us (10%)
  other arithmetic  3.58 us (2%)
  local copies, waits for them, and re-layouts  3.09 us (2%)
    ppermute x12, waiting for transfers between devices, from_gather_ring(): return lax.ppermute(array, ('ra', 'dp'), ring_pairs(True, distance))  22.4 us
    pallas_call x11, Pallas kernels, call(): pl.pallas_call(body, out_shape=out_shape, in_specs=[pl.BlockSpec(memory_s...  17.8 us
    ppermute x12, starting transfers between devices, from_gather_ring(): return lax.ppermute(array, ('ra', 'dp'), ring_pairs(True, distance))  17.7 us
    ppermute x9, waiting for transfers between devices, from_sum_ring(): return lax.ppermute(array, ('ra', 'dp'), ring_pairs(False, distance))  15.2 us
    ppermute x6, waiting for transfers between devices, to_sum_ring(): return lax.ppermute(array, ('ra', 'dp'), ring_pairs(False, -distance))  14.3 us
    ppermute x9, starting transfers between devices, from_sum_ring(): return lax.ppermute(array, ('ra', 'dp'), ring_pairs(False, distance))  14.2 us
    ppermute x3, waiting for transfers between devices, to_gather_ring(): return lax.ppermute(array, ('ra', 'dp'), ring_pairs(True, -distance))  9.97 us
    ppermute x3, waiting for transfers between devices, from_plane(): lax.ppermute(array, 'cb', [((y + distance) % 4, y) for y in range(4)])  9.66 us
  transfers between devices with their start and end apart: 40, of which 22 were waited for; matrix products, arithmetic and copies ran while one was open for 2% of the time, Pallas kernels for 9%

profile of v2, /device:TPU:0, one launch (start us, length us, event | category | flops | bytes accessed | tf_op | source)
XLA Modules:
  0.0 174.3 jit_solution(4828569113543604106)
XLA Ops:
  2.4 2.9 %collective-permute-start.10 = (bf16[512,512]{1,0:T(8,128)(2,1)S(1)}, bf16[512,512]{1,0:T(8,128)(2,1)S(1)}, u32[]{:S(2)}, u32[]{:S(2)}) collective-permute-start(bf16[512,512]{1,0:T(8,128)(2,1)S(1)} %get-tuple-element.30), channel_id=1, source_target_pairs={{8,0},{33,1},{16,8},{41,9},{24,16},{49,17},{0,24},{57,25},{40,32},... | collective-permute-start | bytes 1572872 | tf_op jit(solution)/shard_map/ppermute | solution.py:29
  7.6 10.0 %collective-permute-done.10.refs_1_ = bf16[512,512]{1,0:T(8,128)(2,1)S(1)} collective-permute-done((bf16[512,512]{1,0:T(8,128)(2,1)S(1)}, bf16[512,512]{1,0:T(8,128)(2,1)S(1)}, u32[]{:S(2)}, u32[]{:S(2)}) %collective-permute-start.10) | collective-permute-done | bytes 524320 | tf_op jit(solution)/shard_map/ppermute | solution.py:29
  17.6 3.7 %collective-permute-done.11.refs_2_ = bf16[512,512]{1,0:T(8,128)(2,1)S(1)} collective-permute-done((bf16[512,512]{1,0:T(8,128)(2,1)S(1)}, bf16[512,512]{1,0:T(8,128)(2,1)S(1)}, u32[]{:S(2)}, u32[]{:S(2)}) %collective-permute-start.11) | collective-permute-done | bytes 524320 | tf_op jit(solution)/shard_map/ppermute | solution.py:29
  22.0 3.1 %collective-permute-start.13 = (bf16[2048,512]{1,0:T(8,128)(2,1)S(1)}, bf16[2048,512]{1,0:T(8,128)(2,1)}, u32[]{:S(2)}, u32[]{:S(2)}) collective-permute-start(bf16[2048,512]{1,0:T(8,128)(2,1)S(1)} %shard_map.84.refs_4_), channel_id=1, source_target_pairs={{2,0},{7,1},{4,2},{1,3},{6,4},{3,5},{0,6},{5,7},{10,8},{15,9},{12,... | collective-permute-start | bytes 6291464 | tf_op jit(solution)/shard_map/ppermute | solution.py:53
  30.5 4.1 %collective-permute-start = (f32[6,128]{1,0:T(8,128)S(1)}, f32[6,128]{1,0:T(8,128)S(1)}, u32[]{:S(2)}, u32[]{:S(2)}) collective-permute-start(f32[6,128]{1,0:T(8,128)S(1)} %reshape.60), channel_id=1, source_target_pairs={{32,0},{9,1},{40,8},{17,9},{48,16},{25,17},{56,24},{1,25},{64,32},... | collective-permute-start | bytes 9224 | tf_op jit(solution)/shard_map/ppermute | solution.py:37
  36.5 4.9 %collective-permute-done.1 = f32[6,128]{1,0:T(8,128)S(1)} collective-permute-done((f32[6,128]{1,0:T(8,128)S(1)}, f32[6,128]{1,0:T(8,128)S(1)}, u32[]{:S(2)}, u32[]{:S(2)}) %collective-permute-start.1) | collective-permute-done | bytes 3104 | tf_op jit(solution)/shard_map/ppermute | solution.py:37
  42.6 3.9 %collective-permute-done.2 = f32[6,128]{1,0:T(8,128)S(1)} collective-permute-done((f32[6,128]{1,0:T(8,128)S(1)}, f32[6,128]{1,0:T(8,128)S(1)}, u32[]{:S(2)}, u32[]{:S(2)}) %collective-permute-start.2) | collective-permute-done | bytes 3104 | tf_op jit(solution)/shard_map/ppermute | solution.py:37
  48.9 2.9 %collective-permute-start.5 = (f32[6,128]{1,0:T(8,128)S(1)}, f32[6,128]{1,0:T(8,128)S(1)}, u32[]{:S(2)}, u32[]{:S(2)}) collective-permute-start(f32[6,128]{1,0:T(8,128)S(1)} %add_add_fusion.1), channel_id=1, source_target_pairs={{16,0},{65,1},{24,8},{73,9},{0,16},{81,17},{8,24},{89,25},{48,32},... | collective-permute-start | bytes 9224 | tf_op jit(solution)/shard_map/ppermute | solution.py:29
  57.5 3.2 %collective-permute-start.7 = (bf16[768,256]{1,0:T(8,128)(2,1)S(1)}, bf16[768,256]{1,0:T(8,128)(2,1)S(1)}, u32[]{:S(2)}, u32[]{:S(2)}) collective-permute-start(bf16[768,256]{1,0:T(8,128)(2,1)S(1)} %shard_map.82.refs_0_), channel_id=1, source_target_pairs={{8,0},{33,1},{16,8},{41,9},{24,16},{49,17},{0,24},{57,25},{40,32},... | collective-permute-start | bytes 1179656 | tf_op jit(solution)/shard_map/ppermute | solution.py:29
  65.2 5.0 %collective-permute-done.7.refs_1_ = bf16[768,256]{1,0:T(8,128)(2,1)S(1)} collective-permute-done((bf16[768,256]{1,0:T(8,128)(2,1)S(1)}, bf16[768,256]{1,0:T(8,128)(2,1)S(1)}, u32[]{:S(2)}, u32[]{:S(2)}) %collective-permute-start.7) | collective-permute-done | bytes 393248 | tf_op jit(solution)/shard_map/ppermute | solution.py:29
  70.2 3.7 %collective-permute-done.8.refs_2_ = bf16[768,256]{1,0:T(8,128)(2,1)S(1)} collective-permute-done((bf16[768,256]{1,0:T(8,128)(2,1)S(1)}, bf16[768,256]{1,0:T(8,128)(2,1)S(1)}, u32[]{:S(2)}, u32[]{:S(2)}) %collective-permute-start.8) | collective-permute-done | bytes 393248 | tf_op jit(solution)/shard_map/ppermute | solution.py:29
  73.9 4.2 %shard_map.90 = (f32[192,1536]{1,0:T(8,128)S(1)}, bf16[192,1536]{1,0:T(8,128)(2,1)S(1)}, bf16[192,1536]{1,0:T(8,128)(2,1)S(1)}, bf16[192,1536]{1,0:T(8,128)(2,1)S(1)}) custom-call(s32[3]{0:T(128)S(1)} %pad_add_fusion.place_ref, bf16[768,256]{1,0:T(8,128)(2,1)S(1)} %shard_map.82.refs_0_, bf16[768,256]{1,0:T(8,128)(2,1)S(1)} %collective-permute-done.7.refs_1_, ...), custom_call_target="tpu_custom_call" | custom-call | flops 2415919104 | bytes 5767168 | tf_op jit(solution)/shard_map/pallas_call | solution.py:67
  78.2 3.5 %collective-permute-start.27 = (bf16[192,1536]{1,0:T(8,128)(2,1)S(1)}, bf16[192,1536]{1,0:T(8,128)(2,1)S(1)}, u32[]{:S(2)}, u32[]{:S(2)}) collective-permute-start(bf16[192,1536]{1,0:T(8,128)(2,1)S(1)} %get-tuple-element.43), channel_id=1, source_target_pairs={{64,0},{17,1},{72,8},{25,9},{80,16},{1,17},{88,24},{9,25},{96,32},... | collective-permute-start | bytes 1769480 | tf_op jit(solution)/shard_map/ppermute | solution.py:41
  83.5 7.0 %collective-permute-done.14.refs_4_ = bf16[1024,512]{1,0:T(8,128)(2,1)S(1)} collective-permute-done((bf16[1024,512]{1,0:T(8,128)(2,1)S(1)}, bf16[1024,512]{1,0:T(8,128)(2,1)S(1)}, u32[]{:S(2)}, u32[]{:S(2)}) %collective-permute-start.14) | collective-permute-done | bytes 1048608 | tf_op jit(solution)/shard_map/ppermute | solution.py:53
  92.3 3.5 %collective-permute-start.16 = (bf16[192,512]{1,0:T(8,128)(2,1)S(1)}, bf16[192,512]{1,0:T(8,128)(2,1)S(1)}, u32[]{:S(2)}, u32[]{:S(2)}) collective-permute-start(bf16[192,512]{1,0:T(8,128)(2,1)S(1)} %get-tuple-element.35), channel_id=1, source_target_pairs={{64,0},{17,1},{72,8},{25,9},{80,16},{1,17},{88,24},{9,25},{96,32},... | collective-permute-start | bytes 589832 | tf_op jit(solution)/shard_map/ppermute | solution.py:41
  96.8 2.7 %collective-permute-start.29 = (bf16[192,1536]{1,0:T(8,128)(2,1)S(1)}, bf16[192,1536]{1,0:T(8,128)(2,1)S(1)}, u32[]{:S(2)}, u32[]{:S(2)}) collective-permute-start(bf16[192,1536]{1,0:T(8,128)(2,1)S(1)} %multiply_convert_fusion.refs_0_), channel_id=1, source_target_pairs={{32,0},{9,1},{40,8},{17,9},{48,16},{25,17},{56,24},{1,25},{64,32},... | collective-permute-start | bytes 1769480 | tf_op jit(solution)/shard_map/ppermute | solution.py:37
  102.8 12.6 %collective-permute-done.17 = bf16[192,512]{1,0:T(8,128)(2,1)S(1)} collective-permute-done((bf16[192,512]{1,0:T(8,128)(2,1)S(1)}, bf16[192,512]{1,0:T(8,128)(2,1)S(1)}, u32[]{:S(2)}, u32[]{:S(2)}) %collective-permute-start.17) | collective-permute-done | bytes 196640 | tf_op jit(solution)/shard_map/ppermute | solution.py:41
  115.5 3.8 %collective-permute-start.18 = (bf16[192,512]{1,0:T(8,128)(2,1)S(1)}, bf16[192,512]{1,0:T(8,128)(2,1)S(1)}, u32[]{:S(2)}, u32[]{:S(2)}) collective-permute-start(bf16[192,512]{1,0:T(8,128)(2,1)S(1)} %multiply_convert_fusion.1.refs_0_), channel_id=1, source_target_pairs={{32,0},{9,1},{40,8},{17,9},{48,16},{25,17},{56,24},{1,25},{64,32},... | collective-permute-start | bytes 589832 | tf_op jit(solution)/shard_map/ppermute | solution.py:37
  120.2 3.1 %shard_map.91 = (f32[768,256]{1,0:T(8,128)S(1)}, f32[768,256]{1,0:T(8,128)S(1)}, f32[768,256]{1,0:T(8,128)S(1)}, f32[768,256]{1,0:T(8,128)S(1)}) custom-call(s32[3]{0:T(128)S(1)} %pad_add_fusion.place_ref, bf16[192,1536]{1,0:T(8,128)(2,1)S(1)} %multiply_convert_fusion.refs_0_, bf16[192,1536]{1,0:T(8,128)(2,1)S(1)} %collective-permute-done.29.refs_1_, ...), custom_call_target="tpu_custom_call" | custom-call | flops 2415919104 | bytes 6553600 | tf_op jit(solution)/shard_map/pallas_call | solution.py:67
  130.1 3.2 %collective-permute-start.33 = (bf16[768,256]{1,0:T(8,128)(2,1)S(1)}, bf16[768,256]{1,0:T(8,128)(2,1)S(1)}, u32[]{:S(2)}, u32[]{:S(2)}) collective-permute-start(bf16[768,256]{1,0:T(8,128)(2,1)S(1)} %get-tuple-element.51), channel_id=1, source_target_pairs={{8,0},{33,1},{16,8},{41,9},{24,16},{49,17},{0,24},{57,25},{40,32},... | collective-permute-start | bytes 1179656 | tf_op jit(solution)/shard_map/ppermute | solution.py:33
  133.3 10.0 %collective-permute-done.32 = bf16[768,256]{1,0:T(8,128)(2,1)S(1)} collective-permute-done((bf16[768,256]{1,0:T(8,128)(2,1)S(1)}, bf16[768,256]{1,0:T(8,128)(2,1)S(1)}, u32[]{:S(2)}, u32[]{:S(2)}) %collective-permute-start.32) | collective-permute-done | bytes 393248 | tf_op jit(solution)/shard_map/ppermute | solution.py:33
  146.2 6.3 %all-to-all-start = ((f32[16,6,128]{2,1,0:T(8,128)}), f32[16,6,128]{2,1,0:T(8,128)S(1)}, u32[]{:S(2)}, u32[]{:S(2)}) async-start(f32[16,6,128]{2,1,0:T(8,128)} %broadcast_in_dim.8), calls=%async_computation | async-start | bytes 131072 | tf_op jit(solution)/shard_map/all_to_all | solution.py:200
  152.6 7.7 %all-to-all-done = f32[16,6,128]{2,1,0:T(8,128)S(1)} async-done(((f32[16,6,128]{2,1,0:T(8,128)}), f32[16,6,128]{2,1,0:T(8,128)S(1)}, u32[]{:S(2)}, u32[]{:S(2)}) %all-to-all-start) | async-done | bytes 49184 | tf_op jit(solution)/shard_map/all_to_all | solution.py:200
  163.9 6.3 %collective-permute-done.36 = bf16[384,256]{1,0:T(8,128)(2,1)S(1)} collective-permute-done((bf16[384,256]{1,0:T(8,128)(2,1)S(1)}, bf16[384,256]{1,0:T(8,128)(2,1)S(1)}, u32[]{:S(2)}, u32[]{:S(2)}) %collective-permute-start.36) | collective-permute-done | bytes 196640 | tf_op jit(solution)/shard_map/ppermute | solution.py:45
  (110 shorter events, 52.7 us)
Async XLA Ops:
  2.4 15.3 %collective-permute-start.10 = (bf16[512,512]{1,0:T(8,128)(2,1)S(1)}, bf16[512,512]{1,0:T(8,128)(2,1)S(1)}, u32[]{:S(2)}, u32[]{:S(2)}) collective-permute-start(bf16[512,512]{1,0:T(8,128)(2,1)S(1)} %get-tuple-element.30), channel_id=1, source_target_pairs={{8,0},{33,1},{16,8},{41,9},{24,16},{49,17},{0,24},{57,25},{40,32},... | collective-permute-start | bytes 1572872 | tf_op jit(solution)/shard_map/ppermute | solution.py:29
  5.3 16.0 %collective-permute-start.11 = (bf16[512,512]{1,0:T(8,128)(2,1)S(1)}, bf16[512,512]{1,0:T(8,128)(2,1)S(1)}, u32[]{:S(2)}, u32[]{:S(2)}) collective-permute-start(bf16[512,512]{1,0:T(8,128)(2,1)S(1)} %get-tuple-element.31), channel_id=1, source_target_pairs={{24,0},{97,1},{0,8},{105,9},{8,16},{113,17},{16,24},{121,25},{56,3... | collective-permute-start | bytes 1572872 | tf_op jit(solution)/shard_map/ppermute | solution.py:29
  5.3 16.0 %collective-permute-start.12 = (bf16[512,512]{1,0:T(8,128)(2,1)S(1)}, bf16[512,512]{1,0:T(8,128)(2,1)S(1)}, u32[]{:S(2)}, u32[]{:S(2)}) collective-permute-start(bf16[512,512]{1,0:T(8,128)(2,1)S(1)} %get-tuple-element.32), channel_id=1, source_target_pairs={{16,0},{65,1},{24,8},{73,9},{0,16},{81,17},{8,24},{89,25},{48,32},... | collective-permute-start | bytes 1572872 | tf_op jit(solution)/shard_map/ppermute | solution.py:29
  22.0 40.3 %collective-permute-start.13 = (bf16[2048,512]{1,0:T(8,128)(2,1)S(1)}, bf16[2048,512]{1,0:T(8,128)(2,1)}, u32[]{:S(2)}, u32[]{:S(2)}) collective-permute-start(bf16[2048,512]{1,0:T(8,128)(2,1)S(1)} %shard_map.84.refs_4_), channel_id=1, source_target_pairs={{2,0},{7,1},{4,2},{1,3},{6,4},{3,5},{0,6},{5,7},{10,8},{15,9},{12,... | collective-permute-start | bytes 6291464 | tf_op jit(solution)/shard_map/ppermute | solution.py:53
  26.9 22.0 %collective-permute-start.21 = (bf16[1024,256]{1,0:T(8,128)(2,1)}, bf16[1024,256]{1,0:T(8,128)(2,1)S(1)}, u32[]{:S(2)}, u32[]{:S(2)}) collective-permute-start(bf16[1024,256]{1,0:T(8,128)(2,1)} %get-tuple-element.38), channel_id=1, source_target_pairs={{8,0},{33,1},{16,8},{41,9},{24,16},{49,17},{0,24},{57,25},{40,32},... | collective-permute-start | bytes 1572872 | tf_op jit(solution)/shard_map/ppermute | solution.py:29
  26.9 22.0 %collective-permute-start.22 = (bf16[1024,256]{1,0:T(8,128)(2,1)}, bf16[1024,256]{1,0:T(8,128)(2,1)}, u32[]{:S(2)}, u32[]{:S(2)}) collective-permute-start(bf16[1024,256]{1,0:T(8,128)(2,1)} %get-tuple-element.39), channel_id=1, source_target_pairs={{24,0},{97,1},{0,8},{105,9},{8,16},{113,17},{16,24},{121,25},{56,3... | collective-permute-start | bytes 1572872 | tf_op jit(solution)/shard_map/ppermute | solution.py:29
  28.9 22.9 %collective-permute-start.23 = (bf16[1024,256]{1,0:T(8,128)(2,1)}, bf16[1024,256]{1,0:T(8,128)(2,1)}, u32[]{:S(2)}, u32[]{:S(2)}) collective-permute-start(bf16[1024,256]{1,0:T(8,128)(2,1)} %get-tuple-element.40), channel_id=1, source_target_pairs={{16,0},{65,1},{24,8},{73,9},{0,16},{81,17},{8,24},{89,25},{48,32},... | collective-permute-start | bytes 1572872 | tf_op jit(solution)/shard_map/ppermute | solution.py:29
  53.2 28.8 %collective-permute-start.24 = (bf16[4096,256]{1,0:T(8,128)(2,1)S(1)}, bf16[4096,256]{1,0:T(8,128)(2,1)S(1)}, u32[]{:S(2)}, u32[]{:S(2)}) collective-permute-start(bf16[4096,256]{1,0:T(8,128)(2,1)S(1)} %shard_map.88.refs_4_), channel_id=1, source_target_pairs={{2,0},{7,1},{4,2},{1,3},{6,4},{3,5},{0,6},{5,7},{10,8},{15,9},{12,... | collective-permute-start | bytes 6291464 | tf_op jit(solution)/shard_map/ppermute | solution.py:53
  57.5 12.7 %collective-permute-start.7 = (bf16[768,256]{1,0:T(8,128)(2,1)S(1)}, bf16[768,256]{1,0:T(8,128)(2,1)S(1)}, u32[]{:S(2)}, u32[]{:S(2)}) collective-permute-start(bf16[768,256]{1,0:T(8,128)(2,1)S(1)} %shard_map.82.refs_0_), channel_id=1, source_target_pairs={{8,0},{33,1},{16,8},{41,9},{24,16},{49,17},{0,24},{57,25},{40,32},... | collective-permute-start | bytes 1179656 | tf_op jit(solution)/shard_map/ppermute | solution.py:29
  60.7 13.2 %collective-permute-start.8 = (bf16[768,256]{1,0:T(8,128)(2,1)S(1)}, bf16[768,256]{1,0:T(8,128)(2,1)S(1)}, u32[]{:S(2)}, u32[]{:S(2)}) collective-permute-start(bf16[768,256]{1,0:T(8,128)(2,1)S(1)} %shard_map.82.refs_0_), channel_id=1, source_target_pairs={{24,0},{97,1},{0,8},{105,9},{8,16},{113,17},{16,24},{121,25},{56,3... | collective-permute-start | bytes 1179656 | tf_op jit(solution)/shard_map/ppermute | solution.py:29
  60.7 13.2 %collective-permute-start.9 = (bf16[768,256]{1,0:T(8,128)(2,1)S(1)}, bf16[768,256]{1,0:T(8,128)(2,1)S(1)}, u32[]{:S(2)}, u32[]{:S(2)}) collective-permute-start(bf16[768,256]{1,0:T(8,128)(2,1)S(1)} %shard_map.82.refs_0_), channel_id=1, source_target_pairs={{16,0},{65,1},{24,8},{73,9},{0,16},{81,17},{8,24},{89,25},{48,32},... | collective-permute-start | bytes 1179656 | tf_op jit(solution)/shard_map/ppermute | solution.py:29
  64.0 26.5 %collective-permute-start.14 = (bf16[1024,512]{1,0:T(8,128)(2,1)S(1)}, bf16[1024,512]{1,0:T(8,128)(2,1)S(1)}, u32[]{:S(2)}, u32[]{:S(2)}) collective-permute-start(bf16[1024,512]{1,0:T(8,128)(2,1)S(1)} %shard_map.85), channel_id=1, source_target_pairs={{2,0},{7,1},{4,2},{1,3},{6,4},{3,5},{0,6},{5,7},{10,8},{15,9},{12,... | collective-permute-start | bytes 3145736 | tf_op jit(solution)/shard_map/ppermute | solution.py:53
  78.1 14.2 %collective-permute-start.26 = (bf16[192,1536]{1,0:T(8,128)(2,1)S(1)}, bf16[192,1536]{1,0:T(8,128)(2,1)S(1)}, u32[]{:S(2)}, u32[]{:S(2)}) collective-permute-start(bf16[192,1536]{1,0:T(8,128)(2,1)S(1)} %get-tuple-element.42), channel_id=1, source_target_pairs={{96,0},{25,1},{104,8},{1,9},{112,16},{9,17},{120,24},{17,25},{0,32... | collective-permute-start | bytes 1769480 | tf_op jit(solution)/shard_map/ppermute | solution.py:41
  78.2 17.6 %collective-permute-start.27 = (bf16[192,1536]{1,0:T(8,128)(2,1)S(1)}, bf16[192,1536]{1,0:T(8,128)(2,1)S(1)}, u32[]{:S(2)}, u32[]{:S(2)}) collective-permute-start(bf16[192,1536]{1,0:T(8,128)(2,1)S(1)} %get-tuple-element.43), channel_id=1, source_target_pairs={{64,0},{17,1},{72,8},{25,9},{80,16},{1,17},{88,24},{9,25},{96,32},... | collective-permute-start | bytes 1769480 | tf_op jit(solution)/shard_map/ppermute | solution.py:41
  81.7 14.8 %collective-permute-start.28 = (bf16[192,1536]{1,0:T(8,128)(2,1)S(1)}, bf16[192,1536]{1,0:T(8,128)(2,1)S(1)}, u32[]{:S(2)}, u32[]{:S(2)}) collective-permute-start(bf16[192,1536]{1,0:T(8,128)(2,1)S(1)} %get-tuple-element.44), channel_id=1, source_target_pairs={{32,0},{9,1},{40,8},{17,9},{48,16},{25,17},{56,24},{1,25},{64,32},... | collective-permute-start | bytes 1769480 | tf_op jit(solution)/shard_map/ppermute | solution.py:41
  82.6 40.7 %collective-permute-start.25 = (bf16[2048,256]{1,0:T(8,128)(2,1)S(1)}, bf16[2048,256]{1,0:T(8,128)(2,1)S(1)}, u32[]{:S(2)}, u32[]{:S(2)}) collective-permute-start(bf16[2048,256]{1,0:T(8,128)(2,1)S(1)} %shard_map.89), channel_id=1, source_target_pairs={{2,0},{7,1},{4,2},{1,3},{6,4},{3,5},{0,6},{5,7},{10,8},{15,9},{12,... | collective-permute-start | bytes 3145736 | tf_op jit(solution)/shard_map/ppermute | solution.py:53
  96.8 22.4 %collective-permute-start.29 = (bf16[192,1536]{1,0:T(8,128)(2,1)S(1)}, bf16[192,1536]{1,0:T(8,128)(2,1)S(1)}, u32[]{:S(2)}, u32[]{:S(2)}) collective-permute-start(bf16[192,1536]{1,0:T(8,128)(2,1)S(1)} %multiply_convert_fusion.refs_0_), channel_id=1, source_target_pairs={{32,0},{9,1},{40,8},{17,9},{48,16},{25,17},{56,24},{1,25},{64,32},... | collective-permute-start | bytes 1769480 | tf_op jit(solution)/shard_map/ppermute | solution.py:37
  99.5 19.7 %collective-permute-start.30 = (bf16[192,1536]{1,0:T(8,128)(2,1)S(1)}, bf16[192,1536]{1,0:T(8,128)(2,1)S(1)}, u32[]{:S(2)}, u32[]{:S(2)}) collective-permute-start(bf16[192,1536]{1,0:T(8,128)(2,1)S(1)} %multiply_convert_fusion.refs_0_), channel_id=1, source_target_pairs={{64,0},{17,1},{72,8},{25,9},{80,16},{1,17},{88,24},{9,25},{96,32},... | collective-permute-start | bytes 1769480 | tf_op jit(solution)/shard_map/ppermute | solution.py:37
  99.5 20.7 %collective-permute-start.31 = (bf16[192,1536]{1,0:T(8,128)(2,1)S(1)}, bf16[192,1536]{1,0:T(8,128)(2,1)S(1)}, u32[]{:S(2)}, u32[]{:S(2)}) collective-permute-start(bf16[192,1536]{1,0:T(8,128)(2,1)S(1)} %multiply_convert_fusion.refs_0_), channel_id=1, source_target_pairs={{96,0},{25,1},{104,8},{1,9},{112,16},{9,17},{120,24},{17,25},{0,32... | collective-permute-start | bytes 1769480 | tf_op jit(solution)/shard_map/ppermute | solution.py:37
  101.5 13.8 %collective-permute-start.17 = (bf16[192,512]{1,0:T(8,128)(2,1)S(1)}, bf16[192,512]{1,0:T(8,128)(2,1)S(1)}, u32[]{:S(2)}, u32[]{:S(2)}) collective-permute-start(bf16[192,512]{1,0:T(8,128)(2,1)S(1)} %get-tuple-element.36), channel_id=1, source_target_pairs={{32,0},{9,1},{40,8},{17,9},{48,16},{25,17},{56,24},{1,25},{64,32},... | collective-permute-start | bytes 589832 | tf_op jit(solution)/shard_map/ppermute | solution.py:41
  130.0 13.3 %collective-permute-start.32 = (bf16[768,256]{1,0:T(8,128)(2,1)S(1)}, bf16[768,256]{1,0:T(8,128)(2,1)S(1)}, u32[]{:S(2)}, u32[]{:S(2)}) collective-permute-start(bf16[768,256]{1,0:T(8,128)(2,1)S(1)} %get-tuple-element.50), channel_id=1, source_target_pairs={{24,0},{97,1},{0,8},{105,9},{8,16},{113,17},{16,24},{121,25},{56,3... | collective-permute-start | bytes 1179656 | tf_op jit(solution)/shard_map/ppermute | solution.py:33
  130.1 13.2 %collective-permute-start.33 = (bf16[768,256]{1,0:T(8,128)(2,1)S(1)}, bf16[768,256]{1,0:T(8,128)(2,1)S(1)}, u32[]{:S(2)}, u32[]{:S(2)}) collective-permute-start(bf16[768,256]{1,0:T(8,128)(2,1)S(1)} %get-tuple-element.51), channel_id=1, source_target_pairs={{8,0},{33,1},{16,8},{41,9},{24,16},{49,17},{0,24},{57,25},{40,32},... | collective-permute-start | bytes 1179656 | tf_op jit(solution)/shard_map/ppermute | solution.py:33
  146.2 14.0 %all-to-all-start = ((f32[16,6,128]{2,1,0:T(8,128)}), f32[16,6,128]{2,1,0:T(8,128)S(1)}, u32[]{:S(2)}, u32[]{:S(2)}) async-start(f32[16,6,128]{2,1,0:T(8,128)} %broadcast_in_dim.8), calls=%async_computation | async-start | bytes 131072 | tf_op jit(solution)/shard_map/all_to_all | solution.py:200
  163.0 10.7 %collective-permute-start.38 = (bf16[384,256]{1,0:T(8,128)(2,1)S(1)}, bf16[384,256]{1,0:T(8,128)(2,1)S(1)}, u32[]{:S(2)}, u32[]{:S(2)}) collective-permute-start(bf16[384,256]{1,0:T(8,128)(2,1)S(1)} %get-tuple-element.58), channel_id=1, source_target_pairs={{6,0},{0,2},{2,4},{4,6},{7,1},{1,3},{3,5},{5,7},{14,8},{8,10},{10,... | collective-permute-start | bytes 589832 | tf_op jit(solution)/shard_map/ppermute | solution.py:45
  (23 other events, 153.7 us)

commit v3 on v1

--- a/solution.py
+++ b/solution.py
@@ -53,7 +53,7 @@
     return lax.dot_general(a, b, (((1,), (0,)), ((), ())), preferred_element_type=f32)
 
 
-def call(body, out_shape, flops, turn, *operands):
+def call(body, out_shape, flops, turn, *operands, mib=24):
     size = sum(o.size * o.dtype.itemsize for o in operands)
     specs = [pl.BlockSpec(memory_space=pltpu.SMEM)] if turn is not None else []
     whole = pl.BlockSpec(memory_space=pltpu.VMEM)
@@ -62,7 +62,7 @@
         out_shape=out_shape,
         in_specs=specs + [whole] * len(operands),
         out_specs=[whole] * len(out_shape),
-        compiler_params=pltpu.CompilerParams(vmem_limit_bytes=24 * 2**20),
+        compiler_params=pltpu.CompilerParams(vmem_limit_bytes=mib * 2**20),
         cost_estimate=pl.CostEstimate(flops=flops, bytes_accessed=size, transcendentals=0),
     )(*([turn] if turn is not None else []), *operands)
 
@@ -76,7 +76,7 @@
 
     rows = sum(block.shape[0] for block in blocks)
     shape = jax.ShapeDtypeStruct((rows, blocks[0].shape[1]), blocks[0].dtype)
-    return call(stack, [shape], 10**8, None, *blocks)[0]
+    return call(stack, [shape], 10**8, None, *blocks, mib=9)[0]
 
 
 def up_products(turn, features, weights):
@@ -149,14 +149,23 @@
     return call(down, shapes, flops, turn, *chunks, *flat, *begun)
 
 
-def group_sums(mixed, width):
+def own_sums(mixed):
     sums = jnp.stack([jnp.sum(mixed, axis=1), jnp.sum(mixed * mixed, axis=1)])
+    return sums.reshape(-1, 128)
+
+
+def scales(sums, width):
+    sums = sums.reshape(2, -1)
+    mean = sums[0] / width
+    return mean[:, None], lax.rsqrt(sums[1] / width - mean * mean + norm_eps)[:, None]
+
+
+def group_sums(mixed):
+    sums = own_sums(mixed)
     members = lax.axis_size("ra")
-    sent = jnp.broadcast_to(sums.reshape(1, -1, 128), (members, sums.size // 128, 128))
+    sent = jnp.broadcast_to(sums[None], (members, *sums.shape))
     sums = lax.all_to_all(sent, "ra", 0, 0, tiled=True)
-    sums = sums.sum(axis=0).reshape(2, -1)
-    mean = sums[0] / width
-    return mean, lax.rsqrt(sums[1] / width - mean * mean + norm_eps)
+    return sums.sum(axis=0)
 
 
 def layer(carried, branch_in, gain_in, bias_in, up_weight, down_weight, gain_out, bias_out):
@@ -178,37 +187,31 @@
     def down_for(distance):
         return lax.dynamic_slice(down_weight, (columns_for(distance), 0), (wide, held))
 
-    def gathered(own, block_for):
-        own = stacked(own, *[from_gather_ring(block_for(-j), j) for j in others])
-        near = {d: from_plane(own, d) for d in (1, 3)}
-        cut = own.shape[0] // 2
-        far = (from_plane(near[1][:cut], 1), from_plane(near[3][cut:], 3))
-        return own, near, far
-
-    up_own, up_near, up_far = gathered(up_for(0), up_for)
-    down_own, down_near, down_far = gathered(down_for(0), down_for)
+    def gathered(block_for):
+        own = block_for(0)
+        own_by_y = {d: from_plane(own, d) for d in (1, 3)}
+        blocks = [from_gather_ring(block_for(-j), j) for j in others]
+        rest = stacked(*blocks)
+        rest_by_y = {d: from_plane(rest, d) for d in (1, 3)}
+        cut = own.shape[0]
+        first = stacked(own_by_y[1], rest_by_y[1][:cut])
+        far = (from_plane(first, 1), from_plane(rest_by_y[3][cut:], 3))
+        return (own, rest), [(own_by_y[d], rest_by_y[d]) for d in (1, 3)], far
+
+    up_own, up_near, up_far = gathered(up_for)
+    down_own, down_near, down_far = gathered(down_for)
 
     def quarter(array):
         return lax.dynamic_slice(array, (y * few, 0), (few, held)).astype(f32)
 
     mixed_in = residual_scale * quarter(carried) + quarter(branch_in)
-    theirs = from_other_core(mixed_in)
-    scales = jnp.concatenate([gain_in[None], bias_in[None], jnp.zeros((6, held), f32)], axis=0)
-    sent = stacked(mixed_in, theirs, scales)
-    arrived = [sent] + [from_gather_ring(sent, j) for j in others]
-    mean, inverse = group_sums(mixed_in, width)
-    own_half = jnp.stack([mean, inverse]).reshape(-1, 128)
-    other_half = from_other_core(own_half)
-    mean, inverse = (
-        jnp.concatenate([mine.reshape(2, -1)[k] for mine in (own_half, other_half)])[:, None]
-        for k in range(2)
-    )
-
-    def normed_of(piece):
-        tokens, gain, bias = piece[: 2 * few], piece[2 * few], piece[2 * few + 1]
-        return ((tokens - mean) * inverse * gain + bias).astype(bf16)
-
-    features = [normed_of(piece) for piece in arrived]
+    sums = own_sums(mixed_in)
+    sums = sum([from_sum_ring(sums, j) for j in others], sums)
+    sums = sum([from_gather_ring(sums, j) for j in others], sums)
+    mean, inverse = scales(sums, width)
+    normed = ((mixed_in - mean) * inverse * gain_in + bias_in).astype(bf16)
+    both = stacked(normed, from_other_core(normed))
+    features = [both] + [from_gather_ring(both, j) for j in others]
 
     def activated(weights):
         parts = up_products(turn, features, weights)
@@ -218,25 +221,17 @@
         own = jnp.square(jnp.maximum(total, 0.0)).astype(bf16)
         return [own] + [from_sum_ring(own, j) for j in (1, 2, 3)]
 
-    hidden_own = activated([(up_own,)])
-    hidden_near = activated([(up_near[1],), (up_near[3],)])
+    hidden_near = activated([up_own] + up_near)
     hidden_far = activated([up_far])
-    begun = down_products(
-        turn,
-        [hidden_own, hidden_near],
-        [(down_own,), (down_near[1],), (down_near[3],)],
-        [],
-        False,
-    )
+    begun = down_products(turn, [hidden_near], [down_own] + down_near, [], False)
     parts = down_products(turn, [hidden_far], [down_far], begun, True)
     total = parts[0]
     for j, part in zip(others, parts[1:]):
         total = total + to_gather_ring(part, j).astype(f32)
     mine, theirs = total[:few], from_other_core(total[few:])
-    mixed_out = residual_scale * features[0][:few].astype(f32) + (mine + theirs)
-    mean, inverse = group_sums(mixed_out, width)
-    out = (mixed_out - mean[:, None]) * inverse[:, None] * gain_out + bias_out
-    out = out.astype(bf16)
+    mixed_out = residual_scale * normed.astype(f32) + (mine + theirs)
+    mean, inverse = scales(group_sums(mixed_out), width)
+    out = ((mixed_out - mean) * inverse * gain_out + bias_out).astype(bf16)
     result = jnp.zeros(carried.shape, bf16)
     for d in range(4):
         block = from_plane(out, d) if d else out

time: 192 us -> 175 us (0.911)
  waiting for transfers between devices: 96.5 us -> 78.5 us
  Pallas kernels: 7.54 us -> 10.6 us
  starting transfers between devices: 76.3 us -> 74.3 us
    ppermute x9, waiting for transfers between devices: 19.5 us -> 2.67 us  [from_sum_ring(): return lax.ppermute(array, ('ra', 'dp'), ring_pairs(False, distance))]
    ppermute x9 -> x6, waiting for transfers between devices: 2.54 us -> 18.1 us  [to_sum_ring(): return lax.ppermute(array, ('ra', 'dp'), ring_pairs(False, -distance))]
    ppermute x11 -> x15, waiting for transfers between devices: 36.1 us -> 23.9 us  [from_plane(): lax.ppermute(array, 'cb', [((y + distance) % 4, y) for y in range(4)])]
    ppermute x9 -> x6, starting transfers between devices: 17.5 us -> 6.59 us  [to_sum_ring(): return lax.ppermute(array, ('ra', 'dp'), ring_pairs(False, -distance))]
    ppermute x9, starting transfers between devices: 10.6 us -> 19.8 us  [from_sum_ring(): return lax.ppermute(array, ('ra', 'dp'), ring_pairs(False, distance))]
    ppermute x9 -> x12, waiting for transfers between devices: 19.9 us -> 13 us  [from_gather_ring(): return lax.ppermute(array, ('ra', 'dp'), ring_pairs(True, distance))]
    all_to_all x2 -> x1, starting transfers between devices: 13 us -> 8.16 us  [group_sums(): sums = lax.all_to_all(sent, 'ra', 0, 0, tiled=True)]
    ppermute x11 -> x15, starting transfers between devices: 17.1 us -> 21.5 us  [from_plane(): lax.ppermute(array, 'cb', [((y + distance) % 4, y) for y in range(4)])]
  transfers between devices with their start and end apart: 46 -> 48, of which waited for: 24 -> 19; matrix products, arithmetic and copies ran while one was open for 4% -> 2% of each run, Pallas kernels for 3% -> 5%
where the time goes in v3:
time: 175 us
  waiting for transfers between devices  78.5 us (45%)
  starting transfers between devices  74.3 us (42%)
  Pallas kernels  10.6 us (6%)
  local copies, waits for them, and re-layouts  7.25 us (4%)
  other arithmetic  3.51 us (2%)
    ppermute x15, waiting for transfers between devices, from_plane(): lax.ppermute(array, 'cb', [((y + distance) % 4, y) for y in range(4)])  23.9 us
    ppermute x15, starting transfers between devices, from_plane(): lax.ppermute(array, 'cb', [((y + distance) % 4, y) for y in range(4)])  21.5 us
    ppermute x9, starting transfers between devices, from_sum_ring(): return lax.ppermute(array, ('ra', 'dp'), ring_pairs(False, distance))  19.8 us
    ppermute x6, waiting for transfers between devices, to_sum_ring(): return lax.ppermute(array, ('ra', 'dp'), ring_pairs(False, -distance))  18.1 us
    ppermute x12, starting transfers between devices, from_gather_ring(): return lax.ppermute(array, ('ra', 'dp'), ring_pairs(True, distance))  14.7 us
    ppermute x12, waiting for transfers between devices, from_gather_ring(): return lax.ppermute(array, ('ra', 'dp'), ring_pairs(True, distance))  13 us
    pallas_call x9, Pallas kernels, call(): pl.pallas_call(body, out_shape=out_shape, in_specs=specs + [whole] * len(...  10.6 us
    ppermute x3, waiting for transfers between devices, to_gather_ring(): return lax.ppermute(array, ('ra', 'dp'), ring_pairs(True, -distance))  9.97 us
  transfers between devices with their start and end apart: 48, of which 19 were waited for; matrix products, arithmetic and copies ran while one was open for 2% of the time, Pallas kernels for 5%

profile of v3, /device:TPU:0, one launch (start us, length us, event | category | flops | bytes accessed | tf_op | source)
XLA Modules:
  0.0 174.5 jit_solution(16261233909191770343)
XLA Ops:
  1.3 4.1 %collective-permute-start.2 = (f32[6,128]{1,0:T(8,128)S(1)}, f32[6,128]{1,0:T(8,128)S(1)}, u32[]{:S(2)}, u32[]{:S(2)}) collective-permute-start(f32[6,128]{1,0:T(8,128)S(1)} %reshape.63), channel_id=1, source_target_pairs={{64,0},{17,1},{72,8},{25,9},{80,16},{1,17},{88,24},{9,25},{96,32},... | collective-permute-start | bytes 9224 | tf_op jit(solution)/shard_map/ppermute | solution.py:37
  10.2 3.1 %collective-permute-start.5 = (f32[6,128]{1,0:T(8,128)S(1)}, f32[6,128]{1,0:T(8,128)S(1)}, u32[]{:S(2)}, u32[]{:S(2)}) collective-permute-start(f32[6,128]{1,0:T(8,128)S(1)} %add_add_fusion.1), channel_id=1, source_target_pairs={{16,0},{65,1},{24,8},{73,9},{0,16},{81,17},{8,24},{89,25},{48,32},... | collective-permute-start | bytes 9224 | tf_op jit(solution)/shard_map/ppermute | solution.py:29
  13.9 2.6 %collective-permute-start.3 = (f32[6,128]{1,0:T(8,128)S(1)}, f32[6,128]{1,0:T(8,128)S(1)}, u32[]{:S(2)}, u32[]{:S(2)}) collective-permute-start(f32[6,128]{1,0:T(8,128)S(1)} %add_add_fusion.1), channel_id=1, source_target_pairs={{8,0},{33,1},{16,8},{41,9},{24,16},{49,17},{0,24},{57,25},{40,32},... | collective-permute-start | bytes 9224 | tf_op jit(solution)/shard_map/ppermute | solution.py:29
  23.3 5.8 %collective-permute-done.13.refs_2_ = bf16[256,512]{1,0:T(8,128)(2,1)S(1)} collective-permute-done((bf16[256,512]{1,0:T(8,128)(2,1)S(1)}, bf16[256,512]{1,0:T(8,128)(2,1)S(1)}, u32[]{:S(2)}, u32[]{:S(2)}) %collective-permute-start.13) | collective-permute-done | bytes 262176 | tf_op jit(solution)/shard_map/ppermute | solution.py:29
  29.1 2.7 %collective-permute-done.12.refs_1_ = bf16[256,512]{1,0:T(8,128)(2,1)S(1)} collective-permute-done((bf16[256,512]{1,0:T(8,128)(2,1)S(1)}, bf16[256,512]{1,0:T(8,128)(2,1)S(1)}, u32[]{:S(2)}, u32[]{:S(2)}) %collective-permute-start.12) | collective-permute-done | bytes 262176 | tf_op jit(solution)/shard_map/ppermute | solution.py:29
  32.3 2.9 %collective-permute-start.14 = (bf16[768,512]{1,0:T(8,128)(2,1)S(1)}, bf16[768,512]{1,0:T(8,128)(2,1)S(1)}, u32[]{:S(2)}, u32[]{:S(2)}) collective-permute-start(bf16[768,512]{1,0:T(8,128)(2,1)S(1)} %shard_map.83.refs_5_), channel_id=1, source_target_pairs={{2,0},{4,2},{6,4},{0,6},{3,1},{5,3},{7,5},{1,7},{10,8},{12,10},{14... | collective-permute-start | bytes 2359304 | tf_op jit(solution)/shard_map/ppermute | solution.py:45
  42.9 4.5 %collective-permute-done.9.refs_3_ = bf16[768,256]{1,0:T(8,128)(2,1)S(1)} collective-permute-done((bf16[768,256]{1,0:T(8,128)(2,1)S(1)}, bf16[768,256]{1,0:T(8,128)(2,1)S(1)}, u32[]{:S(2)}, u32[]{:S(2)}) %collective-permute-start.9) | collective-permute-done | bytes 393248 | tf_op jit(solution)/shard_map/ppermute | solution.py:29
  48.9 2.9 %collective-permute-start.25 = (bf16[512,256]{1,0:T(8,128)(2,1)}, bf16[512,256]{1,0:T(8,128)(2,1)S(1)}, u32[]{:S(2)}, u32[]{:S(2)}) collective-permute-start(bf16[512,256]{1,0:T(8,128)(2,1)} %get-tuple-element.45), channel_id=1, source_target_pairs={{8,0},{33,1},{16,8},{41,9},{24,16},{49,17},{0,24},{57,25},{40,32},... | collective-permute-start | bytes 786440 | tf_op jit(solution)/shard_map/ppermute | solution.py:29
  53.9 3.2 %collective-permute-start.15 = (bf16[512,512]{1,0:T(8,128)(2,1)S(1)}, bf16[512,512]{1,0:T(8,128)(2,1)S(1)}, u32[]{:S(2)}, u32[]{:S(2)}) collective-permute-start(bf16[512,512]{1,0:T(8,128)(2,1)S(1)} %shard_map.84), channel_id=1, source_target_pairs={{2,0},{4,2},{6,4},{0,6},{3,1},{5,3},{7,5},{1,7},{10,8},{12,10},{14... | collective-permute-start | bytes 1572872 | tf_op jit(solution)/shard_map/ppermute | solution.py:45
  57.2 3.7 %shard_map.88 = (f32[192,1536]{1,0:T(8,128)S(1)}, bf16[192,1536]{1,0:T(8,128)(2,1)S(1)}, bf16[192,1536]{1,0:T(8,128)(2,1)S(1)}, bf16[192,1536]{1,0:T(8,128)(2,1)S(1)}) custom-call(s32[1]{0:T(128)} %bitcast.2.turn_ref, bf16[768,256]{1,0:T(8,128)(2,1)S(1)} %shard_map.82.refs_0_, bf16[768,256]{1,0:T(8,128)(2,1)} %collective-permute-done.7.refs_1_, ...), custom_call_target="tpu_custom_call" | custom-call | flops 2415919104 | bytes 4718592 | tf_op jit(solution)/shard_map/pallas_call | solution.py:60
  61.0 3.0 %collective-permute-start.34 = (bf16[192,1536]{1,0:T(8,128)(2,1)S(1)}, bf16[192,1536]{1,0:T(8,128)(2,1)S(1)}, u32[]{:S(2)}, u32[]{:S(2)}) collective-permute-start(bf16[192,1536]{1,0:T(8,128)(2,1)S(1)} %get-tuple-element.27), channel_id=1, source_target_pairs={{64,0},{17,1},{72,8},{25,9},{80,16},{1,17},{88,24},{9,25},{96,32},... | collective-permute-start | bytes 1769480 | tf_op jit(solution)/shard_map/ppermute | solution.py:41
  65.3 2.7 %collective-permute-done.17.refs_5_ = bf16[512,512]{1,0:T(8,128)(2,1)S(1)} collective-permute-done((bf16[512,512]{1,0:T(8,128)(2,1)S(1)}, bf16[512,512]{1,0:T(8,128)(2,1)S(1)}, u32[]{:S(2)}, u32[]{:S(2)}) %collective-permute-start.17) | collective-permute-done | bytes 524320 | tf_op jit(solution)/shard_map/ppermute | solution.py:45
  68.0 3.2 %collective-permute-start.28 = (bf16[1536,256]{1,0:T(8,128)(2,1)S(1)}, bf16[1536,256]{1,0:T(8,128)(2,1)S(1)}, u32[]{:S(2)}, u32[]{:S(2)}) collective-permute-start(bf16[1536,256]{1,0:T(8,128)(2,1)S(1)} %shard_map.86.refs_5_), channel_id=1, source_target_pairs={{2,0},{4,2},{6,4},{0,6},{3,1},{5,3},{7,5},{1,7},{10,8},{12,10},{14... | collective-permute-start | bytes 2359304 | tf_op jit(solution)/shard_map/ppermute | solution.py:45
  73.4 5.0 %collective-permute-done.33 = bf16[192,1536]{1,0:T(8,128)(2,1)S(1)} collective-permute-done((bf16[192,1536]{1,0:T(8,128)(2,1)S(1)}, bf16[192,1536]{1,0:T(8,128)(2,1)S(1)}, u32[]{:S(2)}, u32[]{:S(2)}) %collective-permute-start.33) | collective-permute-done | bytes 589856 | tf_op jit(solution)/shard_map/ppermute | solution.py:41
  78.4 3.2 %collective-permute-start.24 = (bf16[512,256]{1,0:T(8,128)(2,1)S(1)}, bf16[512,256]{1,0:T(8,128)(2,1)S(1)}, u32[]{:S(2)}, u32[]{:S(2)}) collective-permute-start(bf16[512,256]{1,0:T(8,128)(2,1)S(1)} %get-tuple-element.46.refs_4_), channel_id=1, source_target_pairs={{2,0},{4,2},{6,4},{0,6},{3,1},{5,3},{7,5},{1,7},{10,8},{12,10},{14... | collective-permute-start | bytes 786440 | tf_op jit(solution)/shard_map/ppermute | solution.py:45
  82.0 10.6 %collective-permute-done.39.refs_8_ = bf16[512,256]{1,0:T(8,128)(2,1)S(1)} collective-permute-done((bf16[512,256]{1,0:T(8,128)(2,1)S(1)}, bf16[512,256]{1,0:T(8,128)(2,1)S(1)}, u32[]{:S(2)}, u32[]{:S(2)}) %collective-permute-start.39) | collective-permute-done | bytes 262176 | tf_op jit(solution)/shard_map/ppermute | solution.py:45
  92.5 3.6 %collective-permute-start.38 = (bf16[192,1536]{1,0:T(8,128)(2,1)S(1)}, bf16[192,1536]{1,0:T(8,128)(2,1)S(1)}, u32[]{:S(2)}, u32[]{:S(2)}) collective-permute-start(bf16[192,1536]{1,0:T(8,128)(2,1)S(1)} %multiply_convert_fusion.refs_0_), channel_id=1, source_target_pairs={{96,0},{25,1},{104,8},{1,9},{112,16},{9,17},{120,24},{17,25},{0,32... | collective-permute-start | bytes 1769480 | tf_op jit(solution)/shard_map/ppermute | solution.py:37
  102.2 11.5 %collective-permute-done.19 = bf16[192,512]{1,0:T(8,128)(2,1)S(1)} collective-permute-done((bf16[192,512]{1,0:T(8,128)(2,1)S(1)}, bf16[192,512]{1,0:T(8,128)(2,1)S(1)}, u32[]{:S(2)}, u32[]{:S(2)}) %collective-permute-start.19) | collective-permute-done | bytes 196640 | tf_op jit(solution)/shard_map/ppermute | solution.py:41
  115.2 3.0 %collective-permute-start.29 = (bf16[1024,256]{1,0:T(8,128)(2,1)S(1)}, bf16[1024,256]{1,0:T(8,128)(2,1)S(1)}, u32[]{:S(2)}, u32[]{:S(2)}) collective-permute-start(bf16[1024,256]{1,0:T(8,128)(2,1)S(1)} %shard_map.87), channel_id=1, source_target_pairs={{2,0},{4,2},{6,4},{0,6},{3,1},{5,3},{7,5},{1,7},{10,8},{12,10},{14... | collective-permute-start | bytes 1572872 | tf_op jit(solution)/shard_map/ppermute | solution.py:45
  129.3 3.2 %collective-permute-start.41 = (bf16[768,256]{1,0:T(8,128)(2,1)S(1)}, bf16[768,256]{1,0:T(8,128)(2,1)S(1)}, u32[]{:S(2)}, u32[]{:S(2)}) collective-permute-start(bf16[768,256]{1,0:T(8,128)(2,1)S(1)} %get-tuple-element.35), channel_id=1, source_target_pairs={{8,0},{33,1},{16,8},{41,9},{24,16},{49,17},{0,24},{57,25},{40,32},... | collective-permute-start | bytes 1179656 | tf_op jit(solution)/shard_map/ppermute | solution.py:33
  132.6 10.0 %collective-permute-done.40 = bf16[768,256]{1,0:T(8,128)(2,1)S(1)} collective-permute-done((bf16[768,256]{1,0:T(8,128)(2,1)S(1)}, bf16[768,256]{1,0:T(8,128)(2,1)S(1)}, u32[]{:S(2)}, u32[]{:S(2)}) %collective-permute-start.40) | collective-permute-done | bytes 393248 | tf_op jit(solution)/shard_map/ppermute | solution.py:33
  145.5 8.2 %all-to-all-start = ((f32[16,6,128]{2,1,0:T(8,128)}), f32[16,6,128]{2,1,0:T(8,128)S(1)}, u32[]{:S(2)}, u32[]{:S(2)}) async-start(f32[16,6,128]{2,1,0:T(8,128)} %broadcast_in_dim.8), calls=%async_computation | async-start | bytes 131072 | tf_op jit(solution)/shard_map/all_to_all | solution.py:167
  153.7 7.6 %all-to-all-done = f32[16,6,128]{2,1,0:T(8,128)S(1)} async-done(((f32[16,6,128]{2,1,0:T(8,128)}), f32[16,6,128]{2,1,0:T(8,128)S(1)}, u32[]{:S(2)}, u32[]{:S(2)}) %all-to-all-start) | async-done | bytes 49184 | tf_op jit(solution)/shard_map/all_to_all | solution.py:167
  163.8 5.5 %collective-permute-done.44 = bf16[384,256]{1,0:T(8,128)(2,1)S(1)} collective-permute-done((bf16[384,256]{1,0:T(8,128)(2,1)S(1)}, bf16[384,256]{1,0:T(8,128)(2,1)S(1)}, u32[]{:S(2)}, u32[]{:S(2)}) %collective-permute-start.44) | collective-permute-done | bytes 196640 | tf_op jit(solution)/shard_map/ppermute | solution.py:45
  (139 shorter events, 58.3 us)
Async XLA Ops:
  17.8 20.2 %collective-permute-start.32 = (bf16[256,512]{1,0:T(8,128)(2,1)S(1)}, bf16[256,512]{1,0:T(8,128)(2,1)S(1)}, u32[]{:S(2)}, u32[]{:S(2)}) collective-permute-start(bf16[256,512]{1,0:T(8,128)(2,1)S(1)} %get-tuple-element.50.refs_4_), channel_id=1, source_target_pairs={{6,0},{0,2},{2,4},{4,6},{7,1},{1,3},{3,5},{5,7},{14,8},{8,10},{10,... | collective-permute-start | bytes 786440 | tf_op jit(solution)/shard_map/ppermute | solution.py:45
  19.5 20.7 %collective-permute-start.10 = (bf16[256,512]{1,0:T(8,128)(2,1)S(1)}, bf16[256,512]{1,0:T(8,128)(2,1)S(1)}, u32[]{:S(2)}, u32[]{:S(2)}) collective-permute-start(bf16[256,512]{1,0:T(8,128)(2,1)S(1)} %get-tuple-element.50.refs_4_), channel_id=1, source_target_pairs={{2,0},{4,2},{6,4},{0,6},{3,1},{5,3},{7,5},{1,7},{10,8},{12,10},{14... | collective-permute-start | bytes 786440 | tf_op jit(solution)/shard_map/ppermute | solution.py:45
  31.9 17.0 %collective-permute-start.16 = (bf16[768,512]{1,0:T(8,128)(2,1)S(1)}, bf16[768,512]{1,0:T(8,128)(2,1)S(1)}, u32[]{:S(2)}, u32[]{:S(2)}) collective-permute-start(bf16[768,512]{1,0:T(8,128)(2,1)S(1)} %shard_map.83.refs_5_), channel_id=1, source_target_pairs={{6,0},{0,2},{2,4},{4,6},{7,1},{1,3},{3,5},{5,7},{14,8},{8,10},{10,... | collective-permute-start | bytes 2359304 | tf_op jit(solution)/shard_map/ppermute | solution.py:45
  32.3 19.5 %collective-permute-start.14 = (bf16[768,512]{1,0:T(8,128)(2,1)S(1)}, bf16[768,512]{1,0:T(8,128)(2,1)S(1)}, u32[]{:S(2)}, u32[]{:S(2)}) collective-permute-start(bf16[768,512]{1,0:T(8,128)(2,1)S(1)} %shard_map.83.refs_5_), channel_id=1, source_target_pairs={{2,0},{4,2},{6,4},{0,6},{3,1},{5,3},{7,5},{1,7},{10,8},{12,10},{14... | collective-permute-start | bytes 2359304 | tf_op jit(solution)/shard_map/ppermute | solution.py:45
  38.8 15.1 %collective-permute-start.8 = (bf16[768,256]{1,0:T(8,128)(2,1)S(1)}, bf16[768,256]{1,0:T(8,128)(2,1)}, u32[]{:S(2)}, u32[]{:S(2)}) collective-permute-start(bf16[768,256]{1,0:T(8,128)(2,1)S(1)} %shard_map.82.refs_0_), channel_id=1, source_target_pairs={{24,0},{97,1},{0,8},{105,9},{8,16},{113,17},{16,24},{121,25},{56,3... | collective-permute-start | bytes 1179656 | tf_op jit(solution)/shard_map/ppermute | solution.py:29
  40.2 13.8 %collective-permute-start.7 = (bf16[768,256]{1,0:T(8,128)(2,1)S(1)}, bf16[768,256]{1,0:T(8,128)(2,1)}, u32[]{:S(2)}, u32[]{:S(2)}) collective-permute-start(bf16[768,256]{1,0:T(8,128)(2,1)S(1)} %shard_map.82.refs_0_), channel_id=1, source_target_pairs={{8,0},{33,1},{16,8},{41,9},{24,16},{49,17},{0,24},{57,25},{40,32},... | collective-permute-start | bytes 1179656 | tf_op jit(solution)/shard_map/ppermute | solution.py:29
  53.9 14.2 %collective-permute-start.17 = (bf16[512,512]{1,0:T(8,128)(2,1)S(1)}, bf16[512,512]{1,0:T(8,128)(2,1)S(1)}, u32[]{:S(2)}, u32[]{:S(2)}) collective-permute-start(bf16[512,512]{1,0:T(8,128)(2,1)S(1)} %slice.45), channel_id=1, source_target_pairs={{6,0},{0,2},{2,4},{4,6},{7,1},{1,3},{3,5},{5,7},{14,8},{8,10},{10,... | collective-permute-start | bytes 1572872 | tf_op jit(solution)/shard_map/ppermute | solution.py:45
  53.9 14.1 %collective-permute-start.15 = (bf16[512,512]{1,0:T(8,128)(2,1)S(1)}, bf16[512,512]{1,0:T(8,128)(2,1)S(1)}, u32[]{:S(2)}, u32[]{:S(2)}) collective-permute-start(bf16[512,512]{1,0:T(8,128)(2,1)S(1)} %shard_map.84), channel_id=1, source_target_pairs={{2,0},{4,2},{6,4},{0,6},{3,1},{5,3},{7,5},{1,7},{10,8},{12,10},{14... | collective-permute-start | bytes 1572872 | tf_op jit(solution)/shard_map/ppermute | solution.py:45
  60.9 17.5 %collective-permute-start.33 = (bf16[192,1536]{1,0:T(8,128)(2,1)S(1)}, bf16[192,1536]{1,0:T(8,128)(2,1)S(1)}, u32[]{:S(2)}, u32[]{:S(2)}) collective-permute-start(bf16[192,1536]{1,0:T(8,128)(2,1)S(1)} %get-tuple-element.26), channel_id=1, source_target_pairs={{96,0},{25,1},{104,8},{1,9},{112,16},{9,17},{120,24},{17,25},{0,32... | collective-permute-start | bytes 1769480 | tf_op jit(solution)/shard_map/ppermute | solution.py:41
  61.0 17.4 %collective-permute-start.34 = (bf16[192,1536]{1,0:T(8,128)(2,1)S(1)}, bf16[192,1536]{1,0:T(8,128)(2,1)S(1)}, u32[]{:S(2)}, u32[]{:S(2)}) collective-permute-start(bf16[192,1536]{1,0:T(8,128)(2,1)S(1)} %get-tuple-element.27), channel_id=1, source_target_pairs={{64,0},{17,1},{72,8},{25,9},{80,16},{1,17},{88,24},{9,25},{96,32},... | collective-permute-start | bytes 1769480 | tf_op jit(solution)/shard_map/ppermute | solution.py:41
  64.1 17.6 %collective-permute-start.35 = (bf16[192,1536]{1,0:T(8,128)(2,1)S(1)}, bf16[192,1536]{1,0:T(8,128)(2,1)S(1)}, u32[]{:S(2)}, u32[]{:S(2)}) collective-permute-start(bf16[192,1536]{1,0:T(8,128)(2,1)S(1)} %get-tuple-element.28), channel_id=1, source_target_pairs={{32,0},{9,1},{40,8},{17,9},{48,16},{25,17},{56,24},{1,25},{64,32},... | collective-permute-start | bytes 1769480 | tf_op jit(solution)/shard_map/ppermute | solution.py:41
  68.0 29.3 %collective-permute-start.30 = (bf16[1536,256]{1,0:T(8,128)(2,1)S(1)}, bf16[1536,256]{1,0:T(8,128)(2,1)S(1)}, u32[]{:S(2)}, u32[]{:S(2)}) collective-permute-start(bf16[1536,256]{1,0:T(8,128)(2,1)S(1)} %shard_map.86.refs_5_), channel_id=1, source_target_pairs={{6,0},{0,2},{2,4},{4,6},{7,1},{1,3},{3,5},{5,7},{14,8},{8,10},{10,... | collective-permute-start | bytes 2359304 | tf_op jit(solution)/shard_map/ppermute | solution.py:45
  68.0 30.8 %collective-permute-start.28 = (bf16[1536,256]{1,0:T(8,128)(2,1)S(1)}, bf16[1536,256]{1,0:T(8,128)(2,1)S(1)}, u32[]{:S(2)}, u32[]{:S(2)}) collective-permute-start(bf16[1536,256]{1,0:T(8,128)(2,1)S(1)} %shard_map.86.refs_5_), channel_id=1, source_target_pairs={{2,0},{4,2},{6,4},{0,6},{3,1},{5,3},{7,5},{1,7},{10,8},{12,10},{14... | collective-permute-start | bytes 2359304 | tf_op jit(solution)/shard_map/ppermute | solution.py:45
  78.4 14.1 %collective-permute-start.39 = (bf16[512,256]{1,0:T(8,128)(2,1)S(1)}, bf16[512,256]{1,0:T(8,128)(2,1)S(1)}, u32[]{:S(2)}, u32[]{:S(2)}) collective-permute-start(bf16[512,256]{1,0:T(8,128)(2,1)S(1)} %get-tuple-element.46.refs_4_), channel_id=1, source_target_pairs={{6,0},{0,2},{2,4},{4,6},{7,1},{1,3},{3,5},{5,7},{14,8},{8,10},{10,... | collective-permute-start | bytes 786440 | tf_op jit(solution)/shard_map/ppermute | solution.py:45
  78.4 17.7 %collective-permute-start.24 = (bf16[512,256]{1,0:T(8,128)(2,1)S(1)}, bf16[512,256]{1,0:T(8,128)(2,1)S(1)}, u32[]{:S(2)}, u32[]{:S(2)}) collective-permute-start(bf16[512,256]{1,0:T(8,128)(2,1)S(1)} %get-tuple-element.46.refs_4_), channel_id=1, source_target_pairs={{2,0},{4,2},{6,4},{0,6},{3,1},{5,3},{7,5},{1,7},{10,8},{12,10},{14... | collective-permute-start | bytes 786440 | tf_op jit(solution)/shard_map/ppermute | solution.py:45
  81.6 18.1 %collective-permute-start.18 = (bf16[192,512]{1,0:T(8,128)(2,1)S(1)}, bf16[192,512]{1,0:T(8,128)(2,1)S(1)}, u32[]{:S(2)}, u32[]{:S(2)}) collective-permute-start(bf16[192,512]{1,0:T(8,128)(2,1)S(1)} %get-tuple-element.22), channel_id=1, source_target_pairs={{96,0},{25,1},{104,8},{1,9},{112,16},{9,17},{120,24},{17,25},{0,32... | collective-permute-start | bytes 589832 | tf_op jit(solution)/shard_map/ppermute | solution.py:41
  92.5 25.8 %collective-permute-start.38 = (bf16[192,1536]{1,0:T(8,128)(2,1)S(1)}, bf16[192,1536]{1,0:T(8,128)(2,1)S(1)}, u32[]{:S(2)}, u32[]{:S(2)}) collective-permute-start(bf16[192,1536]{1,0:T(8,128)(2,1)S(1)} %multiply_convert_fusion.refs_0_), channel_id=1, source_target_pairs={{96,0},{25,1},{104,8},{1,9},{112,16},{9,17},{120,24},{17,25},{0,32... | collective-permute-start | bytes 1769480 | tf_op jit(solution)/shard_map/ppermute | solution.py:37
  96.1 24.2 %collective-permute-start.37 = (bf16[192,1536]{1,0:T(8,128)(2,1)S(1)}, bf16[192,1536]{1,0:T(8,128)(2,1)S(1)}, u32[]{:S(2)}, u32[]{:S(2)}) collective-permute-start(bf16[192,1536]{1,0:T(8,128)(2,1)S(1)} %multiply_convert_fusion.refs_0_), channel_id=1, source_target_pairs={{64,0},{17,1},{72,8},{25,9},{80,16},{1,17},{88,24},{9,25},{96,32},... | collective-permute-start | bytes 1769480 | tf_op jit(solution)/shard_map/ppermute | solution.py:37
  97.4 25.1 %collective-permute-start.36 = (bf16[192,1536]{1,0:T(8,128)(2,1)S(1)}, bf16[192,1536]{1,0:T(8,128)(2,1)S(1)}, u32[]{:S(2)}, u32[]{:S(2)}) collective-permute-start(bf16[192,1536]{1,0:T(8,128)(2,1)S(1)} %multiply_convert_fusion.refs_0_), channel_id=1, source_target_pairs={{32,0},{9,1},{40,8},{17,9},{48,16},{25,17},{56,24},{1,25},{64,32},... | collective-permute-start | bytes 1769480 | tf_op jit(solution)/shard_map/ppermute | solution.py:37
  98.8 14.8 %collective-permute-start.19 = (bf16[192,512]{1,0:T(8,128)(2,1)S(1)}, bf16[192,512]{1,0:T(8,128)(2,1)S(1)}, u32[]{:S(2)}, u32[]{:S(2)}) collective-permute-start(bf16[192,512]{1,0:T(8,128)(2,1)S(1)} %get-tuple-element.23), channel_id=1, source_target_pairs={{64,0},{17,1},{72,8},{25,9},{80,16},{1,17},{88,24},{9,25},{96,32},... | collective-permute-start | bytes 589832 | tf_op jit(solution)/shard_map/ppermute | solution.py:41
  99.7 15.5 %collective-permute-start.20 = (bf16[192,512]{1,0:T(8,128)(2,1)S(1)}, bf16[192,512]{1,0:T(8,128)(2,1)S(1)}, u32[]{:S(2)}, u32[]{:S(2)}) collective-permute-start(bf16[192,512]{1,0:T(8,128)(2,1)S(1)} %get-tuple-element.24), channel_id=1, source_target_pairs={{32,0},{9,1},{40,8},{17,9},{48,16},{25,17},{56,24},{1,25},{64,32},... | collective-permute-start | bytes 589832 | tf_op jit(solution)/shard_map/ppermute | solution.py:41
  113.6 13.5 %collective-permute-start.31 = (bf16[1024,256]{1,0:T(8,128)(2,1)S(1)}, bf16[1024,256]{1,0:T(8,128)(2,1)S(1)}, u32[]{:S(2)}, u32[]{:S(2)}) collective-permute-start(bf16[1024,256]{1,0:T(8,128)(2,1)S(1)} %slice.47), channel_id=1, source_target_pairs={{6,0},{0,2},{2,4},{4,6},{7,1},{1,3},{3,5},{5,7},{14,8},{8,10},{10,... | collective-permute-start | bytes 1572872 | tf_op jit(solution)/shard_map/ppermute | solution.py:45
  129.2 13.3 %collective-permute-start.40 = (bf16[768,256]{1,0:T(8,128)(2,1)S(1)}, bf16[768,256]{1,0:T(8,128)(2,1)S(1)}, u32[]{:S(2)}, u32[]{:S(2)}) collective-permute-start(bf16[768,256]{1,0:T(8,128)(2,1)S(1)} %get-tuple-element.34), channel_id=1, source_target_pairs={{24,0},{97,1},{0,8},{105,9},{8,16},{113,17},{16,24},{121,25},{56,3... | collective-permute-start | bytes 1179656 | tf_op jit(solution)/shard_map/ppermute | solution.py:33
  145.5 15.8 %all-to-all-start = ((f32[16,6,128]{2,1,0:T(8,128)}), f32[16,6,128]{2,1,0:T(8,128)S(1)}, u32[]{:S(2)}, u32[]{:S(2)}) async-start(f32[16,6,128]{2,1,0:T(8,128)} %broadcast_in_dim.8), calls=%async_computation | async-start | bytes 131072 | tf_op jit(solution)/shard_map/all_to_all | solution.py:167
  (36 other events, 308.2 us)

commit v4 on v3

--- a/solution.py
+++ b/solution.py
@@ -80,33 +80,40 @@
 
 
 def up_products(turn, features, weights):
-    rows = features[0].shape[0] // 4
+    rows = features.shape[0] // 4
     flat = [w for ws in weights for w in ws]
     wide = flat[0].shape[1]
 
-    def up(turn_ref, *refs):
-        pieces, refs = refs[: len(features)], refs[len(features) :]
+    def up(turn_ref, a_ref, *refs):
         w_refs, outs = refs[: len(flat)], refs[len(flat) :]
         for i, out in enumerate(outs):
             start = pl.multiple_of((turn_ref[0] + i) % 4 * rows, rows)
-            blocks = [piece[pl.ds(start, rows), :] for piece in pieces]
             at = 0
             for n, ws in enumerate(weights):
-                total, left = None, list(blocks)
+                total, done = None, 0
                 for w_ref in w_refs[at : at + len(ws)]:
-                    done = 0
-                    while done < w_ref.shape[0]:
-                        block = left.pop(0)
-                        term = dot(block, w_ref[done : done + block.shape[1], :])
-                        total = term if total is None else total + term
-                        done += block.shape[1]
+                    k = w_ref.shape[0]
+                    term = dot(a_ref[pl.ds(start, rows), done : done + k], w_ref[...])
+                    total = term if total is None else total + term
+                    done += k
                 at += len(ws)
                 out[:, n * wide : (n + 1) * wide] = total.astype(out.dtype)
 
     full = wide * len(weights)
     shapes = [jax.ShapeDtypeStruct((rows, full), bf16 if i else f32) for i in range(4)]
-    flops = 2 * 4 * rows * full * sum(p.shape[1] for p in features)
-    return call(up, shapes, flops, turn, *features, *flat)
+    return call(up, shapes, 2 * features.size * full, turn, features, *flat)
+
+
+def placed(y, blocks):
+    rows = blocks[0].shape[0]
+
+    def place(y_ref, *refs):
+        for d, ref in enumerate(refs[:-1]):
+            start = pl.multiple_of((y_ref[0] + d) % 4 * rows, rows)
+            refs[-1][pl.ds(start, rows), :] = ref[...]
+
+    shape = jax.ShapeDtypeStruct((4 * rows, blocks[0].shape[1]), blocks[0].dtype)
+    return call(place, [shape], 10**8, y.reshape(1).astype(jnp.int32), *blocks, mib=6)[0]
 
 
 def down_products(turn, hidden, weights, begun, last):
@@ -174,6 +181,7 @@
     z, x = r // 4, r % 4
     a, b = jnp.where(c == 0, x, z), jnp.where(c == 0, z, x)
     turn = ((b - 2 * c) % 4).reshape(1).astype(jnp.int32)
+    carried, turn = lax.optimization_barrier((carried, turn))
     held = carried.shape[1]
     few = carried.shape[0] // 4
     wide = up_weight.shape[1] // 8
@@ -207,11 +215,13 @@
     mixed_in = residual_scale * quarter(carried) + quarter(branch_in)
     sums = own_sums(mixed_in)
     sums = sum([from_sum_ring(sums, j) for j in others], sums)
-    sums = sum([from_gather_ring(sums, j) for j in others], sums)
+    arrived = [from_gather_ring(sums, j) for j in others]
+    sums = sum(arrived, sums)
     mean, inverse = scales(sums, width)
     normed = ((mixed_in - mean) * inverse * gain_in + bias_in).astype(bf16)
     both = stacked(normed, from_other_core(normed))
     features = [both] + [from_gather_ring(both, j) for j in others]
+    features = jnp.concatenate(features, axis=1)
 
     def activated(weights):
         parts = up_products(turn, features, weights)
@@ -232,11 +242,7 @@
     mixed_out = residual_scale * normed.astype(f32) + (mine + theirs)
     mean, inverse = scales(group_sums(mixed_out), width)
     out = ((mixed_out - mean) * inverse * gain_out + bias_out).astype(bf16)
-    result = jnp.zeros(carried.shape, bf16)
-    for d in range(4):
-        block = from_plane(out, d) if d else out
-        result = lax.dynamic_update_slice(result, block, ((y + d) % 4 * few, 0))
-    return result
+    return placed(y, [out] + [from_plane(out, d) for d in (1, 2, 3)])
 
 
 def solution(mesh):

time: 175 us -> 173 us (0.989)
  starting transfers between devices: 74.3 us -> 59 us
  blocking collectives: 0 us -> 12.9 us
  waiting for transfers between devices: 78.5 us -> 86.6 us
  local copies, waits for them, and re-layouts: 7.25 us -> 1.54 us
  Pallas kernels: 10.6 us -> 8.34 us
    all_to_all x0 -> x1, blocking collectives: none -> 12.9 us  [group_sums(): sums = lax.all_to_all(sent, 'ra', 0, 0, tiled=True)]
    all_to_all x1 -> x0, starting transfers between devices: 8.16 us -> none  [group_sums(): sums = lax.all_to_all(sent, 'ra', 0, 0, tiled=True)]
    all_to_all x1 -> x0, waiting for transfers between devices: 7.65 us -> none  [group_sums(): sums = lax.all_to_all(sent, 'ra', 0, 0, tiled=True)]
    ppermute x12, waiting for transfers between devices: 13 us -> 18.1 us  [from_gather_ring(): return lax.ppermute(array, ('ra', 'dp'), ring_pairs(True, distance))]
    ppermute x15, starting transfers between devices: 21.5 us -> 17.4 us  [from_plane(): lax.ppermute(array, 'cb', [((y + distance) % 4, y) for y in range(4)])]
    ppermute x15, waiting for transfers between devices: 23.9 us -> 28 us  [from_plane(): lax.ppermute(array, 'cb', [((y + distance) % 4, y) for y in range(4)])]
    unnamed x24 -> x10, local copies, waits for them, and re-layouts: 3.49 us -> 0.03 us
    ppermute x6, waiting for transfers between devices: 18.1 us -> 21.4 us  [to_sum_ring(): return lax.ppermute(array, ('ra', 'dp'), ring_pairs(False, -distance))]
  transfers between devices with their start and end apart: 48 -> 47, of which waited for: 19 -> 18; matrix products, arithmetic and copies ran while one was open for 2% -> 2% of each run, Pallas kernels for 5% -> 4%
where the time goes in v4:
time: 173 us; the launch traced here: 172 us
  waiting for transfers between devices  86.6 us (50%)
  starting transfers between devices  59 us (34%)
  blocking collectives  12.9 us (7%)
  Pallas kernels  8.34 us (5%)
  other arithmetic  3.69 us (2%)
    ppermute x15, waiting for transfers between devices, from_plane(): lax.ppermute(array, 'cb', [((y + distance) % 4, y) for y in range(4)])  28 us
    ppermute x6, waiting for transfers between devices, to_sum_ring(): return lax.ppermute(array, ('ra', 'dp'), ring_pairs(False, -distance))  21.4 us
    ppermute x12, waiting for transfers between devices, from_gather_ring(): return lax.ppermute(array, ('ra', 'dp'), ring_pairs(True, distance))  18.1 us
    ppermute x15, starting transfers between devices, from_plane(): lax.ppermute(array, 'cb', [((y + distance) % 4, y) for y in range(4)])  17.4 us
    ppermute x9, starting transfers between devices, from_sum_ring(): return lax.ppermute(array, ('ra', 'dp'), ring_pairs(False, distance))  16.9 us
    ppermute x12, starting transfers between devices, from_gather_ring(): return lax.ppermute(array, ('ra', 'dp'), ring_pairs(True, distance))  14.3 us
    all_to_all x1, blocking collectives, group_sums(): sums = lax.all_to_all(sent, 'ra', 0, 0, tiled=True)  12.9 us
    ppermute x3, waiting for transfers between devices, to_gather_ring(): return lax.ppermute(array, ('ra', 'dp'), ring_pairs(True, -distance))  9.97 us
  transfers between devices with their start and end apart: 47, of which 18 were waited for; matrix products, arithmetic and copies ran while one was open for 2% of the time, Pallas kernels for 4%

profile of v4, /device:TPU:0, one launch (start us, length us, event | category | flops | bytes accessed | tf_op | source)
XLA Modules:
  0.0 172.5 jit_solution(13473088001169634524)
XLA Ops:
  1.3 4.1 %collective-permute-start.2 = (f32[6,128]{1,0:T(8,128)S(1)}, f32[6,128]{1,0:T(8,128)S(1)}, u32[]{:S(2)}, u32[]{:S(2)}) collective-permute-start(f32[6,128]{1,0:T(8,128)S(1)} %reshape.68), channel_id=1, source_target_pairs={{64,0},{17,1},{72,8},{25,9},{80,16},{1,17},{88,24},{9,25},{96,32},... | collective-permute-start | bytes 9224 | tf_op jit(solution)/shard_map/ppermute | solution.py:37
  10.2 3.1 %collective-permute-start.5 = (f32[6,128]{1,0:T(8,128)S(1)}, f32[6,128]{1,0:T(8,128)S(1)}, u32[]{:S(2)}, u32[]{:S(2)}) collective-permute-start(f32[6,128]{1,0:T(8,128)S(1)} %add_add_fusion.1), channel_id=1, source_target_pairs={{16,0},{65,1},{24,8},{73,9},{0,16},{81,17},{8,24},{89,25},{48,32},... | collective-permute-start | bytes 9224 | tf_op jit(solution)/shard_map/ppermute | solution.py:29
  13.9 2.6 %collective-permute-start.3 = (f32[6,128]{1,0:T(8,128)S(1)}, f32[6,128]{1,0:T(8,128)S(1)}, u32[]{:S(2)}, u32[]{:S(2)}) collective-permute-start(f32[6,128]{1,0:T(8,128)S(1)} %add_add_fusion.1), channel_id=1, source_target_pairs={{8,0},{33,1},{16,8},{41,9},{24,16},{49,17},{0,24},{57,25},{40,32},... | collective-permute-start | bytes 9224 | tf_op jit(solution)/shard_map/ppermute | solution.py:29
  20.0 5.8 %collective-permute-done.13.refs_2_ = bf16[256,512]{1,0:T(8,128)(2,1)S(1)} collective-permute-done((bf16[256,512]{1,0:T(8,128)(2,1)S(1)}, bf16[256,512]{1,0:T(8,128)(2,1)S(1)}, u32[]{:S(2)}, u32[]{:S(2)}) %collective-permute-start.13) | collective-permute-done | bytes 262176 | tf_op jit(solution)/shard_map/ppermute | solution.py:29
  25.9 2.7 %collective-permute-done.12.refs_1_ = bf16[256,512]{1,0:T(8,128)(2,1)S(1)} collective-permute-done((bf16[256,512]{1,0:T(8,128)(2,1)S(1)}, bf16[256,512]{1,0:T(8,128)(2,1)S(1)}, u32[]{:S(2)}, u32[]{:S(2)}) %collective-permute-start.12) | collective-permute-done | bytes 262176 | tf_op jit(solution)/shard_map/ppermute | solution.py:29
  38.1 6.1 %collective-permute-done.9 = bf16[768,256]{1,0:T(8,128)(2,1)S(1)} collective-permute-done((bf16[768,256]{1,0:T(8,128)(2,1)S(1)}, bf16[768,256]{1,0:T(8,128)(2,1)S(1)}, u32[]{:S(2)}, u32[]{:S(2)}) %collective-permute-start.9) | collective-permute-done | bytes 393248 | tf_op jit(solution)/shard_map/ppermute | solution.py:29
  44.5 3.5 %collective-permute-done.8 = bf16[768,256]{1,0:T(8,128)(2,1)S(1)} collective-permute-done((bf16[768,256]{1,0:T(8,128)(2,1)S(1)}, bf16[768,256]{1,0:T(8,128)(2,1)S(1)}, u32[]{:S(2)}, u32[]{:S(2)}) %collective-permute-start.8) | collective-permute-done | bytes 393248 | tf_op jit(solution)/shard_map/ppermute | solution.py:29
  52.6 3.2 %collective-permute-done.10.refs_0_.refs_2_ = bf16[256,512]{1,0:T(8,128)(2,1)S(1)} collective-permute-done((bf16[256,512]{1,0:T(8,128)(2,1)S(1)}, bf16[256,512]{1,0:T(8,128)(2,1)S(1)}, u32[]{:S(2)}, u32[]{:S(2)}) %collective-permute-start.10) | collective-permute-done | bytes 262176 | tf_op jit(solution)/shard_map/ppermute | solution.py:45
  56.2 2.9 %collective-permute-start.15 = (bf16[512,512]{1,0:T(8,128)(2,1)S(1)}, bf16[512,512]{1,0:T(8,128)(2,1)S(1)}, u32[]{:S(2)}, u32[]{:S(2)}) collective-permute-start(bf16[512,512]{1,0:T(8,128)(2,1)S(1)} %shard_map.84), channel_id=1, source_target_pairs={{2,0},{4,2},{6,4},{0,6},{3,1},{5,3},{7,5},{1,7},{10,8},{12,10},{14... | collective-permute-start | bytes 1572872 | tf_op jit(solution)/shard_map/ppermute | solution.py:45
  59.1 2.6 %shard_map.88 = (f32[192,1536]{1,0:T(8,128)S(1)}, bf16[192,1536]{1,0:T(8,128)(2,1)S(1)}, bf16[192,1536]{1,0:T(8,128)(2,1)S(1)}, bf16[192,1536]{1,0:T(8,128)(2,1)S(1)}) custom-call(s32[1]{0:T(128)} %bitcast.1.turn_ref, bf16[768,1024]{1,0:T(8,128)(2,1)S(1)} %pad_maximum_fusion.a_ref, bf16[256,512]{1,0:T(8,128)(2,1)S(1)} %get-tuple-element.52.refs_0_, ...), custom_call_target="tpu_custom_call" | custom-call | flops 2415919104 | bytes 4718592 | tf_op jit(solution)/shard_map/pallas_call | solution.py:60
  61.9 3.6 %collective-permute-start.34 = (bf16[192,1536]{1,0:T(8,128)(2,1)S(1)}, bf16[192,1536]{1,0:T(8,128)(2,1)S(1)}, u32[]{:S(2)}, u32[]{:S(2)}) collective-permute-start(bf16[192,1536]{1,0:T(8,128)(2,1)S(1)} %get-tuple-element.31), channel_id=1, source_target_pairs={{64,0},{17,1},{72,8},{25,9},{80,16},{1,17},{88,24},{9,25},{96,32},... | collective-permute-start | bytes 1769480 | tf_op jit(solution)/shard_map/ppermute | solution.py:41
  66.0 3.5 %collective-permute-done.17.refs_1_ = bf16[512,512]{1,0:T(8,128)(2,1)S(1)} collective-permute-done((bf16[512,512]{1,0:T(8,128)(2,1)S(1)}, bf16[512,512]{1,0:T(8,128)(2,1)S(1)}, u32[]{:S(2)}, u32[]{:S(2)}) %collective-permute-start.17) | collective-permute-done | bytes 524320 | tf_op jit(solution)/shard_map/ppermute | solution.py:45
  69.5 3.2 %collective-permute-start.28 = (bf16[1536,256]{1,0:T(8,128)(2,1)S(1)}, bf16[1536,256]{1,0:T(8,128)(2,1)S(1)}, u32[]{:S(2)}, u32[]{:S(2)}) collective-permute-start(bf16[1536,256]{1,0:T(8,128)(2,1)S(1)} %shard_map.86.refs_5_), channel_id=1, source_target_pairs={{2,0},{4,2},{6,4},{0,6},{3,1},{5,3},{7,5},{1,7},{10,8},{12,10},{14... | collective-permute-start | bytes 2359304 | tf_op jit(solution)/shard_map/ppermute | solution.py:45
  73.8 5.8 %collective-permute-done.34 = bf16[192,1536]{1,0:T(8,128)(2,1)S(1)} collective-permute-done((bf16[192,1536]{1,0:T(8,128)(2,1)S(1)}, bf16[192,1536]{1,0:T(8,128)(2,1)S(1)}, u32[]{:S(2)}, u32[]{:S(2)}) %collective-permute-start.34) | collective-permute-done | bytes 589856 | tf_op jit(solution)/shard_map/ppermute | solution.py:41
  81.5 12.1 %collective-permute-done.39.refs_8_ = bf16[512,256]{1,0:T(8,128)(2,1)S(1)} collective-permute-done((bf16[512,256]{1,0:T(8,128)(2,1)S(1)}, bf16[512,256]{1,0:T(8,128)(2,1)S(1)}, u32[]{:S(2)}, u32[]{:S(2)}) %collective-permute-start.39) | collective-permute-done | bytes 262176 | tf_op jit(solution)/shard_map/ppermute | solution.py:45
  95.1 2.6 %collective-permute-start.36 = (bf16[192,1536]{1,0:T(8,128)(2,1)S(1)}, bf16[192,1536]{1,0:T(8,128)(2,1)S(1)}, u32[]{:S(2)}, u32[]{:S(2)}) collective-permute-start(bf16[192,1536]{1,0:T(8,128)(2,1)S(1)} %multiply_convert_fusion.refs_0_), channel_id=1, source_target_pairs={{32,0},{9,1},{40,8},{17,9},{48,16},{25,17},{56,24},{1,25},{64,32},... | collective-permute-start | bytes 1769480 | tf_op jit(solution)/shard_map/ppermute | solution.py:37
  100.6 10.9 %collective-permute-done.19 = bf16[192,512]{1,0:T(8,128)(2,1)S(1)} collective-permute-done((bf16[192,512]{1,0:T(8,128)(2,1)S(1)}, bf16[192,512]{1,0:T(8,128)(2,1)S(1)}, u32[]{:S(2)}, u32[]{:S(2)}) %collective-permute-start.19) | collective-permute-done | bytes 196640 | tf_op jit(solution)/shard_map/ppermute | solution.py:41
  111.5 4.7 %collective-permute-done.20 = bf16[192,512]{1,0:T(8,128)(2,1)S(1)} collective-permute-done((bf16[192,512]{1,0:T(8,128)(2,1)S(1)}, bf16[192,512]{1,0:T(8,128)(2,1)S(1)}, u32[]{:S(2)}, u32[]{:S(2)}) %collective-permute-start.20) | collective-permute-done | bytes 196640 | tf_op jit(solution)/shard_map/ppermute | solution.py:41
  118.8 2.9 %collective-permute-start.22 = (bf16[192,512]{1,0:T(8,128)(2,1)S(1)}, bf16[192,512]{1,0:T(8,128)(2,1)S(1)}, u32[]{:S(2)}, u32[]{:S(2)}) collective-permute-start(bf16[192,512]{1,0:T(8,128)(2,1)S(1)} %multiply_convert_fusion.1.refs_0_), channel_id=1, source_target_pairs={{64,0},{17,1},{72,8},{25,9},{80,16},{1,17},{88,24},{9,25},{96,32},... | collective-permute-start | bytes 589832 | tf_op jit(solution)/shard_map/ppermute | solution.py:37
  125.9 4.4 %collective-permute-done.22.refs_2_ = bf16[192,512]{1,0:T(8,128)(2,1)S(1)} collective-permute-done((bf16[192,512]{1,0:T(8,128)(2,1)S(1)}, bf16[192,512]{1,0:T(8,128)(2,1)S(1)}, u32[]{:S(2)}, u32[]{:S(2)}) %collective-permute-start.22) | collective-permute-done | bytes 196640 | tf_op jit(solution)/shard_map/ppermute | solution.py:37
  131.3 3.2 %collective-permute-start.41 = (bf16[768,256]{1,0:T(8,128)(2,1)S(1)}, bf16[768,256]{1,0:T(8,128)(2,1)S(1)}, u32[]{:S(2)}, u32[]{:S(2)}) collective-permute-start(bf16[768,256]{1,0:T(8,128)(2,1)S(1)} %get-tuple-element.39), channel_id=1, source_target_pairs={{8,0},{33,1},{16,8},{41,9},{24,16},{49,17},{0,24},{57,25},{40,32},... | collective-permute-start | bytes 1179656 | tf_op jit(solution)/shard_map/ppermute | solution.py:33
  134.6 10.0 %collective-permute-done.40 = bf16[768,256]{1,0:T(8,128)(2,1)S(1)} collective-permute-done((bf16[768,256]{1,0:T(8,128)(2,1)S(1)}, bf16[768,256]{1,0:T(8,128)(2,1)S(1)}, u32[]{:S(2)}, u32[]{:S(2)}) %collective-permute-start.40) | collective-permute-done | bytes 393248 | tf_op jit(solution)/shard_map/ppermute | solution.py:33
  146.8 12.9 %all_to_all.5 = f32[16,6,128]{2,1,0:T(8,128)S(1)} all-to-all(f32[16,6,128]{2,1,0:T(8,128)S(1)} %broadcast_in_dim.5), channel_id=1, replica_groups=mesh['ra'=16,'cb'=4,'dp'=2] {'ra'}, dimensions={0} | all-to-all | bytes 98304 | tf_op jit(solution)/shard_map/all_to_all | solution.py:174
  163.2 7.7 %collective-permute-done.46.refs_3_ = bf16[384,256]{1,0:T(8,128)(2,1)S(1)} collective-permute-done((bf16[384,256]{1,0:T(8,128)(2,1)S(1)}, bf16[384,256]{1,0:T(8,128)(2,1)S(1)}, u32[]{:S(2)}, u32[]{:S(2)}) %collective-permute-start.46) | collective-permute-done | bytes 196640 | tf_op jit(solution)/shard_map/ppermute | solution.py:45
  (122 shorter events, 48.0 us)
Async XLA Ops:
  28.6 21.6 %collective-permute-start.16 = (bf16[768,512]{1,0:T(8,128)(2,1)S(1)}, bf16[768,512]{1,0:T(8,128)(2,1)S(1)}, u32[]{:S(2)}, u32[]{:S(2)}) collective-permute-start(bf16[768,512]{1,0:T(8,128)(2,1)S(1)} %shard_map.83.refs_1_), channel_id=1, source_target_pairs={{6,0},{0,2},{2,4},{4,6},{7,1},{1,3},{3,5},{5,7},{14,8},{8,10},{10,... | collective-permute-start | bytes 2359304 | tf_op jit(solution)/shard_map/ppermute | solution.py:45
  30.3 21.2 %collective-permute-start.14 = (bf16[768,512]{1,0:T(8,128)(2,1)S(1)}, bf16[768,512]{1,0:T(8,128)(2,1)S(1)}, u32[]{:S(2)}, u32[]{:S(2)}) collective-permute-start(bf16[768,512]{1,0:T(8,128)(2,1)S(1)} %shard_map.83.refs_1_), channel_id=1, source_target_pairs={{2,0},{4,2},{6,4},{0,6},{3,1},{5,3},{7,5},{1,7},{10,8},{12,10},{14... | collective-permute-start | bytes 2359304 | tf_op jit(solution)/shard_map/ppermute | solution.py:45
  34.8 13.2 %collective-permute-start.8 = (bf16[768,256]{1,0:T(8,128)(2,1)S(1)}, bf16[768,256]{1,0:T(8,128)(2,1)S(1)}, u32[]{:S(2)}, u32[]{:S(2)}) collective-permute-start(bf16[768,256]{1,0:T(8,128)(2,1)S(1)} %shard_map.82), channel_id=1, source_target_pairs={{24,0},{97,1},{0,8},{105,9},{8,16},{113,17},{16,24},{121,25},{56,3... | collective-permute-start | bytes 1179656 | tf_op jit(solution)/shard_map/ppermute | solution.py:29
  36.2 13.7 %collective-permute-start.7 = (bf16[768,256]{1,0:T(8,128)(2,1)S(1)}, bf16[768,256]{1,0:T(8,128)(2,1)S(1)}, u32[]{:S(2)}, u32[]{:S(2)}) collective-permute-start(bf16[768,256]{1,0:T(8,128)(2,1)S(1)} %shard_map.82), channel_id=1, source_target_pairs={{8,0},{33,1},{16,8},{41,9},{24,16},{49,17},{0,24},{57,25},{40,32},... | collective-permute-start | bytes 1179656 | tf_op jit(solution)/shard_map/ppermute | solution.py:29
  44.1 12.0 %collective-permute-start.32 = (bf16[256,512]{1,0:T(8,128)(2,1)S(1)}, bf16[256,512]{1,0:T(8,128)(2,1)S(1)}, u32[]{:S(2)}, u32[]{:S(2)}) collective-permute-start(bf16[256,512]{1,0:T(8,128)(2,1)S(1)} %get-tuple-element.52.refs_0_), channel_id=1, source_target_pairs={{6,0},{0,2},{2,4},{4,6},{7,1},{1,3},{3,5},{5,7},{14,8},{8,10},{10,... | collective-permute-start | bytes 786440 | tf_op jit(solution)/shard_map/ppermute | solution.py:45
  51.5 13.9 %collective-permute-start.26 = (bf16[512,256]{1,0:T(8,128)(2,1)S(1)}, bf16[512,256]{1,0:T(8,128)(2,1)S(1)}, u32[]{:S(2)}, u32[]{:S(2)}) collective-permute-start(bf16[512,256]{1,0:T(8,128)(2,1)S(1)} %get-tuple-element.49), channel_id=1, source_target_pairs={{24,0},{97,1},{0,8},{105,9},{8,16},{113,17},{16,24},{121,25},{56,3... | collective-permute-start | bytes 786440 | tf_op jit(solution)/shard_map/ppermute | solution.py:29
  55.8 13.7 %collective-permute-start.17 = (bf16[512,512]{1,0:T(8,128)(2,1)S(1)}, bf16[512,512]{1,0:T(8,128)(2,1)S(1)}, u32[]{:S(2)}, u32[]{:S(2)}) collective-permute-start(bf16[512,512]{1,0:T(8,128)(2,1)S(1)} %slice.45), channel_id=1, source_target_pairs={{6,0},{0,2},{2,4},{4,6},{7,1},{1,3},{3,5},{5,7},{14,8},{8,10},{10,... | collective-permute-start | bytes 1572872 | tf_op jit(solution)/shard_map/ppermute | solution.py:45
  56.2 13.3 %collective-permute-start.15 = (bf16[512,512]{1,0:T(8,128)(2,1)S(1)}, bf16[512,512]{1,0:T(8,128)(2,1)S(1)}, u32[]{:S(2)}, u32[]{:S(2)}) collective-permute-start(bf16[512,512]{1,0:T(8,128)(2,1)S(1)} %shard_map.84), channel_id=1, source_target_pairs={{2,0},{4,2},{6,4},{0,6},{3,1},{5,3},{7,5},{1,7},{10,8},{12,10},{14... | collective-permute-start | bytes 1572872 | tf_op jit(solution)/shard_map/ppermute | solution.py:45
  61.8 12.0 %collective-permute-start.33 = (bf16[192,1536]{1,0:T(8,128)(2,1)S(1)}, bf16[192,1536]{1,0:T(8,128)(2,1)S(1)}, u32[]{:S(2)}, u32[]{:S(2)}) collective-permute-start(bf16[192,1536]{1,0:T(8,128)(2,1)S(1)} %get-tuple-element.30), channel_id=1, source_target_pairs={{96,0},{25,1},{104,8},{1,9},{112,16},{9,17},{120,24},{17,25},{0,32... | collective-permute-start | bytes 1769480 | tf_op jit(solution)/shard_map/ppermute | solution.py:41
  61.9 17.7 %collective-permute-start.34 = (bf16[192,1536]{1,0:T(8,128)(2,1)S(1)}, bf16[192,1536]{1,0:T(8,128)(2,1)S(1)}, u32[]{:S(2)}, u32[]{:S(2)}) collective-permute-start(bf16[192,1536]{1,0:T(8,128)(2,1)S(1)} %get-tuple-element.31), channel_id=1, source_target_pairs={{64,0},{17,1},{72,8},{25,9},{80,16},{1,17},{88,24},{9,25},{96,32},... | collective-permute-start | bytes 1769480 | tf_op jit(solution)/shard_map/ppermute | solution.py:41
  65.4 15.7 %collective-permute-start.35 = (bf16[192,1536]{1,0:T(8,128)(2,1)S(1)}, bf16[192,1536]{1,0:T(8,128)(2,1)S(1)}, u32[]{:S(2)}, u32[]{:S(2)}) collective-permute-start(bf16[192,1536]{1,0:T(8,128)(2,1)S(1)} %get-tuple-element.32), channel_id=1, source_target_pairs={{32,0},{9,1},{40,8},{17,9},{48,16},{25,17},{56,24},{1,25},{64,32},... | collective-permute-start | bytes 1769480 | tf_op jit(solution)/shard_map/ppermute | solution.py:41
  69.5 25.6 %collective-permute-start.30 = (bf16[1536,256]{1,0:T(8,128)(2,1)S(1)}, bf16[1536,256]{1,0:T(8,128)(2,1)S(1)}, u32[]{:S(2)}, u32[]{:S(2)}) collective-permute-start(bf16[1536,256]{1,0:T(8,128)(2,1)S(1)} %shard_map.86.refs_5_), channel_id=1, source_target_pairs={{6,0},{0,2},{2,4},{4,6},{7,1},{1,3},{3,5},{5,7},{14,8},{8,10},{10,... | collective-permute-start | bytes 2359304 | tf_op jit(solution)/shard_map/ppermute | solution.py:45
  69.5 28.2 %collective-permute-start.28 = (bf16[1536,256]{1,0:T(8,128)(2,1)S(1)}, bf16[1536,256]{1,0:T(8,128)(2,1)S(1)}, u32[]{:S(2)}, u32[]{:S(2)}) collective-permute-start(bf16[1536,256]{1,0:T(8,128)(2,1)S(1)} %shard_map.86.refs_5_), channel_id=1, source_target_pairs={{2,0},{4,2},{6,4},{0,6},{3,1},{5,3},{7,5},{1,7},{10,8},{12,10},{14... | collective-permute-start | bytes 2359304 | tf_op jit(solution)/shard_map/ppermute | solution.py:45
  73.7 19.9 %collective-permute-start.39 = (bf16[512,256]{1,0:T(8,128)(2,1)S(1)}, bf16[512,256]{1,0:T(8,128)(2,1)S(1)}, u32[]{:S(2)}, u32[]{:S(2)}) collective-permute-start(bf16[512,256]{1,0:T(8,128)(2,1)S(1)} %get-tuple-element.48.refs_4_), channel_id=1, source_target_pairs={{6,0},{0,2},{2,4},{4,6},{7,1},{1,3},{3,5},{5,7},{14,8},{8,10},{10,... | collective-permute-start | bytes 786440 | tf_op jit(solution)/shard_map/ppermute | solution.py:45
  79.6 14.4 %collective-permute-start.24 = (bf16[512,256]{1,0:T(8,128)(2,1)S(1)}, bf16[512,256]{1,0:T(8,128)(2,1)S(1)}, u32[]{:S(2)}, u32[]{:S(2)}) collective-permute-start(bf16[512,256]{1,0:T(8,128)(2,1)S(1)} %get-tuple-element.48.refs_4_), channel_id=1, source_target_pairs={{2,0},{4,2},{6,4},{0,6},{3,1},{5,3},{7,5},{1,7},{10,8},{12,10},{14... | collective-permute-start | bytes 786440 | tf_op jit(solution)/shard_map/ppermute | solution.py:45
  81.2 18.6 %collective-permute-start.18 = (bf16[192,512]{1,0:T(8,128)(2,1)S(1)}, bf16[192,512]{1,0:T(8,128)(2,1)S(1)}, u32[]{:S(2)}, u32[]{:S(2)}) collective-permute-start(bf16[192,512]{1,0:T(8,128)(2,1)S(1)} %get-tuple-element.26), channel_id=1, source_target_pairs={{96,0},{25,1},{104,8},{1,9},{112,16},{9,17},{120,24},{17,25},{0,32... | collective-permute-start | bytes 589832 | tf_op jit(solution)/shard_map/ppermute | solution.py:41
  93.6 23.2 %collective-permute-start.38 = (bf16[192,1536]{1,0:T(8,128)(2,1)S(1)}, bf16[192,1536]{1,0:T(8,128)(2,1)S(1)}, u32[]{:S(2)}, u32[]{:S(2)}) collective-permute-start(bf16[192,1536]{1,0:T(8,128)(2,1)S(1)} %multiply_convert_fusion.refs_0_), channel_id=1, source_target_pairs={{96,0},{25,1},{104,8},{1,9},{112,16},{9,17},{120,24},{17,25},{0,32... | collective-permute-start | bytes 1769480 | tf_op jit(solution)/shard_map/ppermute | solution.py:37
  94.0 24.9 %collective-permute-start.37 = (bf16[192,1536]{1,0:T(8,128)(2,1)S(1)}, bf16[192,1536]{1,0:T(8,128)(2,1)S(1)}, u32[]{:S(2)}, u32[]{:S(2)}) collective-permute-start(bf16[192,1536]{1,0:T(8,128)(2,1)S(1)} %multiply_convert_fusion.refs_0_), channel_id=1, source_target_pairs={{64,0},{17,1},{72,8},{25,9},{80,16},{1,17},{88,24},{9,25},{96,32},... | collective-permute-start | bytes 1769480 | tf_op jit(solution)/shard_map/ppermute | solution.py:37
  95.1 26.7 %collective-permute-start.36 = (bf16[192,1536]{1,0:T(8,128)(2,1)S(1)}, bf16[192,1536]{1,0:T(8,128)(2,1)S(1)}, u32[]{:S(2)}, u32[]{:S(2)}) collective-permute-start(bf16[192,1536]{1,0:T(8,128)(2,1)S(1)} %multiply_convert_fusion.refs_0_), channel_id=1, source_target_pairs={{32,0},{9,1},{40,8},{17,9},{48,16},{25,17},{56,24},{1,25},{64,32},... | collective-permute-start | bytes 1769480 | tf_op jit(solution)/shard_map/ppermute | solution.py:37
  97.7 13.7 %collective-permute-start.19 = (bf16[192,512]{1,0:T(8,128)(2,1)S(1)}, bf16[192,512]{1,0:T(8,128)(2,1)S(1)}, u32[]{:S(2)}, u32[]{:S(2)}) collective-permute-start(bf16[192,512]{1,0:T(8,128)(2,1)S(1)} %get-tuple-element.27), channel_id=1, source_target_pairs={{64,0},{17,1},{72,8},{25,9},{80,16},{1,17},{88,24},{9,25},{96,32},... | collective-permute-start | bytes 589832 | tf_op jit(solution)/shard_map/ppermute | solution.py:41
  99.8 16.4 %collective-permute-start.20 = (bf16[192,512]{1,0:T(8,128)(2,1)S(1)}, bf16[192,512]{1,0:T(8,128)(2,1)S(1)}, u32[]{:S(2)}, u32[]{:S(2)}) collective-permute-start(bf16[192,512]{1,0:T(8,128)(2,1)S(1)} %get-tuple-element.28), channel_id=1, source_target_pairs={{32,0},{9,1},{40,8},{17,9},{48,16},{25,17},{56,24},{1,25},{64,32},... | collective-permute-start | bytes 589832 | tf_op jit(solution)/shard_map/ppermute | solution.py:41
  111.5 13.5 %collective-permute-start.31 = (bf16[1024,256]{1,0:T(8,128)(2,1)S(1)}, bf16[1024,256]{1,0:T(8,128)(2,1)S(1)}, u32[]{:S(2)}, u32[]{:S(2)}) collective-permute-start(bf16[1024,256]{1,0:T(8,128)(2,1)S(1)} %slice.47), channel_id=1, source_target_pairs={{6,0},{0,2},{2,4},{4,6},{7,1},{1,3},{3,5},{5,7},{14,8},{8,10},{10,... | collective-permute-start | bytes 1572872 | tf_op jit(solution)/shard_map/ppermute | solution.py:45
  131.2 13.3 %collective-permute-start.40 = (bf16[768,256]{1,0:T(8,128)(2,1)S(1)}, bf16[768,256]{1,0:T(8,128)(2,1)S(1)}, u32[]{:S(2)}, u32[]{:S(2)}) collective-permute-start(bf16[768,256]{1,0:T(8,128)(2,1)S(1)} %get-tuple-element.38), channel_id=1, source_target_pairs={{24,0},{97,1},{0,8},{105,9},{8,16},{113,17},{16,24},{121,25},{56,3... | collective-permute-start | bytes 1179656 | tf_op jit(solution)/shard_map/ppermute | solution.py:33
  131.3 13.2 %collective-permute-start.41 = (bf16[768,256]{1,0:T(8,128)(2,1)S(1)}, bf16[768,256]{1,0:T(8,128)(2,1)S(1)}, u32[]{:S(2)}, u32[]{:S(2)}) collective-permute-start(bf16[768,256]{1,0:T(8,128)(2,1)S(1)} %get-tuple-element.39), channel_id=1, source_target_pairs={{8,0},{33,1},{16,8},{41,9},{24,16},{49,17},{0,24},{57,25},{40,32},... | collective-permute-start | bytes 1179656 | tf_op jit(solution)/shard_map/ppermute | solution.py:33
  (28 other events, 294.0 us)

commit v5 on v4

--- a/solution.py
+++ b/solution.py
@@ -201,29 +201,34 @@
         blocks = [from_gather_ring(block_for(-j), j) for j in others]
         rest = stacked(*blocks)
         rest_by_y = {d: from_plane(rest, d) for d in (1, 3)}
-        cut = own.shape[0]
-        first = stacked(own_by_y[1], rest_by_y[1][:cut])
-        far = (from_plane(first, 1), from_plane(rest_by_y[3][cut:], 3))
-        return (own, rest), [(own_by_y[d], rest_by_y[d]) for d in (1, 3)], far
-
-    up_own, up_near, up_far = gathered(up_for)
-    down_own, down_near, down_far = gathered(down_for)
-
-    def quarter(array):
-        return lax.dynamic_slice(array, (y * few, 0), (few, held)).astype(f32)
-
-    mixed_in = residual_scale * quarter(carried) + quarter(branch_in)
+        return (own, rest), [(own_by_y[d], rest_by_y[d]) for d in (1, 3)]
+
+    up_own, up_near = gathered(up_for)
+    down_own, down_near = gathered(down_for)
+
+    def quarters(array):
+        taken = [
+            lax.dynamic_slice(array, ((y + d) % 4 * few, 0), (few, held)) for d in (0, 2)
+        ]
+        return jnp.concatenate(taken, axis=0).astype(f32)
+
+    mixed_in = residual_scale * quarters(carried) + quarters(branch_in)
     sums = own_sums(mixed_in)
     sums = sum([from_sum_ring(sums, j) for j in others], sums)
     arrived = [from_gather_ring(sums, j) for j in others]
     sums = sum(arrived, sums)
     mean, inverse = scales(sums, width)
     normed = ((mixed_in - mean) * inverse * gain_in + bias_in).astype(bf16)
-    both = stacked(normed, from_other_core(normed))
-    features = [both] + [from_gather_ring(both, j) for j in others]
-    features = jnp.concatenate(features, axis=1)
-
-    def activated(weights):
+    other = from_other_core(normed)
+
+    def features_of(first):
+        both = stacked(normed[first : first + few], other[first : first + few])
+        pieces = [both] + [from_gather_ring(both, j) for j in others]
+        return jnp.concatenate(pieces, axis=1)
+
+    near_features, far_features = features_of(0), features_of(few)
+
+    def activated(features, weights):
         parts = up_products(turn, features, weights)
         total = parts[0]
         for j in (1, 2, 3):
@@ -231,15 +236,20 @@
         own = jnp.square(jnp.maximum(total, 0.0)).astype(bf16)
         return [own] + [from_sum_ring(own, j) for j in (1, 2, 3)]
 
-    hidden_near = activated([up_own] + up_near)
-    hidden_far = activated([up_far])
-    begun = down_products(turn, [hidden_near], [down_own] + down_near, [], False)
-    parts = down_products(turn, [hidden_far], [down_far], begun, True)
-    total = parts[0]
-    for j, part in zip(others, parts[1:]):
-        total = total + to_gather_ring(part, j).astype(f32)
+    def summed(parts):
+        total = parts[0]
+        for j, part in zip(others, parts[1:]):
+            total = total + to_gather_ring(part, j).astype(f32)
+        return total
+
+    hidden_near = activated(near_features, [up_own] + up_near)
+    hidden_far = activated(far_features, [up_own])
+    far_parts = down_products(turn, [hidden_far], [down_own], [], True)
+    for_far = summed(far_parts)
+    near_parts = down_products(turn, [hidden_near], [down_own] + down_near, [], True)
+    total = summed(near_parts) + from_plane(for_far, 2)
     mine, theirs = total[:few], from_other_core(total[few:])
-    mixed_out = residual_scale * normed.astype(f32) + (mine + theirs)
+    mixed_out = residual_scale * normed[:few].astype(f32) + (mine + theirs)
     mean, inverse = scales(group_sums(mixed_out), width)
     out = ((mixed_out - mean) * inverse * gain_out + bias_out).astype(bf16)
     return placed(y, [out] + [from_plane(out, d) for d in (1, 2, 3)])

time: 173 us -> 195 us (1.13)
  starting transfers between devices: 59 us -> 98.1 us
  waiting for transfers between devices: 86.6 us -> 67 us
  blocking collectives: 12.9 us -> 17.2 us
    ppermute x6, waiting for transfers between devices: 21.4 us -> 2.46 us  [to_sum_ring(): return lax.ppermute(array, ('ra', 'dp'), ring_pairs(False, -distance))]
    ppermute x9, waiting for transfers between devices: 5.96 us -> 21.9 us  [from_sum_ring(): return lax.ppermute(array, ('ra', 'dp'), ring_pairs(False, distance))]
    ppermute x3 -> x6, starting transfers between devices: 3.3 us -> 17.4 us  [to_gather_ring(): return lax.ppermute(array, ('ra', 'dp'), ring_pairs(True, -distance))]
    ppermute x12 -> x15, starting transfers between devices: 14.3 us -> 26.6 us  [from_gather_ring(): return lax.ppermute(array, ('ra', 'dp'), ring_pairs(True, distance))]
    ppermute x12 -> x15, waiting for transfers between devices: 18.1 us -> 7.82 us  [from_gather_ring(): return lax.ppermute(array, ('ra', 'dp'), ring_pairs(True, distance))]
    ppermute x15 -> x12, waiting for transfers between devices: 28 us -> 18.5 us  [from_plane(): lax.ppermute(array, 'cb', [((y + distance) % 4, y) for y in range(4)])]
    ppermute x15 -> x12, starting transfers between devices: 17.4 us -> 22.2 us  [from_plane(): lax.ppermute(array, 'cb', [((y + distance) % 4, y) for y in range(4)])]
    ppermute x3 -> x6, waiting for transfers between devices: 9.97 us -> 14.6 us  [to_gather_ring(): return lax.ppermute(array, ('ra', 'dp'), ring_pairs(True, -distance))]
  transfers between devices with their start and end apart: 47 -> 50, of which waited for: 18 -> 25; matrix products, arithmetic and copies ran while one was open for 2% -> 1% of each run, Pallas kernels for 4% -> 4%
where the time goes in v5:
time: 195 us
  starting transfers between devices  98.1 us (50%)
  waiting for transfers between devices  67 us (34%)
  blocking collectives  17.2 us (9%)
  Pallas kernels  8.29 us (4%)
  other arithmetic  2.28 us (1%)
    ppermute x15, starting transfers between devices, from_gather_ring(): return lax.ppermute(array, ('ra', 'dp'), ring_pairs(True, distance))  26.6 us
    ppermute x12, starting transfers between devices, from_plane(): lax.ppermute(array, 'cb', [((y + distance) % 4, y) for y in range(4)])  22.2 us
    ppermute x9, waiting for transfers between devices, from_sum_ring(): return lax.ppermute(array, ('ra', 'dp'), ring_pairs(False, distance))  21.9 us
    ppermute x9, starting transfers between devices, from_sum_ring(): return lax.ppermute(array, ('ra', 'dp'), ring_pairs(False, distance))  20.9 us
    ppermute x12, waiting for transfers between devices, from_plane(): lax.ppermute(array, 'cb', [((y + distance) % 4, y) for y in range(4)])  18.5 us
    ppermute x6, starting transfers between devices, to_gather_ring(): return lax.ppermute(array, ('ra', 'dp'), ring_pairs(True, -distance))  17.4 us
    all_to_all x1, blocking collectives, group_sums(): sums = lax.all_to_all(sent, 'ra', 0, 0, tiled=True)  17.2 us
    ppermute x6, waiting for transfers between devices, to_gather_ring(): return lax.ppermute(array, ('ra', 'dp'), ring_pairs(True, -distance))  14.6 us
  transfers between devices with their start and end apart: 50, of which 25 were waited for; matrix products, arithmetic and copies ran while one was open for 1% of the time, Pallas kernels for 4%

profile of v5, /device:TPU:0, one launch (start us, length us, event | category | flops | bytes accessed | tf_op | source)
XLA Modules:
  0.0 195.1 jit_solution(14388246386846171043)
XLA Ops:
  1.8 4.1 %collective-permute-start.2 = (f32[12,128]{1,0:T(8,128)S(1)}, f32[12,128]{1,0:T(8,128)S(1)}, u32[]{:S(2)}, u32[]{:S(2)}) collective-permute-start(f32[12,128]{1,0:T(8,128)S(1)} %reshape.68), channel_id=1, source_target_pairs={{64,0},{17,1},{72,8},{25,9},{80,16},{1,17},{88,24},{9,25},{96,32},... | collective-permute-start | bytes 18440 | tf_op jit(solution)/shard_map/ppermute | solution.py:37
  10.7 3.1 %collective-permute-start.5 = (f32[12,128]{1,0:T(8,128)S(1)}, f32[12,128]{1,0:T(8,128)S(1)}, u32[]{:S(2)}, u32[]{:S(2)}) collective-permute-start(f32[12,128]{1,0:T(8,128)S(1)} %add_add_fusion.2), channel_id=1, source_target_pairs={{16,0},{65,1},{24,8},{73,9},{0,16},{81,17},{8,24},{89,25},{48,32},... | collective-permute-start | bytes 18440 | tf_op jit(solution)/shard_map/ppermute | solution.py:29
  27.3 3.3 %collective-permute-start.33 = (bf16[768,256]{1,0:T(8,128)(2,1)S(1)}, bf16[768,256]{1,0:T(8,128)(2,1)S(1)}, u32[]{:S(2)}, u32[]{:S(2)}) collective-permute-start(bf16[768,256]{1,0:T(8,128)(2,1)S(1)} %shard_map.87), channel_id=1, source_target_pairs={{8,0},{33,1},{16,8},{41,9},{24,16},{49,17},{0,24},{57,25},{40,32},... | collective-permute-start | bytes 1179656 | tf_op jit(solution)/shard_map/ppermute | solution.py:29
  39.7 3.2 %collective-permute-start.7 = (bf16[768,256]{1,0:T(8,128)(2,1)S(1)}, bf16[768,256]{1,0:T(8,128)(2,1)S(1)}, u32[]{:S(2)}, u32[]{:S(2)}) collective-permute-start(bf16[768,256]{1,0:T(8,128)(2,1)S(1)} %shard_map.82), channel_id=1, source_target_pairs={{8,0},{33,1},{16,8},{41,9},{24,16},{49,17},{0,24},{57,25},{40,32},... | collective-permute-start | bytes 1179656 | tf_op jit(solution)/shard_map/ppermute | solution.py:29
  43.4 2.9 %collective-permute-start.14 = (bf16[768,512]{1,0:T(8,128)(2,1)S(1)}, bf16[768,512]{1,0:T(8,128)(2,1)S(1)}, u32[]{:S(2)}, u32[]{:S(2)}) collective-permute-start(bf16[768,512]{1,0:T(8,128)(2,1)S(1)} %shard_map.83.refs_1_), channel_id=1, source_target_pairs={{2,0},{4,2},{6,4},{0,6},{3,1},{5,3},{7,5},{1,7},{10,8},{12,10},{14... | collective-permute-start | bytes 2359304 | tf_op jit(solution)/shard_map/ppermute | solution.py:45
  57.2 3.8 %collective-permute-start.25 = (bf16[512,256]{1,0:T(8,128)(2,1)S(1)}, bf16[512,256]{1,0:T(8,128)(2,1)S(1)}, u32[]{:S(2)}, u32[]{:S(2)}) collective-permute-start(bf16[512,256]{1,0:T(8,128)(2,1)S(1)} %get-tuple-element.46), channel_id=1, source_target_pairs={{16,0},{65,1},{24,8},{73,9},{0,16},{81,17},{8,24},{89,25},{48,32},... | collective-permute-start | bytes 786440 | tf_op jit(solution)/shard_map/ppermute | solution.py:29
  63.0 3.7 %collective-permute-done.13.refs_2_ = bf16[256,512]{1,0:T(8,128)(2,1)S(1)} collective-permute-done((bf16[256,512]{1,0:T(8,128)(2,1)S(1)}, bf16[256,512]{1,0:T(8,128)(2,1)S(1)}, u32[]{:S(2)}, u32[]{:S(2)}) %collective-permute-start.13) | collective-permute-done | bytes 262176 | tf_op jit(solution)/shard_map/ppermute | solution.py:45
  69.8 4.3 %collective-permute-start.18 = (bf16[192,1536]{1,0:T(8,128)(2,1)S(1)}, bf16[192,1536]{1,0:T(8,128)(2,1)S(1)}, u32[]{:S(2)}, u32[]{:S(2)}) collective-permute-start(bf16[192,1536]{1,0:T(8,128)(2,1)S(1)} %get-tuple-element.27), channel_id=1, source_target_pairs={{64,0},{17,1},{72,8},{25,9},{80,16},{1,17},{88,24},{9,25},{96,32},... | collective-permute-start | bytes 1769480 | tf_op jit(solution)/shard_map/ppermute | solution.py:41
  79.6 10.8 %collective-permute-done.40.refs_2_ = bf16[192,512]{1,0:T(8,128)(2,1)S(1)} collective-permute-done((bf16[192,512]{1,0:T(8,128)(2,1)S(1)}, bf16[192,512]{1,0:T(8,128)(2,1)S(1)}, u32[]{:S(2)}, u32[]{:S(2)}) %collective-permute-start.40) | collective-permute-done | bytes 196640 | tf_op jit(solution)/shard_map/ppermute | solution.py:37
  92.3 3.8 %collective-permute-start.26 = (bf16[512,256]{1,0:T(8,128)(2,1)S(1)}, bf16[512,256]{1,0:T(8,128)(2,1)S(1)}, u32[]{:S(2)}, u32[]{:S(2)}) collective-permute-start(bf16[512,256]{1,0:T(8,128)(2,1)S(1)} %get-tuple-element.48.refs_4_), channel_id=1, source_target_pairs={{2,0},{4,2},{6,4},{0,6},{3,1},{5,3},{7,5},{1,7},{10,8},{12,10},{14... | collective-permute-start | bytes 786440 | tf_op jit(solution)/shard_map/ppermute | solution.py:45
  97.2 3.9 %collective-permute-done.28.refs_8_ = bf16[512,256]{1,0:T(8,128)(2,1)S(1)} collective-permute-done((bf16[512,256]{1,0:T(8,128)(2,1)S(1)}, bf16[512,256]{1,0:T(8,128)(2,1)S(1)}, u32[]{:S(2)}, u32[]{:S(2)}) %collective-permute-start.28) | collective-permute-done | bytes 262176 | tf_op jit(solution)/shard_map/ppermute | solution.py:45
  101.1 3.3 %collective-permute-start.27 = (bf16[1536,256]{1,0:T(8,128)(2,1)S(1)}, bf16[1536,256]{1,0:T(8,128)(2,1)S(1)}, u32[]{:S(2)}, u32[]{:S(2)}) collective-permute-start(bf16[1536,256]{1,0:T(8,128)(2,1)S(1)} %shard_map.85.refs_5_), channel_id=1, source_target_pairs={{2,0},{4,2},{6,4},{0,6},{3,1},{5,3},{7,5},{1,7},{10,8},{12,10},{14... | collective-permute-start | bytes 2359304 | tf_op jit(solution)/shard_map/ppermute | solution.py:45
  107.6 3.3 %collective-permute-start.44 = (bf16[768,256]{1,0:T(8,128)(2,1)S(1)}, bf16[768,256]{1,0:T(8,128)(2,1)S(1)}, u32[]{:S(2)}, u32[]{:S(2)}) collective-permute-start(bf16[768,256]{1,0:T(8,128)(2,1)S(1)} %get-tuple-element.40), channel_id=1, source_target_pairs={{16,0},{65,1},{24,8},{73,9},{0,16},{81,17},{8,24},{89,25},{48,32},... | collective-permute-start | bytes 1179656 | tf_op jit(solution)/shard_map/ppermute | solution.py:33
  113.3 6.4 %collective-permute-start.22 = (bf16[192,1536]{1,0:T(8,128)(2,1)S(1)}, bf16[192,1536]{1,0:T(8,128)(2,1)S(1)}, u32[]{:S(2)}, u32[]{:S(2)}) collective-permute-start(bf16[192,1536]{1,0:T(8,128)(2,1)S(1)} %multiply_convert_fusion.refs_0_), channel_id=1, source_target_pairs={{96,0},{25,1},{104,8},{1,9},{112,16},{9,17},{120,24},{17,25},{0,32... | collective-permute-start | bytes 1769480 | tf_op jit(solution)/shard_map/ppermute | solution.py:37
  123.7 3.4 %collective-permute-start.20 = (bf16[192,1536]{1,0:T(8,128)(2,1)S(1)}, bf16[192,1536]{1,0:T(8,128)(2,1)S(1)}, u32[]{:S(2)}, u32[]{:S(2)}) collective-permute-start(bf16[192,1536]{1,0:T(8,128)(2,1)S(1)} %multiply_convert_fusion.refs_0_), channel_id=1, source_target_pairs={{32,0},{9,1},{40,8},{17,9},{48,16},{25,17},{56,24},{1,25},{64,32},... | collective-permute-start | bytes 1769480 | tf_op jit(solution)/shard_map/ppermute | solution.py:37
  127.4 3.0 %collective-permute-start.45 = (f32[768,256]{1,0:T(8,128)S(1)}, f32[768,256]{1,0:T(8,128)S(1)}, u32[]{:S(2)}, u32[]{:S(2)}) collective-permute-start(f32[768,256]{1,0:T(8,128)S(1)} %convert_add_fusion), channel_id=1, source_target_pairs={{4,0},{6,2},{0,4},{2,6},{5,1},{7,3},{1,5},{3,7},{12,8},{14,10},{8,... | collective-permute-start | bytes 2359304 | tf_op jit(solution)/shard_map/ppermute | solution.py:45
  130.4 3.8 %collective-permute-done.21.refs_2_ = bf16[192,1536]{1,0:T(8,128)(2,1)S(1)} collective-permute-done((bf16[192,1536]{1,0:T(8,128)(2,1)S(1)}, bf16[192,1536]{1,0:T(8,128)(2,1)S(1)}, u32[]{:S(2)}, u32[]{:S(2)}) %collective-permute-start.21) | collective-permute-done | bytes 589856 | tf_op jit(solution)/shard_map/ppermute | solution.py:37
  134.2 5.2 %collective-permute-done.20.refs_1_ = bf16[192,1536]{1,0:T(8,128)(2,1)S(1)} collective-permute-done((bf16[192,1536]{1,0:T(8,128)(2,1)S(1)}, bf16[192,1536]{1,0:T(8,128)(2,1)S(1)}, u32[]{:S(2)}, u32[]{:S(2)}) %collective-permute-start.20) | collective-permute-done | bytes 589856 | tf_op jit(solution)/shard_map/ppermute | solution.py:37
  142.0 3.1 %collective-permute-start.30 = (bf16[768,256]{1,0:T(8,128)(2,1)S(1)}, bf16[768,256]{1,0:T(8,128)(2,1)S(1)}, u32[]{:S(2)}, u32[]{:S(2)}) collective-permute-start(bf16[768,256]{1,0:T(8,128)(2,1)S(1)} %get-tuple-element.30), channel_id=1, source_target_pairs={{24,0},{97,1},{0,8},{105,9},{8,16},{113,17},{16,24},{121,25},{56,3... | collective-permute-start | bytes 1179656 | tf_op jit(solution)/shard_map/ppermute | solution.py:33
  145.1 6.4 %collective-permute-start.31 = (bf16[768,256]{1,0:T(8,128)(2,1)S(1)}, bf16[768,256]{1,0:T(8,128)(2,1)S(1)}, u32[]{:S(2)}, u32[]{:S(2)}) collective-permute-start(bf16[768,256]{1,0:T(8,128)(2,1)S(1)} %get-tuple-element.31), channel_id=1, source_target_pairs={{8,0},{33,1},{16,8},{41,9},{24,16},{49,17},{0,24},{57,25},{40,32},... | collective-permute-start | bytes 1179656 | tf_op jit(solution)/shard_map/ppermute | solution.py:33
  152.8 4.3 %collective-permute-done.30 = bf16[768,256]{1,0:T(8,128)(2,1)S(1)} collective-permute-done((bf16[768,256]{1,0:T(8,128)(2,1)S(1)}, bf16[768,256]{1,0:T(8,128)(2,1)S(1)}, u32[]{:S(2)}, u32[]{:S(2)}) %collective-permute-start.30) | collective-permute-done | bytes 393248 | tf_op jit(solution)/shard_map/ppermute | solution.py:33
  157.1 3.8 %collective-permute-done.31 = bf16[768,256]{1,0:T(8,128)(2,1)S(1)} collective-permute-done((bf16[768,256]{1,0:T(8,128)(2,1)S(1)}, bf16[768,256]{1,0:T(8,128)(2,1)S(1)}, u32[]{:S(2)}, u32[]{:S(2)}) %collective-permute-start.31) | collective-permute-done | bytes 393248 | tf_op jit(solution)/shard_map/ppermute | solution.py:33
  165.1 17.2 %all_to_all.5 = f32[16,6,128]{2,1,0:T(8,128)S(1)} all-to-all(f32[16,6,128]{2,1,0:T(8,128)S(1)} %broadcast_in_dim.5), channel_id=1, replica_groups=mesh['ra'=16,'cb'=4,'dp'=2] {'ra'}, dimensions={0} | all-to-all | bytes 98304 | tf_op jit(solution)/shard_map/all_to_all | solution.py:174
  185.9 7.7 %collective-permute-done.49.refs_3_ = bf16[384,256]{1,0:T(8,128)(2,1)S(1)} collective-permute-done((bf16[384,256]{1,0:T(8,128)(2,1)S(1)}, bf16[384,256]{1,0:T(8,128)(2,1)S(1)}, u32[]{:S(2)}, u32[]{:S(2)}) %collective-permute-start.49) | collective-permute-done | bytes 196640 | tf_op jit(solution)/shard_map/ppermute | solution.py:45
  (130 shorter events, 76.9 us)
Async XLA Ops:
  22.9 16.8 %collective-permute-start.35 = (bf16[768,256]{1,0:T(8,128)(2,1)S(1)}, bf16[768,256]{1,0:T(8,128)(2,1)S(1)}, u32[]{:S(2)}, u32[]{:S(2)}) collective-permute-start(bf16[768,256]{1,0:T(8,128)(2,1)S(1)} %shard_map.87), channel_id=1, source_target_pairs={{16,0},{65,1},{24,8},{73,9},{0,16},{81,17},{8,24},{89,25},{48,32},... | collective-permute-start | bytes 1179656 | tf_op jit(solution)/shard_map/ppermute | solution.py:29
  25.8 17.2 %collective-permute-start.34 = (bf16[768,256]{1,0:T(8,128)(2,1)S(1)}, bf16[768,256]{1,0:T(8,128)(2,1)S(1)}, u32[]{:S(2)}, u32[]{:S(2)}) collective-permute-start(bf16[768,256]{1,0:T(8,128)(2,1)S(1)} %shard_map.87), channel_id=1, source_target_pairs={{24,0},{97,1},{0,8},{105,9},{8,16},{113,17},{16,24},{121,25},{56,3... | collective-permute-start | bytes 1179656 | tf_op jit(solution)/shard_map/ppermute | solution.py:29
  27.3 16.0 %collective-permute-start.33 = (bf16[768,256]{1,0:T(8,128)(2,1)S(1)}, bf16[768,256]{1,0:T(8,128)(2,1)S(1)}, u32[]{:S(2)}, u32[]{:S(2)}) collective-permute-start(bf16[768,256]{1,0:T(8,128)(2,1)S(1)} %shard_map.87), channel_id=1, source_target_pairs={{8,0},{33,1},{16,8},{41,9},{24,16},{49,17},{0,24},{57,25},{40,32},... | collective-permute-start | bytes 1179656 | tf_op jit(solution)/shard_map/ppermute | solution.py:29
  35.0 12.5 %collective-permute-start.9 = (bf16[768,256]{1,0:T(8,128)(2,1)S(1)}, bf16[768,256]{1,0:T(8,128)(2,1)S(1)}, u32[]{:S(2)}, u32[]{:S(2)}) collective-permute-start(bf16[768,256]{1,0:T(8,128)(2,1)S(1)} %shard_map.82), channel_id=1, source_target_pairs={{16,0},{65,1},{24,8},{73,9},{0,16},{81,17},{8,24},{89,25},{48,32},... | collective-permute-start | bytes 1179656 | tf_op jit(solution)/shard_map/ppermute | solution.py:29
  43.0 23.7 %collective-permute-start.16 = (bf16[768,512]{1,0:T(8,128)(2,1)S(1)}, bf16[768,512]{1,0:T(8,128)(2,1)S(1)}, u32[]{:S(2)}, u32[]{:S(2)}) collective-permute-start(bf16[768,512]{1,0:T(8,128)(2,1)S(1)} %shard_map.83.refs_1_), channel_id=1, source_target_pairs={{6,0},{0,2},{2,4},{4,6},{7,1},{1,3},{3,5},{5,7},{14,8},{8,10},{10,... | collective-permute-start | bytes 2359304 | tf_op jit(solution)/shard_map/ppermute | solution.py:45
  43.4 23.7 %collective-permute-start.14 = (bf16[768,512]{1,0:T(8,128)(2,1)S(1)}, bf16[768,512]{1,0:T(8,128)(2,1)S(1)}, u32[]{:S(2)}, u32[]{:S(2)}) collective-permute-start(bf16[768,512]{1,0:T(8,128)(2,1)S(1)} %shard_map.83.refs_1_), channel_id=1, source_target_pairs={{2,0},{4,2},{6,4},{0,6},{3,1},{5,3},{7,5},{1,7},{10,8},{12,10},{14... | collective-permute-start | bytes 2359304 | tf_op jit(solution)/shard_map/ppermute | solution.py:45
  54.5 12.2 %collective-permute-start.13 = (bf16[256,512]{1,0:T(8,128)(2,1)S(1)}, bf16[256,512]{1,0:T(8,128)(2,1)S(1)}, u32[]{:S(2)}, u32[]{:S(2)}) collective-permute-start(bf16[256,512]{1,0:T(8,128)(2,1)S(1)} %get-tuple-element.52.refs_0_), channel_id=1, source_target_pairs={{2,0},{4,2},{6,4},{0,6},{3,1},{5,3},{7,5},{1,7},{10,8},{12,10},{14... | collective-permute-start | bytes 786440 | tf_op jit(solution)/shard_map/ppermute | solution.py:45
  57.2 12.6 %collective-permute-start.25 = (bf16[512,256]{1,0:T(8,128)(2,1)S(1)}, bf16[512,256]{1,0:T(8,128)(2,1)S(1)}, u32[]{:S(2)}, u32[]{:S(2)}) collective-permute-start(bf16[512,256]{1,0:T(8,128)(2,1)S(1)} %get-tuple-element.46), channel_id=1, source_target_pairs={{16,0},{65,1},{24,8},{73,9},{0,16},{81,17},{8,24},{89,25},{48,32},... | collective-permute-start | bytes 786440 | tf_op jit(solution)/shard_map/ppermute | solution.py:29
  61.9 12.2 %collective-permute-start.23 = (bf16[512,256]{1,0:T(8,128)(2,1)S(1)}, bf16[512,256]{1,0:T(8,128)(2,1)S(1)}, u32[]{:S(2)}, u32[]{:S(2)}) collective-permute-start(bf16[512,256]{1,0:T(8,128)(2,1)S(1)} %get-tuple-element.47), channel_id=1, source_target_pairs={{8,0},{33,1},{16,8},{41,9},{24,16},{49,17},{0,24},{57,25},{40,32},... | collective-permute-start | bytes 786440 | tf_op jit(solution)/shard_map/ppermute | solution.py:29
  69.7 34.6 %collective-permute-start.17 = (bf16[192,1536]{1,0:T(8,128)(2,1)S(1)}, bf16[192,1536]{1,0:T(8,128)(2,1)S(1)}, u32[]{:S(2)}, u32[]{:S(2)}) collective-permute-start(bf16[192,1536]{1,0:T(8,128)(2,1)S(1)} %get-tuple-element.26), channel_id=1, source_target_pairs={{96,0},{25,1},{104,8},{1,9},{112,16},{9,17},{120,24},{17,25},{0,32... | collective-permute-start | bytes 1769480 | tf_op jit(solution)/shard_map/ppermute | solution.py:41
  69.8 36.2 %collective-permute-start.18 = (bf16[192,1536]{1,0:T(8,128)(2,1)S(1)}, bf16[192,1536]{1,0:T(8,128)(2,1)S(1)}, u32[]{:S(2)}, u32[]{:S(2)}) collective-permute-start(bf16[192,1536]{1,0:T(8,128)(2,1)S(1)} %get-tuple-element.27), channel_id=1, source_target_pairs={{64,0},{17,1},{72,8},{25,9},{80,16},{1,17},{88,24},{9,25},{96,32},... | collective-permute-start | bytes 1769480 | tf_op jit(solution)/shard_map/ppermute | solution.py:41
  74.1 33.5 %collective-permute-start.19 = (bf16[192,1536]{1,0:T(8,128)(2,1)S(1)}, bf16[192,1536]{1,0:T(8,128)(2,1)S(1)}, u32[]{:S(2)}, u32[]{:S(2)}) collective-permute-start(bf16[192,1536]{1,0:T(8,128)(2,1)S(1)} %get-tuple-element.28), channel_id=1, source_target_pairs={{32,0},{9,1},{40,8},{17,9},{48,16},{25,17},{56,24},{1,25},{64,32},... | collective-permute-start | bytes 1769480 | tf_op jit(solution)/shard_map/ppermute | solution.py:41
  77.7 12.7 %collective-permute-start.40 = (bf16[192,512]{1,0:T(8,128)(2,1)S(1)}, bf16[192,512]{1,0:T(8,128)(2,1)S(1)}, u32[]{:S(2)}, u32[]{:S(2)}) collective-permute-start(bf16[192,512]{1,0:T(8,128)(2,1)S(1)} %multiply_convert_fusion.1.refs_0_), channel_id=1, source_target_pairs={{64,0},{17,1},{72,8},{25,9},{80,16},{1,17},{88,24},{9,25},{96,32},... | collective-permute-start | bytes 589832 | tf_op jit(solution)/shard_map/ppermute | solution.py:37
  77.7 14.7 %collective-permute-start.39 = (bf16[192,512]{1,0:T(8,128)(2,1)S(1)}, bf16[192,512]{1,0:T(8,128)(2,1)S(1)}, u32[]{:S(2)}, u32[]{:S(2)}) collective-permute-start(bf16[192,512]{1,0:T(8,128)(2,1)S(1)} %multiply_convert_fusion.1.refs_0_), channel_id=1, source_target_pairs={{32,0},{9,1},{40,8},{17,9},{48,16},{25,17},{56,24},{1,25},{64,32},... | collective-permute-start | bytes 589832 | tf_op jit(solution)/shard_map/ppermute | solution.py:37
  101.1 26.3 %collective-permute-start.29 = (bf16[1536,256]{1,0:T(8,128)(2,1)S(1)}, bf16[1536,256]{1,0:T(8,128)(2,1)S(1)}, u32[]{:S(2)}, u32[]{:S(2)}) collective-permute-start(bf16[1536,256]{1,0:T(8,128)(2,1)S(1)} %shard_map.85.refs_5_), channel_id=1, source_target_pairs={{6,0},{0,2},{2,4},{4,6},{7,1},{1,3},{3,5},{5,7},{14,8},{8,10},{10,... | collective-permute-start | bytes 2359304 | tf_op jit(solution)/shard_map/ppermute | solution.py:45
  101.1 29.3 %collective-permute-start.27 = (bf16[1536,256]{1,0:T(8,128)(2,1)S(1)}, bf16[1536,256]{1,0:T(8,128)(2,1)S(1)}, u32[]{:S(2)}, u32[]{:S(2)}) collective-permute-start(bf16[1536,256]{1,0:T(8,128)(2,1)S(1)} %shard_map.85.refs_5_), channel_id=1, source_target_pairs={{2,0},{4,2},{6,4},{0,6},{3,1},{5,3},{7,5},{1,7},{10,8},{12,10},{14... | collective-permute-start | bytes 2359304 | tf_op jit(solution)/shard_map/ppermute | solution.py:45
  106.0 13.7 %collective-permute-start.43 = (bf16[768,256]{1,0:T(8,128)(2,1)S(1)}, bf16[768,256]{1,0:T(8,128)(2,1)S(1)}, u32[]{:S(2)}, u32[]{:S(2)}) collective-permute-start(bf16[768,256]{1,0:T(8,128)(2,1)S(1)} %get-tuple-element.39), channel_id=1, source_target_pairs={{8,0},{33,1},{16,8},{41,9},{24,16},{49,17},{0,24},{57,25},{40,32},... | collective-permute-start | bytes 1179656 | tf_op jit(solution)/shard_map/ppermute | solution.py:33
  107.6 16.2 %collective-permute-start.44 = (bf16[768,256]{1,0:T(8,128)(2,1)S(1)}, bf16[768,256]{1,0:T(8,128)(2,1)S(1)}, u32[]{:S(2)}, u32[]{:S(2)}) collective-permute-start(bf16[768,256]{1,0:T(8,128)(2,1)S(1)} %get-tuple-element.40), channel_id=1, source_target_pairs={{16,0},{65,1},{24,8},{73,9},{0,16},{81,17},{8,24},{89,25},{48,32},... | collective-permute-start | bytes 1179656 | tf_op jit(solution)/shard_map/ppermute | solution.py:33
  113.3 17.0 %collective-permute-start.22 = (bf16[192,1536]{1,0:T(8,128)(2,1)S(1)}, bf16[192,1536]{1,0:T(8,128)(2,1)S(1)}, u32[]{:S(2)}, u32[]{:S(2)}) collective-permute-start(bf16[192,1536]{1,0:T(8,128)(2,1)S(1)} %multiply_convert_fusion.refs_0_), channel_id=1, source_target_pairs={{96,0},{25,1},{104,8},{1,9},{112,16},{9,17},{120,24},{17,25},{0,32... | collective-permute-start | bytes 1769480 | tf_op jit(solution)/shard_map/ppermute | solution.py:37
  119.7 14.4 %collective-permute-start.21 = (bf16[192,1536]{1,0:T(8,128)(2,1)S(1)}, bf16[192,1536]{1,0:T(8,128)(2,1)S(1)}, u32[]{:S(2)}, u32[]{:S(2)}) collective-permute-start(bf16[192,1536]{1,0:T(8,128)(2,1)S(1)} %multiply_convert_fusion.refs_0_), channel_id=1, source_target_pairs={{64,0},{17,1},{72,8},{25,9},{80,16},{1,17},{88,24},{9,25},{96,32},... | collective-permute-start | bytes 1769480 | tf_op jit(solution)/shard_map/ppermute | solution.py:37
  123.7 15.6 %collective-permute-start.20 = (bf16[192,1536]{1,0:T(8,128)(2,1)S(1)}, bf16[192,1536]{1,0:T(8,128)(2,1)S(1)}, u32[]{:S(2)}, u32[]{:S(2)}) collective-permute-start(bf16[192,1536]{1,0:T(8,128)(2,1)S(1)} %multiply_convert_fusion.refs_0_), channel_id=1, source_target_pairs={{32,0},{9,1},{40,8},{17,9},{48,16},{25,17},{56,24},{1,25},{64,32},... | collective-permute-start | bytes 1769480 | tf_op jit(solution)/shard_map/ppermute | solution.py:37
  127.4 25.4 %collective-permute-start.45 = (f32[768,256]{1,0:T(8,128)S(1)}, f32[768,256]{1,0:T(8,128)S(1)}, u32[]{:S(2)}, u32[]{:S(2)}) collective-permute-start(f32[768,256]{1,0:T(8,128)S(1)} %convert_add_fusion), channel_id=1, source_target_pairs={{4,0},{6,2},{0,4},{2,6},{5,1},{7,3},{1,5},{3,7},{12,8},{14,10},{8,... | collective-permute-start | bytes 2359304 | tf_op jit(solution)/shard_map/ppermute | solution.py:45
  142.0 15.1 %collective-permute-start.30 = (bf16[768,256]{1,0:T(8,128)(2,1)S(1)}, bf16[768,256]{1,0:T(8,128)(2,1)S(1)}, u32[]{:S(2)}, u32[]{:S(2)}) collective-permute-start(bf16[768,256]{1,0:T(8,128)(2,1)S(1)} %get-tuple-element.30), channel_id=1, source_target_pairs={{24,0},{97,1},{0,8},{105,9},{8,16},{113,17},{16,24},{121,25},{56,3... | collective-permute-start | bytes 1179656 | tf_op jit(solution)/shard_map/ppermute | solution.py:33
  145.1 15.9 %collective-permute-start.31 = (bf16[768,256]{1,0:T(8,128)(2,1)S(1)}, bf16[768,256]{1,0:T(8,128)(2,1)S(1)}, u32[]{:S(2)}, u32[]{:S(2)}) collective-permute-start(bf16[768,256]{1,0:T(8,128)(2,1)S(1)} %get-tuple-element.31), channel_id=1, source_target_pairs={{8,0},{33,1},{16,8},{41,9},{24,16},{49,17},{0,24},{57,25},{40,32},... | collective-permute-start | bytes 1179656 | tf_op jit(solution)/shard_map/ppermute | solution.py:33
  (32 other events, 316.1 us)
